TPU v7x, 32 devices: a whole 2x2x4 slice. The times are simulated.
32 devices in a mesh: sp: 8 (over z, y), tp: 4 (over x, core).
Axes of the slice: x: 2, y: 2, z: 4, core: 2. Of those that a mesh axis runs over, the one named last changes fastest.
Arguments:
- inputs: bfloat16 [12288, 2048], P('sp'), may hold values from -6 to 6
- norm_gain: float32 [2048], replicated, may hold values from 0.1 to 1.9
- pool_weight: bfloat16 [2048, 1024], P(None, 'tp'), may hold values from -0.125 to 0.125
- query_weight: bfloat16 [2048, 1024], P(None, 'tp'), may hold values from -0.125 to 0.125
- forget_weight: bfloat16 [2048, 1024], P(None, 'tp'), may hold values from -0.125 to 0.125
- value_weight: bfloat16 [2048, 1024], P(None, 'tp'), may hold values from -0.125 to 0.125
- outgate_weight: bfloat16 [2048, 1024], P(None, 'tp'), may hold values from -0.125 to 0.125
- pool_mix: bfloat16 [4, 256, 256], P('tp'), may hold values from -0.375 to 0.375
- pool_scale: float32 [1024], P('tp'), may hold values from 0.1 to 1.9
- lower_bound: float32 [1024], P('tp'), may hold values from 0.9 to 1
- extra_decay: float32 [12288, 8], P('sp', 'tp'), may hold values from -1 to 0
- recur_gain: float32 [1024], P('tp'), may hold values from 0.1 to 1.9
- init_state: float32 [8, 128, 128], P('tp'), may hold values from -0.013531647 to 0.013531647
- out_pool: bfloat16 [1024, 2048], P('tp'), may hold values from -0.125 to 0.125
- out_recur: bfloat16 [1024, 2048], P('tp'), may hold values from -0.125 to 0.125
Outputs:
- mixed: bfloat16 [12288, 2048], P(('sp', 'tp'))
All inputs are finite; a program needn't handle non-finite values.
Results may differ from a plain program's by a relative error of at most 0.014.
Values may be sent and summed in bfloat16 or wider, within the bound.
No kernel may reach another device: no remote copies, remote signals or barrier semaphores. Data moves between devices by JAX's collectives and lax.ppermute only.
A program may use at most 128 MiB of HBM per device.

v0:
```python
import functools

import jax
import jax.numpy as jnp
from jax import lax
from jax.experimental import pallas as pl
from jax.experimental.pallas import tpu as pltpu
from jax.sharding import PartitionSpec as P

norm_eps = 1e-05
halo_rows = 16
chunk = 128
msg_pad = 16
f32 = jnp.float32
bf16 = jnp.bfloat16


def dot(a, b, dims=((1,), (0,))):
    return lax.dot_general(a, b, (dims, ((), ())), preferred_element_type=f32)


def norm_block(x, gain):
    wide = x.astype(f32)
    mean = jnp.mean(wide * wide, axis=-1, keepdims=True)
    return (wide * lax.rsqrt(mean + norm_eps) * gain).astype(bf16)


def sigmoid(x):
    return 1.0 / (1.0 + jnp.exp(-x))


def lower_triangle(size):
    row = lax.broadcasted_iota(jnp.int32, (size, size), 0)
    col = lax.broadcasted_iota(jnp.int32, (size, size), 1)
    return row >= col


def state_kernel(
    x_ref, gain_ref, fw_ref, vw_ref, lb_ref, extra_ref,
    normed_ref, key_ref, decay_ref, value_ref, start_ref, rows_ref, msg_ref,
    state, total,
):
    step = pl.program_id(0)
    heads, head_k = state.shape[0], state.shape[1]
    tile = x_ref.shape[0]

    @pl.when(step == 0)
    def _():
        state[...] = jnp.zeros_like(state)
        total[...] = jnp.zeros_like(total)

    normed = norm_block(x_ref[...], gain_ref[...])
    normed_ref[...] = normed
    forget = dot(normed, fw_ref[...])
    value = dot(normed, vw_ref[...]).astype(bf16)
    value_ref[...] = value
    gap = 1.0 - lb_ref[...]
    key = gap / (1.0 + jnp.exp(forget))
    extra = extra_ref[...]
    spread = jnp.concatenate(
        [jnp.broadcast_to(extra[:, h : h + 1], (tile, head_k)) for h in range(heads)], axis=1
    )
    log_f = jnp.log(1.0 - key) + spread
    high = log_f.astype(bf16)
    low = (log_f - high.astype(f32)).astype(bf16)
    triangle = lower_triangle(chunk).astype(f32).astype(bf16)
    for c in range(tile // chunk):
        span = slice(c * chunk, (c + 1) * chunk)
        cum = dot(triangle, high[span]) + dot(triangle, low[span])
        middle = cum[chunk // 2 - 1 : chunk // 2]
        last = cum[chunk - 1 :]
        decay_ref[span, :] = jnp.exp(cum - middle)
        key_dec = key[span] * jnp.exp(middle - cum)
        key_ref[span, :] = key_dec.astype(bf16)
        key_end = (key_dec * jnp.exp(last - middle)).astype(bf16)
        before = total[...]
        rows_ref[c] = jnp.concatenate(
            [jnp.exp(middle), jnp.exp(before), jnp.zeros((6, middle.shape[1]), f32)], axis=0
        )
        total[...] = before + last
        whole = jnp.exp(last)
        for h in range(heads):
            lanes = slice(h * head_k, (h + 1) * head_k)
            old = state[h]
            start_ref[c, h] = old.astype(bf16)
            contrib = dot(value[span, lanes], key_end[:, lanes], ((0,), (0,)))
            state[h] = old * whole[:, lanes] + contrib

    @pl.when(step == pl.num_programs(0) - 1)
    def _():
        decay = jnp.exp(total[...])
        high_part = decay.astype(bf16)
        low_part = (decay - high_part.astype(f32)).astype(bf16)
        for h in range(heads):
            lanes = slice(h * head_k, (h + 1) * head_k)
            msg_ref[h, :head_k, :] = state[h].astype(bf16)
            msg_ref[h, head_k:, :] = jnp.concatenate(
                [
                    high_part[:, lanes].astype(f32),
                    low_part[:, lanes].astype(f32),
                    jnp.zeros((msg_pad - 2, head_k), f32),
                ],
                axis=0,
            ).astype(bf16)


def local_kernel(
    place_ref, normed_ref, halo_ref, gain_ref, qw_ref, ow_ref, pw_ref, mix_ref, scale_ref,
    recur_gain_ref, key_ref, decay_ref, value_ref, start_ref, rows_ref,
    local_ref, qtot_ref, gate_ref, ypool_ref,
    tail, band,
):
    step = pl.program_id(0)
    tile = normed_ref.shape[0]
    head_k = start_ref.shape[-1]
    heads = start_ref.shape[1]
    first_pos = place_ref[0]
    window = place_ref[1]

    @pl.when(step == 0)
    def _():
        tail[...] = dot(norm_block(halo_ref[...], gain_ref[...]), pw_ref[...]).astype(bf16)
        row = lax.broadcasted_iota(jnp.int32, band.shape, 0)
        col = lax.broadcasted_iota(jnp.int32, band.shape, 1) - halo_rows
        back = row - col
        band[...] = ((back >= 0) & (back < window)).astype(f32).astype(bf16)

    normed = normed_ref[...]
    query = dot(normed, qw_ref[...])
    outgate = dot(normed, ow_ref[...])
    pool_in = dot(normed, pw_ref[...]).astype(bf16)
    gate_ref[...] = outgate * sigmoid(outgate) * recur_gain_ref[...]
    query = query * sigmoid(query)
    causal = lower_triangle(chunk)
    before = tail[...]
    for c in range(tile // chunk):
        span = slice(c * chunk, (c + 1) * chunk)
        part = pool_in[span]
        sums = dot(band[...], jnp.concatenate([before, part], axis=0))
        before = part[chunk - halo_rows :]
        position = (
            first_pos + step * tile + c * chunk
            + lax.broadcasted_iota(jnp.int32, (chunk, 1), 0)
        )
        count = jnp.minimum(position + 1, window).astype(f32)
        pooled = (sums / count - part.astype(f32)).astype(bf16)
        ypool_ref[span, :] = (dot(pooled, mix_ref[0]) * scale_ref[...]).astype(bf16)

        query_dec = query[span] * decay_ref[span, :]
        query_low = query_dec.astype(bf16)
        query_abs = query_dec * rows_ref[c, 0:1, :]
        qtot_ref[span, :] = (query_abs * rows_ref[c, 1:2, :]).astype(bf16)
        query_abs = query_abs.astype(bf16)
        for h in range(heads):
            lanes = slice(h * head_k, (h + 1) * head_k)
            scores = dot(query_low[:, lanes], key_ref[span, lanes], ((1,), (1,)))
            scores = jnp.where(causal, scores, 0.0).astype(bf16)
            within = dot(scores, value_ref[span, lanes])
            earlier = dot(query_abs[:, lanes], start_ref[c, h], ((1,), (1,)))
            local_ref[span, lanes] = within + earlier
    tail[...] = before


def output_kernel(
    place_ref, msgs_ref, init_ref, local_ref, qtot_ref, gate_ref, y_ref, carried
):
    head_k = init_ref.shape[-1]
    heads = init_ref.shape[0]
    devices = msgs_ref.shape[0]
    me = place_ref[2]

    @pl.when(pl.program_id(0) == 0)
    def _():
        for h in range(heads):
            def step(i, state):
                decay = (
                    msgs_ref[i, h, head_k : head_k + 1, :].astype(f32)
                    + msgs_ref[i, h, head_k + 1 : head_k + 2, :].astype(f32)
                )
                return state * decay + msgs_ref[i, h, :head_k, :].astype(f32)

            carried[h] = lax.fori_loop(0, me, step, init_ref[h].T).astype(bf16)

    for h in range(heads):
        lanes = slice(h * head_k, (h + 1) * head_k)
        recur = local_ref[:, lanes] + dot(qtot_ref[:, lanes], carried[h], ((1,), (1,)))
        mean = jnp.mean(recur * recur, axis=-1, keepdims=True)
        y_ref[:, lanes] = (recur * lax.rsqrt(mean + norm_eps) * gate_ref[:, lanes]).astype(bf16)


def fixed(*shape):
    return pl.BlockSpec(shape, lambda *_: (0,) * len(shape))


def moving(*shape):
    return pl.BlockSpec(shape, lambda i, *_: (i,) + (0,) * (len(shape) - 1))


limits = pltpu.CompilerParams(
    dimension_semantics=("arbitrary",), vmem_limit_bytes=56 * 1024 * 1024
)


def swapped(array, axis, bit):
    devices = lax.axis_size(axis)
    return lax.ppermute(array, axis, [(i, i ^ bit) for i in range(devices)])


def per_device(
    inputs, norm_gain, pool_weight, query_weight, forget_weight, value_weight, outgate_weight,
    pool_mix, pool_scale, lower_bound, extra_decay, recur_gain, init_state, out_pool, out_recur,
):
    rows, width = inputs.shape
    heads, head_k = init_state.shape[:2]
    channels = query_weight.shape[1]
    sp, tp = lax.axis_size("sp"), lax.axis_size("tp")
    sp_index, tp_index = lax.axis_index("sp"), lax.axis_index("tp")
    tile = 2 * chunk
    steps, chunks = rows // tile, tile // chunk
    gain = norm_gain[None]

    halo = lax.ppermute(
        inputs[rows - halo_rows :], "sp", [(i, i + 1) for i in range(sp - 1)]
    )
    sds = jax.ShapeDtypeStruct
    normed, key_dec, decay, value, starts, row_info, msg = pl.pallas_call(
        state_kernel,
        grid=(steps,),
        in_specs=[
            moving(tile, width), fixed(1, width), fixed(width, channels), fixed(width, channels),
            fixed(1, channels), moving(tile, heads),
        ],
        out_specs=[
            moving(tile, width), moving(tile, channels), moving(tile, channels),
            moving(tile, channels), moving(chunks, heads, head_k, head_k),
            moving(chunks, 8, channels), fixed(heads, head_k + msg_pad, head_k),
        ],
        out_shape=[
            sds((rows, width), bf16), sds((rows, channels), bf16), sds((rows, channels), f32),
            sds((rows, channels), bf16), sds((rows // chunk, heads, head_k, head_k), bf16),
            sds((rows // chunk, 8, channels), f32), sds((heads, head_k + msg_pad, head_k), bf16),
        ],
        scratch_shapes=[pltpu.VMEM((heads, head_k, head_k), f32), pltpu.VMEM((1, channels), f32)],
        compiler_params=limits,
        name="state_kernel",
    )(inputs, gain, forget_weight, value_weight, lower_bound[None], extra_decay)

    msgs = lax.all_to_all(
        jnp.broadcast_to(msg[None], (sp,) + msg.shape), "sp", split_axis=0, concat_axis=0,
        tiled=True,
    )
    window = jnp.left_shift(2, tp_index * pool_mix.shape[0])
    place = jnp.stack([sp_index * rows, window, sp_index]).astype(jnp.int32)
    smem = pl.BlockSpec(memory_space=pltpu.SMEM)
    local, qtot, gate, y_pool = pl.pallas_call(
        local_kernel,
        grid=(steps,),
        in_specs=[
            smem, moving(tile, width), fixed(halo_rows, width), fixed(1, width),
            fixed(width, channels), fixed(width, channels), fixed(width, channels),
            fixed(*pool_mix.shape), fixed(1, channels), fixed(1, channels),
            moving(tile, channels), moving(tile, channels), moving(tile, channels),
            moving(chunks, heads, head_k, head_k), moving(chunks, 8, channels),
        ],
        out_specs=[moving(tile, channels)] * 4,
        out_shape=[
            sds((rows, channels), f32), sds((rows, channels), bf16),
            sds((rows, channels), f32), sds((rows, channels), bf16),
        ],
        scratch_shapes=[
            pltpu.VMEM((halo_rows, channels), bf16),
            pltpu.VMEM((chunk, chunk + halo_rows), bf16),
        ],
        compiler_params=limits,
        name="local_kernel",
    )(
        place, normed, halo, gain, query_weight, outgate_weight, pool_weight, pool_mix,
        pool_scale[None], recur_gain[None], key_dec, decay, value, starts, row_info,
    )
    y_recur = pl.pallas_call(
        output_kernel,
        grid=(steps,),
        in_specs=[
            smem, fixed(*msgs.shape), fixed(*init_state.shape), moving(tile, channels),
            moving(tile, channels), moving(tile, channels),
        ],
        out_specs=moving(tile, channels),
        out_shape=sds((rows, channels), bf16),
        scratch_shapes=[pltpu.VMEM((heads, head_k, head_k), bf16)],
        compiler_params=limits,
        name="output_kernel",
    )(place, msgs, init_state, local, qtot, gate)

    def whole(weight):
        bit = 1
        stacked = weight[None]
        order = [0]
        while bit < tp:
            stacked = jnp.concatenate([stacked, swapped(stacked, "tp", tp // 2 // bit)], axis=0)
            order = order + [o ^ (tp // 2 // bit) for o in order]
            bit *= 2
        return stacked, order

    w_pool, order = whole(out_pool)
    w_recur, _ = whole(out_recur)
    pool_seen = lax.all_to_all(
        y_pool.reshape(tp, rows // tp, channels), "tp", split_axis=0, concat_axis=0, tiled=True
    )
    recur_seen = lax.all_to_all(
        y_recur.reshape(tp, rows // tp, channels), "tp", split_axis=0, concat_axis=0, tiled=True
    )
    def project(seen, weights):
        total = None
        for k, offset in enumerate(order):
            piece = lax.dynamic_index_in_dim(seen, tp_index ^ offset, 0, keepdims=False)
            term = jnp.dot(piece, weights[k], preferred_element_type=f32)
            total = term if total is None else total + term
        return total

    mixed = project(pool_seen, w_pool) + project(recur_seen, w_recur)
    return mixed.astype(bf16)


def solution(mesh):
    in_specs = (
        P("sp", None), P(), P(None, "tp"), P(None, "tp"), P(None, "tp"), P(None, "tp"),
        P(None, "tp"), P("tp", None, None), P("tp"), P("tp"), P("sp", "tp"), P("tp"),
        P("tp", None, None), P("tp", None), P("tp", None),
    )
    return jax.shard_map(
        per_device, mesh=mesh, in_specs=in_specs, out_specs=P(("sp", "tp"), None),
        check_vma=False,
    )
```

profile of v0, /device:TPU:16, one launch (start us, length us, event | category | flops | bytes accessed | tf_op | source)
XLA Modules:
  0.0 104.1 jit_solution(14440826186279962571)
XLA Ops:
  0.0 1.5 %collective-permute-start.3 = (bf16[1,256,2048]{2,1,0:T(8,128)(2,1)}, bf16[1,256,2048]{2,1,0:T(8,128)(2,1)S(1)}, u32[]{:S(2)}, u32[]{:S(2)}) collective-permute-start(bf16[1,256,2048]{2,1,0:T(8,128)(2,1)} %bitcast.59), channel_id=1, source_target_pairs={{0,2},{1,3},{2,0},{3,1},{4,6},{5,7},{6,4},{7,5},{8,10},{9,11},{10,... | collective-permute-start | bytes 3145736 | tf_op jit(solution)/shard_map/ppermute | solution.py:206
  2.0 1.9 %copy.16.extra_ref = f32[1536,2]{1,0:T(8,128)} copy(f32[1536,2]{0,1:T(2,128)} %param.25) | data formatting | bytes 24576 | tf_op args[10]
  3.9 13.5 %state_kernel.1 = (bf16[1536,2048]{1,0:T(8,128)(2,1)}, bf16[1536,256]{1,0:T(8,128)(2,1)}, f32[1536,256]{1,0:T(8,128)}, bf16[1536,256]{1,0:T(8,128)(2,1)}, bf16[1...) custom-call(bf16[1536,2048]{1,0:T(8,128)(2,1)} %x_ref.1, f32[1,2048]{1,0:T(1,128)} %bitcast.63, ...), custom_call_target="tpu_custom_call" | custom-call | tf_op jit(solution)/shard_map/state_kernel/pallas_call | solution.py:226
  17.5 1.8 %broadcast_in_dim.29 = bf16[8,2,144,128]{3,2,1,0:T(8,128)(2,1)} broadcast(bf16[2,144,128]{2,1,0:T(8,128)(2,1)} %get-tuple-element.23), dimensions={1,2,3} | broadcast | bytes 663552 | tf_op jit(solution)/shard_map/broadcast_in_dim | solution.py:249
  19.2 6.2 %all-to-all-start.1 = ((bf16[8,2,144,128]{3,2,1,0:T(8,128)(2,1)}), bf16[8,2,144,128]{3,2,1,0:T(8,128)(2,1)}, u32[]{:S(2)}, u32[]{:S(2)}) async-start(bf16[8,2,144,128]{3,2,1,0:T(8,128)(2,1)} %broadcast_in_dim.29), calls=%async_computation.1 | async-start | bytes 1179648 | tf_op jit(solution)/shard_map/all_to_all | solution.py:248
  26.2 3.4 %collective-permute-start = (bf16[16,2048]{1,0:T(8,128)(2,1)S(1)}, bf16[16,2048]{1,0:T(8,128)(2,1)S(1)}, u32[]{:S(2)}, u32[]{:S(2)}) collective-permute-start(bf16[16,2048]{1,0:T(8,128)(2,1)S(1)} %slice.15), channel_id=1, source_target_pairs={{0,4},{4,8},{8,12},{12,16},{16,20},{20,24},{24,28},{1,5},{5,9},{9,... | collective-permute-start | bytes 196616 | tf_op jit(solution)/shard_map/ppermute | solution.py:222
  29.7 1.6 %pad_maximum_fusion.1 = bf16[2,256,2048]{2,1,0:T(8,128)(2,1)} fusion(bf16[1,256,2048]{2,1,0:T(8,128)(2,1)S(1)} %collective-permute-done.3, bf16[1,256,2048]{2,1,0:T(8,128)(2,1)S(1)} %bitcast.60), kind=kLoop, calls=%fused_computation.2 | loop fusion | flops 1048576 | bytes 4194304 | tf_op jit(solution)/shard_map/concatenate | solution.py:299
  31.9 8.8 %collective-permute-done.halo_ref = bf16[16,2048]{1,0:T(8,128)(2,1)S(1)} collective-permute-done((bf16[16,2048]{1,0:T(8,128)(2,1)S(1)}, bf16[16,2048]{1,0:T(8,128)(2,1)S(1)}, u32[]{:S(2)}, u32[]{:S(2)}) %collective-permute-start) | collective-permute-done | bytes 65568 | tf_op jit(solution)/shard_map/ppermute | solution.py:222
  41.3 17.5 %local_kernel.1 = (f32[1536,256]{1,0:T(8,128)}, bf16[1536,256]{1,0:T(8,128)(2,1)}, f32[1536,256]{1,0:T(8,128)}, bf16[1536,256]{1,0:T(8,128)(2,1)}) custom-call(s32[3]{0:T(128)} %pad_add_fusion.place_ref, bf16[1536,2048]{1,0:T(8,128)(2,1)} %get-tuple-element.16.normed_ref, bf16[16,2048]{1,0:T(8,128)(2,1)} %copy-done.9, f32[1,2048]{1,0:T(1,128)} %bitcast.64, ...), custom_call_target="tpu_custom_call" | custom-call | tf_op jit(solution)/shard_map/local_kernel/pallas_call | solution.py:255
  58.9 3.5 %all-to-all-start = ((bf16[4,384,256]{2,1,0:T(8,128)(2,1)}), bf16[4,384,256]{2,1,0:T(8,128)(2,1)S(1)}, u32[]{:S(2)}, u32[]{:S(2)}) async-start(bf16[4,384,256]{2,1,0:T(8,128)(2,1)} %bitcast.62), calls=%async_computation | async-start | bytes 1572864 | tf_op jit(solution)/shard_map/all_to_all | solution.py:306
  62.4 1.7 %pad_maximum_fusion = bf16[2,256,2048]{2,1,0:T(8,128)(2,1)} fusion(bf16[1,256,2048]{2,1,0:T(8,128)(2,1)S(1)} %collective-permute-done.1, bf16[1,256,2048]{2,1,0:T(8,128)(2,1)S(1)} %bitcast.58), kind=kLoop, calls=%fused_computation.1 | loop fusion | flops 1048576 | bytes 4194304 | tf_op jit(solution)/shard_map/concatenate | solution.py:299
  64.6 6.3 %output_kernel.1 = bf16[1536,256]{1,0:T(8,128)(2,1)} custom-call(s32[3]{0:T(128)} %pad_add_fusion.place_ref, bf16[8,2,144,128]{3,2,1,0:T(8,128)(2,1)} %all-to-all-done.1.msgs_ref, f32[2,128,128]{2,1,0:T(8,128)} %init_ref.1, f32[1536,256]{1,0:T(8,128)} %get-tuple-element.24.local_ref, bf16[1536,256]{1,0:T(8,128)(2,1)} %get-tuple-element.25.qtot_ref, ...), custom_call_target="tpu_custom_call" | custom-call | tf_op jit(solution)/shard_map/output_kernel/pallas_call | solution.py:280
  70.9 3.1 %all-to-all-done = bf16[4,384,256]{2,1,0:T(8,128)(2,1)S(1)} async-done(((bf16[4,384,256]{2,1,0:T(8,128)(2,1)}), bf16[4,384,256]{2,1,0:T(8,128)(2,1)S(1)}, u32[]{:S(2)}, u32[]{:S(2)}) %all-to-all-start) | async-done | bytes 786464 | tf_op jit(solution)/shard_map/all_to_all | solution.py:306
  74.0 0.9 copy-done.7
  74.9 4.2 %all-to-all-start.2 = ((bf16[4,384,256]{2,1,0:T(8,128)(2,1)}), bf16[4,384,256]{2,1,0:T(8,128)(2,1)}, u32[]{:S(2)}, u32[]{:S(2)}) async-start(bf16[4,384,256]{2,1,0:T(8,128)(2,1)} %bitcast.61), calls=%async_computation.2 | async-start | bytes 1572864 | tf_op jit(solution)/shard_map/all_to_all | solution.py:309
  79.1 2.0 %fusion.16 = f32[384,2048]{1,0:T(8,128)S(1)} fusion(bf16[256,2048]{1,0:T(8,128)(2,1)} %param.28, bf16[4,384,256]{2,1,0:T(8,128)(2,1)} %copy-done.7, s32[]{:T(128)S(6)} %select_n.17), kind=kOutput, calls=%fused_computation.23 | convolution fusion | flops 402653184 | bytes 4390916 | tf_op jit(solution)/shard_map/dot_general | solution.py:316
  81.1 3.2 %fusion.6 = f32[384,2048]{1,0:T(8,128)} fusion(bf16[1,256,2048]{2,1,0:T(8,128)(2,1)S(1)} %copy-done.6, bf16[4,384,256]{2,1,0:T(8,128)(2,1)} %copy-done.7, s32[]{:T(128)S(6)} %select_n.18), kind=kOutput, calls=%fused_computation.13 | convolution fusion | flops 402653184 | bytes 4390916 | tf_op jit(solution)/shard_map/dot_general | solution.py:316
  84.3 6.4 %all-to-all-done.2 = bf16[4,384,256]{2,1,0:T(8,128)(2,1)} async-done(((bf16[4,384,256]{2,1,0:T(8,128)(2,1)}), bf16[4,384,256]{2,1,0:T(8,128)(2,1)}, u32[]{:S(2)}, u32[]{:S(2)}) %all-to-all-start.2) | async-done | bytes 786464 | tf_op jit(solution)/shard_map/all_to_all | solution.py:309
  90.8 2.0 %fusion.4 = f32[384,2048]{1,0:T(8,128)S(1)} fusion(bf16[1,256,2048]{2,1,0:T(8,128)(2,1)} %copy-done.4, bf16[4,384,256]{2,1,0:T(8,128)(2,1)} %all-to-all-done.2, s32[]{:T(128)S(6)} %select_n.18), kind=kOutput, calls=%fused_computation.11 | convolution fusion | flops 402653184 | bytes 4390916 | tf_op jit(solution)/shard_map/dot_general | solution.py:316
  92.8 1.5 %fusion.11 = f32[384,2048]{1,0:T(8,128)S(1)} fusion(bf16[256,2048]{1,0:T(8,128)(2,1)S(1)} %copy-done.3, bf16[4,384,256]{2,1,0:T(8,128)(2,1)} %all-to-all-done.2, s32[]{:T(128)S(6)} %select_n.17), kind=kOutput, calls=%fused_computation.18 | convolution fusion | flops 402653184 | bytes 4390916 | tf_op jit(solution)/shard_map/dot_general | solution.py:316
  94.3 2.0 %fusion.1 = f32[384,2048]{1,0:T(8,128)S(1)} fusion(bf16[2,256,2048]{2,1,0:T(8,128)(2,1)} %collective-permute-done.4, bf16[4,384,256]{2,1,0:T(8,128)(2,1)} %all-to-all-done.2, s32[]{:T(128)S(6)} %select_n.19), kind=kOutput, calls=%fused_computation.6 | convolution fusion | flops 402653184 | bytes 4390916 | tf_op jit(solution)/shard_map/dot_general | solution.py:316
  96.3 1.8 %fusion.3 = f32[384,2048]{1,0:T(8,128)S(1)} fusion(bf16[2,256,2048]{2,1,0:T(8,128)(2,1)} %collective-permute-done.2, bf16[4,384,256]{2,1,0:T(8,128)(2,1)S(1)} %copy-done.8, s32[]{:T(128)S(6)} %select_n.19), kind=kOutput, calls=%fused_computation.10 | convolution fusion | flops 402653184 | bytes 4390916 | tf_op jit(solution)/shard_map/dot_general | solution.py:316
  98.1 2.0 %fusion.2 = f32[384,2048]{1,0:T(8,128)S(1)} fusion(bf16[2,256,2048]{2,1,0:T(8,128)(2,1)} %collective-permute-done.2, bf16[4,384,256]{2,1,0:T(8,128)(2,1)S(1)} %copy-done.8, s32[]{:T(128)S(6)} %select_n.20), kind=kOutput, calls=%fused_computation.8 | convolution fusion | flops 402653184 | bytes 4390916 | tf_op jit(solution)/shard_map/dot_general | solution.py:316
  100.3 3.8 %add_convert_fusion = bf16[384,2048]{1,0:T(8,128)(2,1)} fusion(f32[384,2048]{1,0:T(8,128)S(1)} %fusion.1, f32[384,2048]{1,0:T(8,128)S(1)} %fusion.11, f32[384,2048]{1,0:T(8,128)S(1)} %fusion.4, f32[384,2048]{1,0:T(8,128)S(1)} %fusion.2, f32[384,2048]{1,0:T(8,128)S(1)} %fusion.3, f32[384,2048]{1,0:T(8,128)S(1)} %fusion.16, f32[384,2048]{1,0:T(8,128)S(1)} %copy-done, ...), kind=kOutput, calls=%fused_computation | convolution fusion | flops 408944640 | bytes 24838148 | tf_op jit(solution)/shard_map/dot_general | solution.py:316
  (29 shorter events, 3.4 us)
Async XLA Ops:
  0.0 29.6 %collective-permute-start.3 = (bf16[1,256,2048]{2,1,0:T(8,128)(2,1)}, bf16[1,256,2048]{2,1,0:T(8,128)(2,1)S(1)}, u32[]{:S(2)}, u32[]{:S(2)}) collective-permute-start(bf16[1,256,2048]{2,1,0:T(8,128)(2,1)} %bitcast.59), channel_id=1, source_target_pairs={{0,2},{1,3},{2,0},{3,1},{4,6},{5,7},{6,4},{7,5},{8,10},{9,11},{10,... | collective-permute-start | bytes 3145736 | tf_op jit(solution)/shard_map/ppermute | solution.py:206
  1.5 60.9 %collective-permute-start.1 = (bf16[1,256,2048]{2,1,0:T(8,128)(2,1)}, bf16[1,256,2048]{2,1,0:T(8,128)(2,1)S(1)}, u32[]{:S(2)}, u32[]{:S(2)}) collective-permute-start(bf16[1,256,2048]{2,1,0:T(8,128)(2,1)} %bitcast.57), channel_id=1, source_target_pairs={{0,2},{1,3},{2,0},{3,1},{4,6},{5,7},{6,4},{7,5},{8,10},{9,11},{10,... | collective-permute-start | bytes 3145736 | tf_op jit(solution)/shard_map/ppermute | solution.py:206
  3.9 25.7 %copy-start.2 = (bf16[256,2048]{1,0:T(8,128)(2,1)S(1)}, bf16[256,2048]{1,0:T(8,128)(2,1)}, u32[]{:S(2)}) copy-start(bf16[256,2048]{1,0:T(8,128)(2,1)} %param.29) | copy-start | bytes 3145732
  19.2 39.7 %all-to-all-start.1 = ((bf16[8,2,144,128]{3,2,1,0:T(8,128)(2,1)}), bf16[8,2,144,128]{3,2,1,0:T(8,128)(2,1)}, u32[]{:S(2)}, u32[]{:S(2)}) async-start(bf16[8,2,144,128]{3,2,1,0:T(8,128)(2,1)} %broadcast_in_dim.29), calls=%async_computation.1 | async-start | bytes 1179648 | tf_op jit(solution)/shard_map/all_to_all | solution.py:248
  26.2 14.5 %collective-permute-start = (bf16[16,2048]{1,0:T(8,128)(2,1)S(1)}, bf16[16,2048]{1,0:T(8,128)(2,1)S(1)}, u32[]{:S(2)}, u32[]{:S(2)}) collective-permute-start(bf16[16,2048]{1,0:T(8,128)(2,1)S(1)} %slice.15), channel_id=1, source_target_pairs={{0,4},{4,8},{8,12},{12,16},{16,20},{20,24},{24,28},{1,5},{5,9},{9,... | collective-permute-start | bytes 196616 | tf_op jit(solution)/shard_map/ppermute | solution.py:222
  29.6 29.2 %copy-start.4 = (bf16[1,256,2048]{2,1,0:T(8,128)(2,1)}, bf16[1,256,2048]{2,1,0:T(8,128)(2,1)S(1)}, u32[]{:S(2)}) copy-start(bf16[1,256,2048]{2,1,0:T(8,128)(2,1)S(1)} %collective-permute-done.3) | copy-start | bytes 3145732
  31.3 63.0 %collective-permute-start.4 = (bf16[2,256,2048]{2,1,0:T(8,128)(2,1)}, bf16[2,256,2048]{2,1,0:T(8,128)(2,1)}, u32[]{:S(2)}, u32[]{:S(2)}) collective-permute-start(bf16[2,256,2048]{2,1,0:T(8,128)(2,1)} %pad_maximum_fusion.1), channel_id=1, source_target_pairs={{0,1},{1,0},{2,3},{3,2},{4,5},{5,4},{6,7},{7,6},{8,9},{9,8},{10,11... | collective-permute-start | bytes 6291464 | tf_op jit(solution)/shard_map/ppermute | solution.py:206
  40.7 0.6 copy-start.9
  41.3 21.1 %copy-start.1 = (bf16[256,2048]{1,0:T(8,128)(2,1)S(1)}, bf16[256,2048]{1,0:T(8,128)(2,1)}, u32[]{:S(2)}) copy-start(bf16[256,2048]{1,0:T(8,128)(2,1)} %param.28) | copy-start | bytes 3145732
  58.9 15.1 %all-to-all-start = ((bf16[4,384,256]{2,1,0:T(8,128)(2,1)}), bf16[4,384,256]{2,1,0:T(8,128)(2,1)S(1)}, u32[]{:S(2)}, u32[]{:S(2)}) async-start(bf16[4,384,256]{2,1,0:T(8,128)(2,1)} %bitcast.62), calls=%async_computation | async-start | bytes 1572864 | tf_op jit(solution)/shard_map/all_to_all | solution.py:306
  62.4 8.5 %copy-start.5 = (bf16[1,256,2048]{2,1,0:T(8,128)(2,1)}, bf16[1,256,2048]{2,1,0:T(8,128)(2,1)S(1)}, u32[]{:S(2)}) copy-start(bf16[1,256,2048]{2,1,0:T(8,128)(2,1)S(1)} %collective-permute-done.1) | copy-start | bytes 3145732
  64.2 32.1 %collective-permute-start.2 = (bf16[2,256,2048]{2,1,0:T(8,128)(2,1)}, bf16[2,256,2048]{2,1,0:T(8,128)(2,1)}, u32[]{:S(2)}, u32[]{:S(2)}) collective-permute-start(bf16[2,256,2048]{2,1,0:T(8,128)(2,1)} %pad_maximum_fusion), channel_id=1, source_target_pairs={{0,1},{1,0},{2,3},{3,2},{4,5},{5,4},{6,7},{7,6},{8,9},{9,8},{10,11... | collective-permute-start | bytes 6291464 | tf_op jit(solution)/shard_map/ppermute | solution.py:206
  74.0 0.9 copy-start.7
  74.9 15.9 %all-to-all-start.2 = ((bf16[4,384,256]{2,1,0:T(8,128)(2,1)}), bf16[4,384,256]{2,1,0:T(8,128)(2,1)}, u32[]{:S(2)}, u32[]{:S(2)}) async-start(bf16[4,384,256]{2,1,0:T(8,128)(2,1)} %bitcast.61), calls=%async_computation.2 | async-start | bytes 1572864 | tf_op jit(solution)/shard_map/all_to_all | solution.py:309
  79.1 2.0 %copy-start.6 = (bf16[1,256,2048]{2,1,0:T(8,128)(2,1)S(1)}, bf16[1,256,2048]{2,1,0:T(8,128)(2,1)}, u32[]{:S(2)}) copy-start(bf16[1,256,2048]{2,1,0:T(8,128)(2,1)} %copy-done.5) | copy-start | bytes 3145732
  90.8 2.0 %copy-start.3 = (bf16[256,2048]{1,0:T(8,128)(2,1)S(1)}, bf16[256,2048]{1,0:T(8,128)(2,1)}, u32[]{:S(2)}) copy-start(bf16[256,2048]{1,0:T(8,128)(2,1)} %param.29) | copy-start | bytes 3145732
  94.3 2.0 %copy-start.8 = (bf16[4,384,256]{2,1,0:T(8,128)(2,1)S(1)}, bf16[4,384,256]{2,1,0:T(8,128)(2,1)}, u32[]{:S(2)}) copy-start(bf16[4,384,256]{2,1,0:T(8,128)(2,1)} %copy-done.7) | copy-start | bytes 2359300
  98.1 2.2 %copy-start = (f32[384,2048]{1,0:T(8,128)S(1)}, f32[384,2048]{1,0:T(8,128)}, u32[]{:S(2)}) copy-start(f32[384,2048]{1,0:T(8,128)} %fusion.6) | copy-start | bytes 9437188
where the time goes:
time: 105 us; the launch traced here: 104 us
  Pallas kernels  37.3 us (36%)
  starting transfers between devices  19.7 us (19%)
  waiting for transfers between devices  18.3 us (17%)
  matrix products  18.2 us (17%)
  local copies, waits for them, and re-layouts  6.3 us (6%)
  other arithmetic  3.98 us (4%)
    dot_general x8, matrix products, project(): term = jnp.dot(piece, weights[k], preferred_element_type=f32)  18.2 us
    pallas_call x1, Pallas kernels, per_device(): pl.pallas_call(local_kernel, grid=(steps,), in_specs=[smem, moving(tile,...  17.5 us
    pallas_call x1, Pallas kernels, per_device(): pl.pallas_call(state_kernel, grid=(steps,), in_specs=[moving(tile, width)...  13.5 us
    ppermute x1, waiting for transfers between devices, per_device(): lax.ppermute(inputs[rows - halo_rows:], 'sp', [(i, i + 1) for i in range(...  8.8 us
    all_to_all x1, waiting for transfers between devices, per_device(): lax.all_to_all(y_recur.reshape(tp, rows // tp, channels), 'tp', split_axi...  6.44 us
    pallas_call x1, Pallas kernels, per_device(): pl.pallas_call(output_kernel, grid=(steps,), in_specs=[smem, fixed(*msgs....  6.28 us
    all_to_all x1, starting transfers between devices, per_device(): lax.all_to_all(jnp.broadcast_to(msg[None], (sp,) + msg.shape), 'sp', spli...  6.17 us
    all_to_all x1, starting transfers between devices, per_device(): lax.all_to_all(y_recur.reshape(tp, rows // tp, channels), 'tp', split_axi...  4.2 us
  transfers between devices with their start and end apart: 8, of which 3 were waited for; matrix products, arithmetic and copies ran while one was open for 18% of the time, Pallas kernels for 36%

commit v1 on v0

v1 whole, which is shorter than its diff:
```python
import functools

import jax
import jax.numpy as jnp
from jax import lax
from jax.experimental import pallas as pl
from jax.experimental.pallas import tpu as pltpu
from jax.sharding import PartitionSpec as P


norm_eps = 1e-05
halo_rows = 16
chunk = 128
msg_pad = 16
f32 = jnp.float32
bf16 = jnp.bfloat16


def dot(a, b, dims=((1,), (0,))):
    return lax.dot_general(a, b, (dims, ((), ())), preferred_element_type=f32)


def sigmoid(x):
    return 1.0 / (1.0 + jnp.exp(-x))


def lower_triangle(size):
    row = lax.broadcasted_iota(jnp.int32, (size, size), 0)
    col = lax.broadcasted_iota(jnp.int32, (size, size), 1)
    return row >= col


def fold_gain(gain_ref, weight_refs, folded):
    lanes = gain_ref.shape[1]
    for b in range(gain_ref.shape[0]):
        rows = slice(b * lanes, (b + 1) * lanes)
        column = jnp.broadcast_to(gain_ref[b : b + 1, :], (lanes, lanes)).T
        at = 0
        for ref in weight_refs:
            for j in range(0, ref.shape[1], lanes):
                part = ref[rows, j : j + lanes].astype(f32) * column
                folded[rows, at : at + lanes] = part.astype(bf16)
                at += lanes


def row_scale(x):
    wide = x.astype(f32)
    return lax.rsqrt(jnp.mean(wide * wide, axis=-1, keepdims=True) + norm_eps)


def split(x):
    high = x.astype(bf16)
    return high, (x - high.astype(f32)).astype(bf16)


def stage_rows(stage, first, value):
    quarter = stage.shape[1]
    slot = (first // quarter) ^ lax.axis_index("tp")
    at = pl.multiple_of(first % quarter, chunk)
    stage[slot, pl.ds(at, value.shape[0]), :] = value


def unstage(stage, refs):
    @pl.when(pl.program_id(0) == pl.num_programs(0) - 1)
    def _():
        for k, ref in enumerate(refs):
            ref[...] = stage[k]


def state_kernel(
    x_ref, gain_ref, fw_ref, vw_ref, lb_ref, extra_ref,
    scale_ref, key_ref, decay_ref, value_ref, start_ref, rows_ref, msg_ref,
    folded, state, total,
):
    step = pl.program_id(0)
    heads, head_k = state.shape[0], state.shape[1]
    tile = x_ref.shape[0]
    channels = fw_ref.shape[1]

    @pl.when(step == 0)
    def _():
        state[...] = jnp.zeros_like(state)
        total[...] = jnp.zeros_like(total)
        fold_gain(gain_ref, (fw_ref, vw_ref), folded)

    x = x_ref[...]
    scale = jnp.broadcast_to(row_scale(x), scale_ref.shape)
    scale_ref[...] = scale
    raw = dot(x, folded[...])
    scales = jnp.concatenate([scale] * (channels // scale.shape[1]), axis=1)
    forget = raw[:, :channels] * scales
    value = (raw[:, channels:] * scales).astype(bf16)
    value_ref[...] = value
    gap = 1.0 - lb_ref[...]
    key = gap / (1.0 + jnp.exp(forget))
    extra_high, extra_low = split(extra_ref[...])
    pick = (
        lax.broadcasted_iota(jnp.int32, (heads, channels), 1) // head_k
        == lax.broadcasted_iota(jnp.int32, (heads, channels), 0)
    ).astype(f32).astype(bf16)
    first = ((0,), (0,))
    log_f = jnp.log(1.0 - key) + (dot(extra_high, pick, first) + dot(extra_low, pick, first))
    high, low = split(log_f)
    triangle = lower_triangle(chunk).astype(f32).astype(bf16)
    for c in range(tile // chunk):
        span = slice(c * chunk, (c + 1) * chunk)
        cum = dot(triangle, high[span]) + dot(triangle, low[span])
        middle = cum[chunk // 2 - 1 : chunk // 2]
        last = cum[chunk - 1 :]
        decay_ref[span, :] = jnp.exp(cum - middle).astype(bf16)
        key_dec = key[span] * jnp.exp(middle - cum)
        key_ref[span, :] = key_dec.astype(bf16)
        key_end = (key_dec * jnp.exp(last - middle)).astype(bf16)
        before = total[...]
        rows_ref[c] = jnp.concatenate(
            [jnp.exp(middle), jnp.exp(before), jnp.zeros((6, middle.shape[1]), f32)], axis=0
        )
        total[...] = before + last
        whole = jnp.exp(last)
        for h in range(heads):
            lanes = slice(h * head_k, (h + 1) * head_k)
            old = state[h]
            start_ref[c, h] = old.astype(bf16)
            contrib = dot(value[span, lanes], key_end[:, lanes], ((0,), (0,)))
            state[h] = old * whole[:, lanes] + contrib

    @pl.when(step == pl.num_programs(0) - 1)
    def _():
        decay_high, decay_low = split(jnp.exp(total[...]))
        for h in range(heads):
            lanes = slice(h * head_k, (h + 1) * head_k)
            ending = state[h].astype(bf16)
            decays = jnp.concatenate(
                [
                    decay_high[:, lanes].astype(f32),
                    decay_low[:, lanes].astype(f32),
                    jnp.zeros((msg_pad - 2, head_k), f32),
                ],
                axis=0,
            ).astype(bf16)
            for i in range(msg_ref.shape[0]):
                msg_ref[i, h, :head_k, :] = ending
                msg_ref[i, h, head_k:, :] = decays


def local_kernel(
    x_ref, halo_ref, gain_ref, qw_ref, ow_ref, pw_ref, mix_ref, pool_scale_ref,
    recur_gain_ref, scale_ref, key_ref, decay_ref, value_ref, start_ref, rows_ref,
    local_ref, qtot_ref, gate_ref, *rest,
):
    ypool_refs, (folded, tail, band, stage) = rest[:-4], rest[-4:]
    step = pl.program_id(0)
    tile = x_ref.shape[0]
    channels = qw_ref.shape[1]
    head_k = start_ref.shape[-1]
    heads = start_ref.shape[1]
    first_pos = lax.axis_index("sp") * (tile * pl.num_programs(0))
    window = jnp.left_shift(2, lax.axis_index("tp") * mix_ref.shape[0])

    @pl.when(step == 0)
    def _():
        fold_gain(gain_ref, (qw_ref, ow_ref, pw_ref), folded)
        halo = halo_ref[...]
        tail[...] = (dot(halo, folded[:, 2 * channels :]) * row_scale(halo)).astype(bf16)
        row = lax.broadcasted_iota(jnp.int32, band.shape, 0)
        col = lax.broadcasted_iota(jnp.int32, band.shape, 1) - halo_rows
        back = row - col
        band[...] = ((back >= 0) & (back < window)).astype(f32).astype(bf16)

    raw = dot(x_ref[...], folded[...])
    scale = scale_ref[...]
    scales = jnp.concatenate([scale] * (channels // scale.shape[1]), axis=1)
    query = raw[:, :channels] * scales
    outgate = raw[:, channels : 2 * channels] * scales
    pool_in = (raw[:, 2 * channels :] * scales).astype(bf16)
    gate_ref[...] = (outgate * sigmoid(outgate) * recur_gain_ref[...]).astype(bf16)
    query = query * sigmoid(query)
    causal = lower_triangle(chunk)
    before = tail[...]
    for c in range(tile // chunk):
        span = slice(c * chunk, (c + 1) * chunk)
        part = pool_in[span]
        sums = dot(band[...], jnp.concatenate([before, part], axis=0))
        before = part[chunk - halo_rows :]
        position = (
            first_pos + step * tile + c * chunk
            + lax.broadcasted_iota(jnp.int32, (chunk, 1), 0)
        )
        count = jnp.minimum(position + 1, window).astype(f32)
        pooled = (sums * (1.0 / count) - part.astype(f32)).astype(bf16)
        y_pool = (dot(pooled, mix_ref[0]) * pool_scale_ref[...]).astype(bf16)
        stage_rows(stage, step * tile + c * chunk, y_pool)

        query_dec = query[span] * decay_ref[span, :].astype(f32)
        query_low = query_dec.astype(bf16)
        query_abs = query_dec * rows_ref[c, 0:1, :]
        qtot_ref[span, :] = (query_abs * rows_ref[c, 1:2, :]).astype(bf16)
        query_abs = query_abs.astype(bf16)
        for h in range(heads):
            lanes = slice(h * head_k, (h + 1) * head_k)
            scores = dot(query_low[:, lanes], key_ref[span, lanes], ((1,), (1,)))
            scores = jnp.where(causal, scores, 0.0).astype(bf16)
            within = dot(scores, value_ref[span, lanes])
            earlier = dot(query_abs[:, lanes], start_ref[c, h], ((1,), (1,)))
            local_ref[span, lanes] = (within + earlier).astype(bf16)
    tail[...] = before
    unstage(stage, ypool_refs)


def output_kernel(msgs_ref, init_ref, local_ref, qtot_ref, gate_ref, *rest):
    y_refs, (carried, stage) = rest[:-2], rest[-2:]
    tile = local_ref.shape[0]
    head_k = init_ref.shape[-1]
    heads = init_ref.shape[0]

    @pl.when(pl.program_id(0) == 0)
    def _():
        for h in range(heads):
            def step(i, state):
                decay = (
                    msgs_ref[i, h, head_k : head_k + 1, :].astype(f32)
                    + msgs_ref[i, h, head_k + 1 : head_k + 2, :].astype(f32)
                )
                return state * decay + msgs_ref[i, h, :head_k, :].astype(f32)

            carried[h] = lax.fori_loop(0, lax.axis_index("sp"), step, init_ref[h].T).astype(bf16)

    pieces = []
    for h in range(heads):
        lanes = slice(h * head_k, (h + 1) * head_k)
        recur = local_ref[:, lanes].astype(f32) + dot(qtot_ref[:, lanes], carried[h], ((1,), (1,)))
        mean = jnp.mean(recur * recur, axis=-1, keepdims=True)
        scaled = recur * lax.rsqrt(mean + norm_eps)
        pieces.append((scaled * gate_ref[:, lanes].astype(f32)).astype(bf16))
    y_recur = jnp.concatenate(pieces, axis=1)
    for c in range(tile // chunk):
        rows = slice(c * chunk, (c + 1) * chunk)
        stage_rows(stage, pl.program_id(0) * tile + c * chunk, y_recur[rows])
    unstage(stage, y_refs)


def project_kernel(count, *refs):
    seen, weights, base, out_ref = refs[:count], refs[count : 2 * count], refs[2 * count : -1], refs[-1]
    total = base[0][...] if base else None
    for piece, weight in zip(seen, weights):
        term = dot(piece[...], weight[...])
        total = term if total is None else total + term
    out_ref[...] = total.astype(out_ref.dtype)


def fixed(*shape):
    return pl.BlockSpec(shape, lambda *_: (0,) * len(shape))


def moving(*shape):
    return pl.BlockSpec(shape, lambda i, *_: (i,) + (0,) * (len(shape) - 1))


limits = pltpu.CompilerParams(
    dimension_semantics=("arbitrary",), vmem_limit_bytes=56 * 1024 * 1024
)


def swapped(array, axis, bit):
    devices = lax.axis_size(axis)
    return lax.ppermute(array, axis, [(i, i ^ bit) for i in range(devices)])


def columns(size, block):
    return pl.BlockSpec((size, block), lambda i: (0, i))


def project(seen, weights, base, out_type):
    rows, channels = seen[0].shape
    width = weights[0].shape[1]
    block = min(width, 512)
    extra = [] if base is None else [base]
    return pl.pallas_call(
        functools.partial(project_kernel, len(seen)),
        grid=(width // block,),
        in_specs=[fixed(rows, channels)] * len(seen)
        + [columns(channels, block)] * len(weights)
        + [columns(rows, block)] * len(extra),
        out_specs=columns(rows, block),
        out_shape=jax.ShapeDtypeStruct((rows, width), out_type),
        compiler_params=limits,
        cost_estimate=pl.CostEstimate(
            flops=2 * len(seen) * rows * channels * width, transcendentals=0,
            bytes_accessed=2 * (len(weights) * channels * width + rows * width),
        ),
        name="project_kernel",
    )(*seen, *weights, *extra)


def per_device(
    inputs, norm_gain, pool_weight, query_weight, forget_weight, value_weight, outgate_weight,
    pool_mix, pool_scale, lower_bound, extra_decay, recur_gain, init_state, out_pool, out_recur,
):
    rows, width = inputs.shape
    heads, head_k = init_state.shape[:2]
    channels = query_weight.shape[1]
    sp, tp = lax.axis_size("sp"), lax.axis_size("tp")
    quarter, tile = rows // tp, 4 * chunk
    steps, chunks = rows // tile, tile // chunk
    lanes = 128
    gain = norm_gain.reshape(width // lanes, lanes)
    sds = jax.ShapeDtypeStruct

    def offsets_of(weight):
        far = swapped(weight, "tp", 2)
        near = swapped(weight, "tp", 1)
        return [weight, near, far, swapped(far, "tp", 1)]

    assert tp == 4
    w_pool = offsets_of(out_pool)
    w_recur = offsets_of(out_recur)

    scale, key_dec, decay, value, starts, row_info, msgs = pl.pallas_call(
        state_kernel,
        grid=(steps,),
        in_specs=[
            moving(tile, width), fixed(*gain.shape), fixed(width, channels),
            fixed(width, channels), fixed(1, channels),
            pl.BlockSpec((heads, tile), lambda i: (0, i)),
        ],
        out_specs=[
            moving(tile, lanes), moving(tile, channels), moving(tile, channels),
            moving(tile, channels), moving(chunks, heads, head_k, head_k),
            moving(chunks, 8, channels), fixed(sp, heads, head_k + msg_pad, head_k),
        ],
        out_shape=[
            sds((rows, lanes), f32), sds((rows, channels), bf16), sds((rows, channels), bf16),
            sds((rows, channels), bf16), sds((rows // chunk, heads, head_k, head_k), bf16),
            sds((rows // chunk, 8, channels), f32),
            sds((sp, heads, head_k + msg_pad, head_k), bf16),
        ],
        scratch_shapes=[
            pltpu.VMEM((width, 2 * channels), bf16), pltpu.VMEM((heads, head_k, head_k), f32),
            pltpu.VMEM((1, channels), f32),
        ],
        compiler_params=limits,
        cost_estimate=pl.CostEstimate(
            flops=4 * rows * width * channels, transcendentals=0, bytes_accessed=2 * rows * width
        ),
        name="state_kernel",
    )(inputs, gain, forget_weight, value_weight, lower_bound[None], extra_decay.T)

    halo = lax.ppermute(
        inputs[rows - halo_rows :], "sp", [(i, i + 1) for i in range(sp - 1)])
    msgs = lax.all_to_all(msgs, "sp", split_axis=0, concat_axis=0, tiled=True)
    local, qtot, gate, *y_pool = pl.pallas_call(
        local_kernel,
        grid=(steps,),
        in_specs=[
            moving(tile, width), fixed(halo_rows, width), fixed(*gain.shape),
            fixed(width, channels), fixed(width, channels), fixed(width, channels),
            fixed(*pool_mix.shape), fixed(1, channels), fixed(1, channels),
            moving(tile, lanes), moving(tile, channels), moving(tile, channels),
            moving(tile, channels), moving(chunks, heads, head_k, head_k),
            moving(chunks, 8, channels),
        ],
        out_specs=[moving(tile, channels)] * 3 + [fixed(quarter, channels)] * tp,
        out_shape=[sds((rows, channels), bf16)] * 3 + [sds((quarter, channels), bf16)] * tp,
        scratch_shapes=[
            pltpu.VMEM((width, 3 * channels), bf16),
            pltpu.VMEM((halo_rows, channels), bf16),
            pltpu.VMEM((chunk, chunk + halo_rows), bf16),
            pltpu.VMEM((tp, quarter, channels), bf16),
        ],
        compiler_params=limits,
        cost_estimate=pl.CostEstimate(
            flops=6 * rows * width * channels, transcendentals=0, bytes_accessed=2 * rows * width
        ),
        name="local_kernel",
    )(
        inputs, halo, gain, query_weight, outgate_weight, pool_weight, pool_mix,
        pool_scale[None], recur_gain[None], scale, key_dec, decay, value, starts, row_info,
    )

    def exchange(pieces):
        return [pieces[0]] + [swapped(pieces[k], "tp", k) for k in range(1, tp)]

    pool_seen = exchange(y_pool)
    out_tile = rows // 2
    y_recur = pl.pallas_call(
        output_kernel,
        grid=(rows // out_tile,),
        in_specs=[
            fixed(*msgs.shape), fixed(*init_state.shape), moving(out_tile, channels),
            moving(out_tile, channels), moving(out_tile, channels),
        ],
        out_specs=[fixed(quarter, channels)] * tp,
        out_shape=[sds((quarter, channels), bf16)] * tp,
        scratch_shapes=[
            pltpu.VMEM((heads, head_k, head_k), bf16), pltpu.VMEM((tp, quarter, channels), bf16),
        ],
        compiler_params=limits,
        cost_estimate=pl.CostEstimate(
            flops=4 * rows * head_k * channels, transcendentals=0,
            bytes_accessed=8 * rows * channels,
        ),
        name="output_kernel",
    )(msgs, init_state, local, qtot, gate)
    recur_seen = exchange(y_recur)
    partial_sum = project(pool_seen, w_pool, None, f32)
    return project(recur_seen, w_recur, partial_sum, bf16)


def solution(mesh):
    in_specs = (
        P("sp", None), P(), P(None, "tp"), P(None, "tp"), P(None, "tp"), P(None, "tp"),
        P(None, "tp"), P("tp", None, None), P("tp"), P("tp"), P("sp", "tp"), P("tp"),
        P("tp", None, None), P("tp", None), P("tp", None),
    )

    return jax.shard_map(
        per_device, mesh=mesh, in_specs=in_specs, out_specs=P(("sp", "tp"), None), check_vma=False
    )
```

time: 105 us -> 102 us (0.971)
  matrix products: 18.2 us -> 0 us
  waiting for transfers between devices: 18.3 us -> 36.4 us
  Pallas kernels: 37.3 us -> 45.4 us
  starting transfers between devices: 19.7 us -> 15.7 us
  other arithmetic: 3.98 us -> 0 us
  local copies, waits for them, and re-layouts: 6.3 us -> 2.99 us
    ppermute x4 -> x12, waiting for transfers between devices: 0.01 us -> 36.4 us  [swapped(): return lax.ppermute(array, axis, [(i, i ^ bit) for i in range(devices)])]
    dot_general x8 -> x0, matrix products: 18.2 us -> none  [project(): term = jnp.dot(piece, weights[k], preferred_element_type=f32)]
    pallas_call x2 -> x4, Pallas kernels: 23.8 us -> 33.5 us  [the longest x1 17.7 us: per_device(): pl.pallas_call(local_kernel, grid=(steps,), in_specs=[moving(tile, width)...]
    all_to_all x3 -> x1, waiting for transfers between devices: 9.53 us -> 0.01 us  [per_device(): msgs = lax.all_to_all(msgs, 'sp', split_axis=0, concat_axis=0, tiled=True)]
    ppermute x1, waiting for transfers between devices: 8.8 us -> 0.01 us  [per_device(): lax.ppermute(inputs[rows - halo_rows:], 'sp', [(i, i + 1) for i in range(...]
    all_to_all x3 -> x1, starting transfers between devices: 13.9 us -> 5.22 us  [per_device(): msgs = lax.all_to_all(msgs, 'sp', split_axis=0, concat_axis=0, tiled=True)]
    ppermute x4 -> x12, starting transfers between devices: 2.49 us -> 7.04 us  [swapped(): return lax.ppermute(array, axis, [(i, i ^ bit) for i in range(devices)])]
    concatenate x2 -> x0, other arithmetic: 3.37 us -> none  [whole(): jnp.concatenate([stacked, swapped(stacked, 'tp', tp // 2 // bit)], axis=0)]
  transfers between devices with their start and end apart: 8 -> 14, of which waited for: 3 -> 7; matrix products, arithmetic and copies ran while one was open for 18% -> 1% of each run, Pallas kernels for 36% -> 39%
where the time goes in v1:
time: 102 us; the launch traced here: 101 us
  Pallas kernels  45.4 us (45%)
  waiting for transfers between devices  36.4 us (36%)
  starting transfers between devices  15.7 us (15%)
  local copies, waits for them, and re-layouts  2.99 us (3%)
    ppermute x12, waiting for transfers between devices, swapped(): return lax.ppermute(array, axis, [(i, i ^ bit) for i in range(devices)])  36.4 us
    pallas_call x1, Pallas kernels, per_device(): pl.pallas_call(local_kernel, grid=(steps,), in_specs=[moving(tile, width)...  17.7 us
    pallas_call x2, Pallas kernels, project(): pl.pallas_call(functools.partial(project_kernel, len(seen)), grid=(width...  11.9 us
    pallas_call x1, Pallas kernels, per_device(): pl.pallas_call(state_kernel, grid=(steps,), in_specs=[moving(tile, width)...  11.9 us
    ppermute x12, starting transfers between devices, swapped(): return lax.ppermute(array, axis, [(i, i ^ bit) for i in range(devices)])  7.04 us
    all_to_all x1, starting transfers between devices, per_device(): msgs = lax.all_to_all(msgs, 'sp', split_axis=0, concat_axis=0, tiled=True)  5.22 us
    pallas_call x1, Pallas kernels, per_device(): pl.pallas_call(output_kernel, grid=(rows // out_tile,), in_specs=[fixed(*...  3.79 us
    ppermute x1, starting transfers between devices, per_device(): lax.ppermute(inputs[rows - halo_rows:], 'sp', [(i, i + 1) for i in range(...  3.42 us
  transfers between devices with their start and end apart: 14, of which 7 were waited for; matrix products, arithmetic and copies ran while one was open for 1% of the time, Pallas kernels for 39%

profile of v1, /device:TPU:16, one launch (start us, length us, event | category | flops | bytes accessed | tf_op | source)
XLA Modules:
  0.0 100.6 jit_solution(8314852767270954544)
XLA Ops:
  0.0 1.5 %collective-permute-start.11 = (bf16[256,2048]{1,0:T(8,128)(2,1)}, bf16[256,2048]{1,0:T(8,128)(2,1)}, u32[]{:S(2)}, u32[]{:S(2)}) collective-permute-start(bf16[256,2048]{1,0:T(8,128)(2,1)} %refs_4_.2), channel_id=1, source_target_pairs={{0,2},{1,3},{2,0},{3,1},{4,6},{5,7},{6,4},{7,5},{8,10},{9,11},{10,... | collective-permute-start | bytes 3145736 | tf_op jit(solution)/shard_map/ppermute | solution.py:266
  1.5 0.5 collective-permute-start.5
  2.0 0.8 slice.3
  2.9 3.4 %collective-permute-start = (bf16[16,2048]{1,0:T(8,128)(2,1)S(1)}, bf16[16,2048]{1,0:T(8,128)(2,1)S(1)}, u32[]{:S(2)}, u32[]{:S(2)}) collective-permute-start(bf16[16,2048]{1,0:T(8,128)(2,1)S(1)} %slice.3), channel_id=1, source_target_pairs={{0,4},{4,8},{8,12},{12,16},{16,20},{20,24},{24,28},{1,5},{5,9},{9,... | collective-permute-start | bytes 196616 | tf_op jit(solution)/shard_map/ppermute | solution.py:348
  6.3 11.9 %state_kernel.1 = (f32[1536,128]{1,0:T(8,128)}, bf16[1536,256]{1,0:T(8,128)(2,1)}, bf16[1536,256]{1,0:T(8,128)(2,1)}, bf16[1536,256]{1,0:T(8,128)(2,1)}, bf16[12...) custom-call(bf16[1536,2048]{1,0:T(8,128)(2,1)} %x_ref.3, f32[16,128]{1,0:T(8,128)} %bitcast.6, ...), custom_call_target="tpu_custom_call" | custom-call | flops 3221225472 | bytes 6291456 | tf_op jit(solution)/shard_map/state_kernel/pallas_call | solution.py:318
  18.2 5.2 %all-to-all-start = ((bf16[8,2,144,128]{3,2,1,0:T(8,128)(2,1)}), bf16[8,2,144,128]{3,2,1,0:T(8,128)(2,1)S(1)}, u32[]{:S(2)}, u32[]{:S(2)}) async-start(bf16[8,2,144,128]{3,2,1,0:T(8,128)(2,1)} %get-tuple-element.23), calls=%async_computation | async-start | bytes 1179648 | tf_op jit(solution)/shard_map/all_to_all | solution.py:350
  23.5 2.9 %collective-permute-done.11.refs_6_ = bf16[256,2048]{1,0:T(8,128)(2,1)} collective-permute-done((bf16[256,2048]{1,0:T(8,128)(2,1)}, bf16[256,2048]{1,0:T(8,128)(2,1)}, u32[]{:S(2)}, u32[]{:S(2)}) %collective-permute-start.11) | collective-permute-done | bytes 1048608 | tf_op jit(solution)/shard_map/ppermute | solution.py:266
  26.9 20.7 %collective-permute-done.5.refs_6_ = bf16[256,2048]{1,0:T(8,128)(2,1)S(1)} collective-permute-done((bf16[256,2048]{1,0:T(8,128)(2,1)}, bf16[256,2048]{1,0:T(8,128)(2,1)S(1)}, u32[]{:S(2)}, u32[]{:S(2)}) %collective-permute-start.5) | collective-permute-done | bytes 1048608 | tf_op jit(solution)/shard_map/ppermute | solution.py:266
  47.6 0.7 copy-done.9
  48.3 17.7 %local_kernel.1 = (bf16[1536,256]{1,0:T(8,128)(2,1)}, bf16[1536,256]{1,0:T(8,128)(2,1)}, bf16[1536,256]{1,0:T(8,128)(2,1)}, bf16[384,256]{1,0:T(8,128)(2,1)}, bf...) custom-call(bf16[1536,2048]{1,0:T(8,128)(2,1)} %x_ref.3, bf16[16,2048]{1,0:T(8,128)(2,1)} %copy-done.9, ...), custom_call_target="tpu_custom_call" | custom-call | flops 4831838208 | bytes 6291456 | tf_op jit(solution)/shard_map/local_kernel/pallas_call | solution.py:351
  66.0 0.5 collective-permute-start.7
  66.5 1.3 %collective-permute-done.7.refs_1_ = bf16[384,256]{1,0:T(8,128)(2,1)S(1)} collective-permute-done((bf16[384,256]{1,0:T(8,128)(2,1)}, bf16[384,256]{1,0:T(8,128)(2,1)S(1)}, u32[]{:S(2)}, u32[]{:S(2)}) %collective-permute-start.7) | collective-permute-done | bytes 196640 | tf_op jit(solution)/shard_map/ppermute | solution.py:266
  67.8 1.5 %collective-permute-start.8 = (bf16[384,256]{1,0:T(8,128)(2,1)}, bf16[384,256]{1,0:T(8,128)(2,1)S(1)}, u32[]{:S(2)}, u32[]{:S(2)}) collective-permute-start(bf16[384,256]{1,0:T(8,128)(2,1)} %get-tuple-element.39), channel_id=1, source_target_pairs={{0,2},{1,3},{2,0},{3,1},{4,6},{5,7},{6,4},{7,5},{8,10},{9,11},{10,... | collective-permute-start | bytes 589832 | tf_op jit(solution)/shard_map/ppermute | solution.py:266
  69.3 5.9 %collective-permute-done.8.refs_2_ = bf16[384,256]{1,0:T(8,128)(2,1)S(1)} collective-permute-done((bf16[384,256]{1,0:T(8,128)(2,1)}, bf16[384,256]{1,0:T(8,128)(2,1)S(1)}, u32[]{:S(2)}, u32[]{:S(2)}) %collective-permute-start.8) | collective-permute-done | bytes 196640 | tf_op jit(solution)/shard_map/ppermute | solution.py:266
  75.2 0.6 collective-permute-start.9
  75.8 0.8 copy-done
  76.6 3.8 %output_kernel.1 = (bf16[384,256]{1,0:T(8,128)(2,1)}, bf16[384,256]{1,0:T(8,128)(2,1)}, bf16[384,256]{1,0:T(8,128)(2,1)}, bf16[384,256]{1,0:T(8,128)(2,1)}) custom-call(bf16[8,2,144,128]{3,2,1,0:T(8,128)(2,1)} %copy-done, f32[2,128,128]{2,1,0:T(8,128)} %init_ref.1, bf16[1536,256]{1,0:T(8,128)(2,1)} %get-tuple-element.30.local_ref, ...), custom_call_target="tpu_custom_call" | custom-call | flops 201326592 | bytes 3145728 | tf_op jit(solution)/shard_map/output_kernel/pallas_call | solution.py:385
  80.4 2.1 %collective-permute-done.9.refs_3_ = bf16[384,256]{1,0:T(8,128)(2,1)S(1)} collective-permute-done((bf16[384,256]{1,0:T(8,128)(2,1)}, bf16[384,256]{1,0:T(8,128)(2,1)S(1)}, u32[]{:S(2)}, u32[]{:S(2)}) %collective-permute-start.9) | collective-permute-done | bytes 196640 | tf_op jit(solution)/shard_map/ppermute | solution.py:266
  82.7 1.2 %collective-permute-start.2 = (bf16[384,256]{1,0:T(8,128)(2,1)}, bf16[384,256]{1,0:T(8,128)(2,1)S(1)}, u32[]{:S(2)}, u32[]{:S(2)}) collective-permute-start(bf16[384,256]{1,0:T(8,128)(2,1)} %get-tuple-element.35), channel_id=1, source_target_pairs={{0,2},{1,3},{2,0},{3,1},{4,6},{5,7},{6,4},{7,5},{8,10},{9,11},{10,... | collective-permute-start | bytes 589832 | tf_op jit(solution)/shard_map/ppermute | solution.py:266
  83.9 0.5 collective-permute-start.3
  84.4 5.8 %project_kernel.2.refs_8_ = f32[384,2048]{1,0:T(8,128)} custom-call(bf16[384,256]{1,0:T(8,128)(2,1)} %get-tuple-element.37.refs_0_, bf16[384,256]{1,0:T(8,128)(2,1)} %copy-done.3, bf16[384,256]{1,0:T(8,128)(2,1)} %copy-done.4, bf16[384,256]{1,0:T(8,128)(2,1)} %copy-done.6, bf16[256,2048]{1,0:T(8,128)(2,1)} %refs_4_.2, ...), custom_call_target="tpu_custom_call" | custom-call | flops 1610612736 | bytes 5767168 | tf_op jit(solution)/shard_map/project_kernel/pallas_call | solution.py:278
  90.7 3.1 %collective-permute-done.3.refs_3_ = bf16[384,256]{1,0:T(8,128)(2,1)S(1)} collective-permute-done((bf16[384,256]{1,0:T(8,128)(2,1)}, bf16[384,256]{1,0:T(8,128)(2,1)S(1)}, u32[]{:S(2)}, u32[]{:S(2)}) %collective-permute-start.3) | collective-permute-done | bytes 196640 | tf_op jit(solution)/shard_map/ppermute | solution.py:266
  93.7 0.7 copy-done.8
  94.4 6.2 %project_kernel.3 = bf16[384,2048]{1,0:T(8,128)(2,1)} custom-call(bf16[384,256]{1,0:T(8,128)(2,1)} %get-tuple-element.33.refs_0_, bf16[384,256]{1,0:T(8,128)(2,1)} %copy-done.5, bf16[384,256]{1,0:T(8,128)(2,1)} %copy-done.7, bf16[384,256]{1,0:T(8,128)(2,1)} %copy-done.8, bf16[256,2048]{1,0:T(8,128)(2,1)} %refs_4_.3, ...), custom_call_target="tpu_custom_call" | custom-call | flops 1610612736 | bytes 5767168 | tf_op jit(solution)/shard_map/project_kernel/pallas_call | solution.py:278
  (30 shorter events, 1.1 us)
Async XLA Ops:
  0.0 26.3 %collective-permute-start.11 = (bf16[256,2048]{1,0:T(8,128)(2,1)}, bf16[256,2048]{1,0:T(8,128)(2,1)}, u32[]{:S(2)}, u32[]{:S(2)}) collective-permute-start(bf16[256,2048]{1,0:T(8,128)(2,1)} %refs_4_.2), channel_id=1, source_target_pairs={{0,2},{1,3},{2,0},{3,1},{4,6},{5,7},{6,4},{7,5},{8,10},{9,11},{10,... | collective-permute-start | bytes 3145736 | tf_op jit(solution)/shard_map/ppermute | solution.py:266
  1.5 46.1 %collective-permute-start.5 = (bf16[256,2048]{1,0:T(8,128)(2,1)}, bf16[256,2048]{1,0:T(8,128)(2,1)S(1)}, u32[]{:S(2)}, u32[]{:S(2)}) collective-permute-start(bf16[256,2048]{1,0:T(8,128)(2,1)} %refs_4_.3), channel_id=1, source_target_pairs={{0,2},{1,3},{2,0},{3,1},{4,6},{5,7},{6,4},{7,5},{8,10},{9,11},{10,... | collective-permute-start | bytes 3145736 | tf_op jit(solution)/shard_map/ppermute | solution.py:266
  2.9 44.7 %collective-permute-start = (bf16[16,2048]{1,0:T(8,128)(2,1)S(1)}, bf16[16,2048]{1,0:T(8,128)(2,1)S(1)}, u32[]{:S(2)}, u32[]{:S(2)}) collective-permute-start(bf16[16,2048]{1,0:T(8,128)(2,1)S(1)} %slice.3), channel_id=1, source_target_pairs={{0,4},{4,8},{8,12},{12,16},{16,20},{20,24},{24,28},{1,5},{5,9},{9,... | collective-permute-start | bytes 196616 | tf_op jit(solution)/shard_map/ppermute | solution.py:348
  6.3 20.1 %copy-start.1 = (bf16[256,2048]{1,0:T(8,128)(2,1)S(1)}, bf16[256,2048]{1,0:T(8,128)(2,1)}, u32[]{:S(2)}) copy-start(bf16[256,2048]{1,0:T(8,128)(2,1)} %refs_4_.3) | copy-start | bytes 3145732
  18.2 57.6 %all-to-all-start = ((bf16[8,2,144,128]{3,2,1,0:T(8,128)(2,1)}), bf16[8,2,144,128]{3,2,1,0:T(8,128)(2,1)S(1)}, u32[]{:S(2)}, u32[]{:S(2)}) async-start(bf16[8,2,144,128]{3,2,1,0:T(8,128)(2,1)} %get-tuple-element.23), calls=%async_computation | async-start | bytes 1179648 | tf_op jit(solution)/shard_map/all_to_all | solution.py:350
  23.5 59.2 %collective-permute-start.10 = (bf16[256,2048]{1,0:T(8,128)(2,1)}, bf16[256,2048]{1,0:T(8,128)(2,1)}, u32[]{:S(2)}, u32[]{:S(2)}) collective-permute-start(bf16[256,2048]{1,0:T(8,128)(2,1)} %refs_4_.2), channel_id=1, source_target_pairs={{0,1},{1,0},{2,3},{3,2},{4,5},{5,4},{6,7},{7,6},{8,9},{9,8},{10,11... | collective-permute-start | bytes 3145736 | tf_op jit(solution)/shard_map/ppermute | solution.py:266
  26.3 57.5 %collective-permute-start.12 = (bf16[256,2048]{1,0:T(8,128)(2,1)}, bf16[256,2048]{1,0:T(8,128)(2,1)}, u32[]{:S(2)}, u32[]{:S(2)}) collective-permute-start(bf16[256,2048]{1,0:T(8,128)(2,1)} %collective-permute-done.11.refs_6_), channel_id=1, source_target_pairs={{0,1},{1,0},{2,3},{3,2},{4,5},{5,4},{6,7},{7,6},{8,9},{9,8},{10,11... | collective-permute-start | bytes 3145736 | tf_op jit(solution)/shard_map/ppermute | solution.py:266
  26.4 63.9 %collective-permute-start.4 = (bf16[256,2048]{1,0:T(8,128)(2,1)S(1)}, bf16[256,2048]{1,0:T(8,128)(2,1)}, u32[]{:S(2)}, u32[]{:S(2)}) collective-permute-start(bf16[256,2048]{1,0:T(8,128)(2,1)S(1)} %copy-done.1), channel_id=1, source_target_pairs={{0,1},{1,0},{2,3},{3,2},{4,5},{5,4},{6,7},{7,6},{8,9},{9,8},{10,11... | collective-permute-start | bytes 3145736 | tf_op jit(solution)/shard_map/ppermute | solution.py:266
  47.6 18.4 %copy-start.2 = (bf16[256,2048]{1,0:T(8,128)(2,1)}, bf16[256,2048]{1,0:T(8,128)(2,1)S(1)}, u32[]{:S(2)}) copy-start(bf16[256,2048]{1,0:T(8,128)(2,1)S(1)} %collective-permute-done.5.refs_6_) | copy-start | bytes 3145732
  47.6 46.1 %collective-permute-start.6 = (bf16[256,2048]{1,0:T(8,128)(2,1)S(1)}, bf16[256,2048]{1,0:T(8,128)(2,1)}, u32[]{:S(2)}, u32[]{:S(2)}) collective-permute-start(bf16[256,2048]{1,0:T(8,128)(2,1)S(1)} %collective-permute-done.5.refs_6_), channel_id=1, source_target_pairs={{0,1},{1,0},{2,3},{3,2},{4,5},{5,4},{6,7},{7,6},{8,9},{9,8},{10,11... | collective-permute-start | bytes 3145736 | tf_op jit(solution)/shard_map/ppermute | solution.py:266
  47.6 0.7 copy-start.9
  66.0 1.8 %collective-permute-start.7 = (bf16[384,256]{1,0:T(8,128)(2,1)}, bf16[384,256]{1,0:T(8,128)(2,1)S(1)}, u32[]{:S(2)}, u32[]{:S(2)}) collective-permute-start(bf16[384,256]{1,0:T(8,128)(2,1)} %get-tuple-element.38), channel_id=1, source_target_pairs={{0,1},{1,0},{2,3},{3,2},{4,5},{5,4},{6,7},{7,6},{8,9},{9,8},{10,11... | collective-permute-start | bytes 589832 | tf_op jit(solution)/shard_map/ppermute | solution.py:266
  67.8 16.6 %copy-start.3 = (bf16[384,256]{1,0:T(8,128)(2,1)}, bf16[384,256]{1,0:T(8,128)(2,1)S(1)}, u32[]{:S(2)}) copy-start(bf16[384,256]{1,0:T(8,128)(2,1)S(1)} %collective-permute-done.7.refs_1_) | copy-start | bytes 589828
  67.8 7.4 %collective-permute-start.8 = (bf16[384,256]{1,0:T(8,128)(2,1)}, bf16[384,256]{1,0:T(8,128)(2,1)S(1)}, u32[]{:S(2)}, u32[]{:S(2)}) collective-permute-start(bf16[384,256]{1,0:T(8,128)(2,1)} %get-tuple-element.39), channel_id=1, source_target_pairs={{0,2},{1,3},{2,0},{3,1},{4,6},{5,7},{6,4},{7,5},{8,10},{9,11},{10,... | collective-permute-start | bytes 589832 | tf_op jit(solution)/shard_map/ppermute | solution.py:266
  75.2 9.2 %copy-start.4 = (bf16[384,256]{1,0:T(8,128)(2,1)}, bf16[384,256]{1,0:T(8,128)(2,1)S(1)}, u32[]{:S(2)}) copy-start(bf16[384,256]{1,0:T(8,128)(2,1)S(1)} %collective-permute-done.8.refs_2_) | copy-start | bytes 589828
  75.2 7.4 %collective-permute-start.9 = (bf16[384,256]{1,0:T(8,128)(2,1)}, bf16[384,256]{1,0:T(8,128)(2,1)S(1)}, u32[]{:S(2)}, u32[]{:S(2)}) collective-permute-start(bf16[384,256]{1,0:T(8,128)(2,1)} %get-tuple-element.40), channel_id=1, source_target_pairs={{0,3},{1,2},{2,1},{3,0},{4,7},{5,6},{6,5},{7,4},{8,11},{9,10},{10,... | collective-permute-start | bytes 589832 | tf_op jit(solution)/shard_map/ppermute | solution.py:266
  75.8 0.8 copy-start
  82.6 1.9 %copy-start.6 = (bf16[384,256]{1,0:T(8,128)(2,1)}, bf16[384,256]{1,0:T(8,128)(2,1)S(1)}, u32[]{:S(2)}) copy-start(bf16[384,256]{1,0:T(8,128)(2,1)S(1)} %collective-permute-done.9.refs_3_) | copy-start | bytes 589828
  82.6 7.7 %collective-permute-start.1 = (bf16[384,256]{1,0:T(8,128)(2,1)}, bf16[384,256]{1,0:T(8,128)(2,1)S(1)}, u32[]{:S(2)}, u32[]{:S(2)}) collective-permute-start(bf16[384,256]{1,0:T(8,128)(2,1)} %get-tuple-element.34), channel_id=1, source_target_pairs={{0,1},{1,0},{2,3},{3,2},{4,5},{5,4},{6,7},{7,6},{8,9},{9,8},{10,11... | collective-permute-start | bytes 589832 | tf_op jit(solution)/shard_map/ppermute | solution.py:266
  82.7 8.0 %collective-permute-start.2 = (bf16[384,256]{1,0:T(8,128)(2,1)}, bf16[384,256]{1,0:T(8,128)(2,1)S(1)}, u32[]{:S(2)}, u32[]{:S(2)}) collective-permute-start(bf16[384,256]{1,0:T(8,128)(2,1)} %get-tuple-element.35), channel_id=1, source_target_pairs={{0,2},{1,3},{2,0},{3,1},{4,6},{5,7},{6,4},{7,5},{8,10},{9,11},{10,... | collective-permute-start | bytes 589832 | tf_op jit(solution)/shard_map/ppermute | solution.py:266
  83.9 9.8 %collective-permute-start.3 = (bf16[384,256]{1,0:T(8,128)(2,1)}, bf16[384,256]{1,0:T(8,128)(2,1)S(1)}, u32[]{:S(2)}, u32[]{:S(2)}) collective-permute-start(bf16[384,256]{1,0:T(8,128)(2,1)} %get-tuple-element.36), channel_id=1, source_target_pairs={{0,3},{1,2},{2,1},{3,0},{4,7},{5,6},{6,5},{7,4},{8,11},{9,10},{10,... | collective-permute-start | bytes 589832 | tf_op jit(solution)/shard_map/ppermute | solution.py:266
  90.2 3.5 %copy-start.5 = (bf16[384,256]{1,0:T(8,128)(2,1)}, bf16[384,256]{1,0:T(8,128)(2,1)S(1)}, u32[]{:S(2)}) copy-start(bf16[384,256]{1,0:T(8,128)(2,1)S(1)} %collective-permute-done.1.refs_1_) | copy-start | bytes 589828
  90.7 3.1 %copy-start.7 = (bf16[384,256]{1,0:T(8,128)(2,1)}, bf16[384,256]{1,0:T(8,128)(2,1)S(1)}, u32[]{:S(2)}) copy-start(bf16[384,256]{1,0:T(8,128)(2,1)S(1)} %collective-permute-done.2.refs_2_) | copy-start | bytes 589828
  93.7 0.7 copy-start.8

commit v2 on v1

--- a/solution.py
+++ b/solution.py
@@ -83,46 +83,58 @@
         total[...] = jnp.zeros_like(total)
         fold_gain(gain_ref, (fw_ref, vw_ref), folded)
 
-    x = x_ref[...]
-    scale = jnp.broadcast_to(row_scale(x), scale_ref.shape)
-    scale_ref[...] = scale
-    raw = dot(x, folded[...])
-    scales = jnp.concatenate([scale] * (channels // scale.shape[1]), axis=1)
-    forget = raw[:, :channels] * scales
-    value = (raw[:, channels:] * scales).astype(bf16)
-    value_ref[...] = value
     gap = 1.0 - lb_ref[...]
-    key = gap / (1.0 + jnp.exp(forget))
-    extra_high, extra_low = split(extra_ref[...])
     pick = (
         lax.broadcasted_iota(jnp.int32, (heads, channels), 1) // head_k
         == lax.broadcasted_iota(jnp.int32, (heads, channels), 0)
     ).astype(f32).astype(bf16)
+    triangle = lower_triangle(chunk).astype(f32).astype(bf16)
+    triangle = jnp.concatenate([triangle, triangle], axis=1)
     first = ((0,), (0,))
-    log_f = jnp.log(1.0 - key) + (dot(extra_high, pick, first) + dot(extra_low, pick, first))
-    high, low = split(log_f)
-    triangle = lower_triangle(chunk).astype(f32).astype(bf16)
-    for c in range(tile // chunk):
-        span = slice(c * chunk, (c + 1) * chunk)
-        cum = dot(triangle, high[span]) + dot(triangle, low[span])
-        middle = cum[chunk // 2 - 1 : chunk // 2]
-        last = cum[chunk - 1 :]
-        decay_ref[span, :] = jnp.exp(cum - middle).astype(bf16)
-        key_dec = key[span] * jnp.exp(middle - cum)
-        key_ref[span, :] = key_dec.astype(bf16)
-        key_end = (key_dec * jnp.exp(last - middle)).astype(bf16)
-        before = total[...]
-        rows_ref[c] = jnp.concatenate(
-            [jnp.exp(middle), jnp.exp(before), jnp.zeros((6, middle.shape[1]), f32)], axis=0
-        )
-        total[...] = before + last
-        whole = jnp.exp(last)
-        for h in range(heads):
-            lanes = slice(h * head_k, (h + 1) * head_k)
-            old = state[h]
-            start_ref[c, h] = old.astype(bf16)
-            contrib = dot(value[span, lanes], key_end[:, lanes], ((0,), (0,)))
-            state[h] = old * whole[:, lanes] + contrib
+
+    def project_block(b):
+        return dot(x_ref[b * 256 : (b + 1) * 256, :], folded[...])
+
+    extra_high, extra_low = split(extra_ref[...])
+    extras = dot(extra_high, pick, first) + dot(extra_low, pick, first)
+    ahead = project_block(0)
+    scale_ref[...] = jnp.broadcast_to(row_scale(x_ref[...]), scale_ref.shape)
+    for b in range(tile // 256):
+        block = slice(b * 256, (b + 1) * 256)
+        raw = ahead
+        if (b + 1) * 256 < tile:
+            ahead = project_block(b + 1)
+        scale = scale_ref[block, :]
+        scales = jnp.concatenate([scale] * (channels // scale.shape[1]), axis=1)
+        forget = raw[:, :channels] * scales
+        value = (raw[:, channels:] * scales).astype(bf16)
+        value_ref[block, :] = value
+        key = gap / (1.0 + jnp.exp(forget))
+        extra = extras[block]
+        high, low = split(jnp.log(1.0 - key) + extra)
+        for j in range(256 // chunk):
+            c = b * (256 // chunk) + j
+            part = slice(j * chunk, (j + 1) * chunk)
+            span = slice(c * chunk, (c + 1) * chunk)
+            cum = dot(triangle, jnp.concatenate([high[part], low[part]], axis=0))
+            middle = cum[chunk // 2 - 1 : chunk // 2]
+            last = cum[chunk - 1 :]
+            decay_ref[span, :] = jnp.exp(cum - middle).astype(bf16)
+            key_dec = key[part] * jnp.exp(middle - cum)
+            key_ref[span, :] = key_dec.astype(bf16)
+            key_end = (key_dec * jnp.exp(last - middle)).astype(bf16)
+            before = total[...]
+            rows_ref[c] = jnp.concatenate(
+                [jnp.exp(middle), jnp.exp(before), jnp.zeros((6, middle.shape[1]), f32)], axis=0
+            )
+            total[...] = before + last
+            whole = jnp.exp(last)
+            for h in range(heads):
+                lanes = slice(h * head_k, (h + 1) * head_k)
+                old = state[h]
+                start_ref[c, h] = old.astype(bf16)
+                contrib = dot(value[part, lanes], key_end[:, lanes], first)
+                state[h] = old * whole[:, lanes] + contrib
 
     @pl.when(step == pl.num_programs(0) - 1)
     def _():
@@ -167,42 +179,53 @@
         back = row - col
         band[...] = ((back >= 0) & (back < window)).astype(f32).astype(bf16)
 
-    raw = dot(x_ref[...], folded[...])
-    scale = scale_ref[...]
-    scales = jnp.concatenate([scale] * (channels // scale.shape[1]), axis=1)
-    query = raw[:, :channels] * scales
-    outgate = raw[:, channels : 2 * channels] * scales
-    pool_in = (raw[:, 2 * channels :] * scales).astype(bf16)
-    gate_ref[...] = (outgate * sigmoid(outgate) * recur_gain_ref[...]).astype(bf16)
-    query = query * sigmoid(query)
     causal = lower_triangle(chunk)
     before = tail[...]
-    for c in range(tile // chunk):
-        span = slice(c * chunk, (c + 1) * chunk)
-        part = pool_in[span]
-        sums = dot(band[...], jnp.concatenate([before, part], axis=0))
-        before = part[chunk - halo_rows :]
-        position = (
-            first_pos + step * tile + c * chunk
-            + lax.broadcasted_iota(jnp.int32, (chunk, 1), 0)
-        )
-        count = jnp.minimum(position + 1, window).astype(f32)
-        pooled = (sums * (1.0 / count) - part.astype(f32)).astype(bf16)
-        y_pool = (dot(pooled, mix_ref[0]) * pool_scale_ref[...]).astype(bf16)
-        stage_rows(stage, step * tile + c * chunk, y_pool)
-
-        query_dec = query[span] * decay_ref[span, :].astype(f32)
-        query_low = query_dec.astype(bf16)
-        query_abs = query_dec * rows_ref[c, 0:1, :]
-        qtot_ref[span, :] = (query_abs * rows_ref[c, 1:2, :]).astype(bf16)
-        query_abs = query_abs.astype(bf16)
-        for h in range(heads):
-            lanes = slice(h * head_k, (h + 1) * head_k)
-            scores = dot(query_low[:, lanes], key_ref[span, lanes], ((1,), (1,)))
-            scores = jnp.where(causal, scores, 0.0).astype(bf16)
-            within = dot(scores, value_ref[span, lanes])
-            earlier = dot(query_abs[:, lanes], start_ref[c, h], ((1,), (1,)))
-            local_ref[span, lanes] = (within + earlier).astype(bf16)
+
+    def project_block(b):
+        return dot(x_ref[b * 256 : (b + 1) * 256, :], folded[...])
+
+    ahead = project_block(0)
+    for b in range(tile // 256):
+        block = slice(b * 256, (b + 1) * 256)
+        raw = ahead
+        if (b + 1) * 256 < tile:
+            ahead = project_block(b + 1)
+        scale = scale_ref[block, :]
+        scales = jnp.concatenate([scale] * (channels // scale.shape[1]), axis=1)
+        query = raw[:, :channels] * scales
+        outgate = raw[:, channels : 2 * channels] * scales
+        pool_in = (raw[:, 2 * channels :] * scales).astype(bf16)
+        gate_ref[block, :] = (outgate * sigmoid(outgate) * recur_gain_ref[...]).astype(bf16)
+        query = query * sigmoid(query)
+        for j in range(256 // chunk):
+            c = b * (256 // chunk) + j
+            part = slice(j * chunk, (j + 1) * chunk)
+            span = slice(c * chunk, (c + 1) * chunk)
+            pool_part = pool_in[part]
+            sums = dot(band[...], jnp.concatenate([before, pool_part], axis=0))
+            before = pool_part[chunk - halo_rows :]
+            position = (
+                first_pos + step * tile + c * chunk
+                + lax.broadcasted_iota(jnp.int32, (chunk, 1), 0)
+            )
+            count = jnp.minimum(position + 1, window).astype(f32)
+            pooled = (sums * (1.0 / count) - pool_part.astype(f32)).astype(bf16)
+            y_pool = (dot(pooled, mix_ref[0]) * pool_scale_ref[...]).astype(bf16)
+            stage_rows(stage, step * tile + c * chunk, y_pool)
+
+            query_dec = query[part] * decay_ref[span, :].astype(f32)
+            query_low = query_dec.astype(bf16)
+            query_abs = query_dec * rows_ref[c, 0:1, :]
+            qtot_ref[span, :] = (query_abs * rows_ref[c, 1:2, :]).astype(bf16)
+            query_abs = query_abs.astype(bf16)
+            for h in range(heads):
+                lanes = slice(h * head_k, (h + 1) * head_k)
+                scores = dot(query_low[:, lanes], key_ref[span, lanes], ((1,), (1,)))
+                scores = jnp.where(causal, scores, 0.0).astype(bf16)
+                within = dot(scores, value_ref[span, lanes])
+                earlier = dot(query_abs[:, lanes], start_ref[c, h], ((1,), (1,)))
+                local_ref[span, lanes] = (within + earlier).astype(bf16)
     tail[...] = before
     unstage(stage, ypool_refs)
 
@@ -239,11 +262,19 @@
     unstage(stage, y_refs)
 
 
-def project_kernel(count, *refs):
-    seen, weights, base, out_ref = refs[:count], refs[count : 2 * count], refs[2 * count : -1], refs[-1]
-    total = base[0][...] if base else None
-    for piece, weight in zip(seen, weights):
-        term = dot(piece[...], weight[...])
+def project_kernel(counts, *refs):
+    refs = list(refs)
+    seen = [refs.pop(0) for _ in counts]
+    groups = [[refs.pop(0) for _ in range(count)] for count in counts]
+    out_ref = refs.pop()
+    total = refs.pop()[...].astype(f32) if refs else None
+    second = pl.program_id(0) >= pl.num_programs(0) // 2
+    for piece, group in zip(seen, groups):
+        weight = group[0][...]
+        if len(group) > 1:
+            mine = (lax.axis_index("sp") % 2 == 1) == second
+            weight = jnp.where(mine, weight, group[1][...])
+        term = dot(piece[...], weight)
         total = term if total is None else total + term
     out_ref[...] = total.astype(out_ref.dtype)
 
@@ -256,9 +287,10 @@
     return pl.BlockSpec(shape, lambda i, *_: (i,) + (0,) * (len(shape) - 1))
 
 
-limits = pltpu.CompilerParams(
-    dimension_semantics=("arbitrary",), vmem_limit_bytes=56 * 1024 * 1024
-)
+def limits(mib):
+    return pltpu.CompilerParams(
+        dimension_semantics=("arbitrary",), vmem_limit_bytes=mib * 1024 * 1024
+    )
 
 
 def swapped(array, axis, bit):
@@ -270,26 +302,44 @@
     return pl.BlockSpec((size, block), lambda i: (0, i))
 
 
+def half_columns(size, width, block, mine):
+    count = width // block // 2
+
+    def index(i):
+        parity = lax.axis_index("sp") % 2
+        half = parity if mine else 1 - parity
+        return 0, jnp.clip(i - count * half, 0, count - 1)
+
+    return pl.BlockSpec((size, block), index)
+
+
 def project(seen, weights, base, out_type):
     rows, channels = seen[0].shape
-    width = weights[0].shape[1]
-    block = min(width, 512)
+    width = weights[0][0].shape[1] * len(weights[0])
+    block = width // 4
     extra = [] if base is None else [base]
+    flat = [array for group in weights for array in group]
+    counts = tuple(len(group) for group in weights)
+    specs = []
+    for count in counts:
+        if count == 1:
+            specs.append(columns(channels, block))
+        else:
+            specs += [half_columns(channels, width, block, mine) for mine in (True, False)]
     return pl.pallas_call(
-        functools.partial(project_kernel, len(seen)),
+        functools.partial(project_kernel, counts),
         grid=(width // block,),
-        in_specs=[fixed(rows, channels)] * len(seen)
-        + [columns(channels, block)] * len(weights)
+        in_specs=[fixed(rows, channels)] * len(seen) + specs
         + [columns(rows, block)] * len(extra),
         out_specs=columns(rows, block),
         out_shape=jax.ShapeDtypeStruct((rows, width), out_type),
-        compiler_params=limits,
+        compiler_params=limits(32),
         cost_estimate=pl.CostEstimate(
             flops=2 * len(seen) * rows * channels * width, transcendentals=0,
             bytes_accessed=2 * (len(weights) * channels * width + rows * width),
         ),
         name="project_kernel",
-    )(*seen, *weights, *extra)
+    )(*seen, *flat, *extra)
 
 
 def per_device(
@@ -306,14 +356,24 @@
     gain = norm_gain.reshape(width // lanes, lanes)
     sds = jax.ShapeDtypeStruct
 
-    def offsets_of(weight):
-        far = swapped(weight, "tp", 2)
-        near = swapped(weight, "tp", 1)
-        return [weight, near, far, swapped(far, "tp", 1)]
-
-    assert tp == 4
-    w_pool = offsets_of(out_pool)
-    w_recur = offsets_of(out_recur)
+    assert tp == 4 and sp % 2 == 0
+    far = swapped(out_pool, "tp", 2)
+    half_width = width // 2
+    half = lax.dynamic_slice_in_dim(
+        out_recur, (lax.axis_index("sp") % 2) * half_width, half_width, axis=1
+    )
+    fetched = swapped(half, "tp", 2)
+    handed = swapped(fetched, "sp", 1)
+    cross_fetched = swapped(fetched, "tp", 1)
+    cross_handed = swapped(handed, "tp", 1)
+    w_pool = [
+        [out_pool], [swapped(out_pool, "tp", 1)], [far],
+        [swapped(far, "tp", 1)],
+    ]
+    w_recur = [
+        [out_recur], [swapped(out_recur, "tp", 1)], [fetched, handed],
+        [cross_fetched, cross_handed],
+    ]
 
     scale, key_dec, decay, value, starts, row_info, msgs = pl.pallas_call(
         state_kernel,
@@ -338,7 +398,7 @@
             pltpu.VMEM((width, 2 * channels), bf16), pltpu.VMEM((heads, head_k, head_k), f32),
             pltpu.VMEM((1, channels), f32),
         ],
-        compiler_params=limits,
+        compiler_params=limits(60),
         cost_estimate=pl.CostEstimate(
             flops=4 * rows * width * channels, transcendentals=0, bytes_accessed=2 * rows * width
         ),
@@ -367,7 +427,7 @@
             pltpu.VMEM((chunk, chunk + halo_rows), bf16),
             pltpu.VMEM((tp, quarter, channels), bf16),
         ],
-        compiler_params=limits,
+        compiler_params=limits(54),
         cost_estimate=pl.CostEstimate(
             flops=6 * rows * width * channels, transcendentals=0, bytes_accessed=2 * rows * width
         ),
@@ -394,7 +454,7 @@
         scratch_shapes=[
             pltpu.VMEM((heads, head_k, head_k), bf16), pltpu.VMEM((tp, quarter, channels), bf16),
         ],
-        compiler_params=limits,
+        compiler_params=limits(40),
         cost_estimate=pl.CostEstimate(
             flops=4 * rows * head_k * channels, transcendentals=0,
             bytes_accessed=8 * rows * channels,
@@ -402,8 +462,8 @@
         name="output_kernel",
     )(msgs, init_state, local, qtot, gate)
     recur_seen = exchange(y_recur)
-    partial_sum = project(pool_seen, w_pool, None, f32)
-    return project(recur_seen, w_recur, partial_sum, bf16)
+    partial_sum = project(pool_seen + recur_seen[:2], w_pool + w_recur[:2], None, bf16)
+    return project(recur_seen[2:], w_recur[2:], partial_sum, bf16)
 
 
 def solution(mesh):

time: 102 us -> 80.9 us (0.79)
  waiting for transfers between devices: 36.4 us -> 18.5 us
  Pallas kernels: 45.4 us -> 35.2 us
  local copies, waits for them, and re-layouts: 2.99 us -> 8.11 us
  starting transfers between devices: 15.7 us -> 17.6 us
    ppermute x12 -> x14, waiting for transfers between devices: 36.4 us -> 18.5 us  [swapped(): return lax.ppermute(array, axis, [(i, i ^ bit) for i in range(devices)])]
    pallas_call x1, Pallas kernels: 17.7 us -> 13.8 us  [per_device(): pl.pallas_call(local_kernel, grid=(steps,), in_specs=[moving(tile, width)...]
    unnamed x20 -> x24, local copies, waits for them, and re-layouts: 2.15 us -> 5.41 us
    pallas_call x2, Pallas kernels: 11.9 us -> 9.42 us  [project(): pl.pallas_call(functools.partial(project_kernel, counts), grid=(width //...]
    pallas_call x1, Pallas kernels: 3.79 us -> 1.33 us  [per_device(): pl.pallas_call(output_kernel, grid=(rows // out_tile,), in_specs=[fixed(*...]
    ppermute x12 -> x14, starting transfers between devices: 7.04 us -> 8.95 us  [swapped(): return lax.ppermute(array, axis, [(i, i ^ bit) for i in range(devices)])]
    dynamic_slice x0 -> x1, local copies, waits for them, and re-layouts: none -> 1.86 us  [per_device(): lax.dynamic_slice_in_dim(out_recur, lax.axis_index('sp') % 2 * half_width...]
    pallas_call x1, Pallas kernels: 11.9 us -> 10.6 us  [per_device(): pl.pallas_call(state_kernel, grid=(steps,), in_specs=[moving(tile, width)...]
  transfers between devices with their start and end apart: 14 -> 16, of which waited for: 7 -> 6; matrix products, arithmetic and copies ran while one was open for 1% -> 3% of each run, Pallas kernels for 39% -> 39%
where the time goes in v2:
time: 80.9 us; the launch traced here: 79.6 us
  Pallas kernels  35.2 us (44%)
  waiting for transfers between devices  18.5 us (23%)
  starting transfers between devices  17.6 us (22%)
  local copies, waits for them, and re-layouts  8.11 us (10%)
    ppermute x14, waiting for transfers between devices, swapped(): return lax.ppermute(array, axis, [(i, i ^ bit) for i in range(devices)])  18.5 us
    pallas_call x1, Pallas kernels, per_device(): pl.pallas_call(local_kernel, grid=(steps,), in_specs=[moving(tile, width)...  13.8 us
    pallas_call x1, Pallas kernels, per_device(): pl.pallas_call(state_kernel, grid=(steps,), in_specs=[moving(tile, width)...  10.6 us
    pallas_call x2, Pallas kernels, project(): pl.pallas_call(functools.partial(project_kernel, counts), grid=(width //...  9.42 us
    ppermute x14, starting transfers between devices, swapped(): return lax.ppermute(array, axis, [(i, i ^ bit) for i in range(devices)])  8.95 us
    unnamed x24, local copies, waits for them, and re-layouts  5.41 us
    all_to_all x1, starting transfers between devices, per_device(): msgs = lax.all_to_all(msgs, 'sp', split_axis=0, concat_axis=0, tiled=True)  5.22 us
    ppermute x1, starting transfers between devices, per_device(): lax.ppermute(inputs[rows - halo_rows:], 'sp', [(i, i + 1) for i in range(...  3.42 us
  transfers between devices with their start and end apart: 16, of which 6 were waited for; matrix products, arithmetic and copies ran while one was open for 3% of the time, Pallas kernels for 39%

profile of v2, /device:TPU:16, one launch (start us, length us, event | category | flops | bytes accessed | tf_op | source)
XLA Modules:
  0.0 79.6 jit_solution(7233034008990738959)
XLA Ops:
  0.0 1.5 %collective-permute-start.12 = (bf16[256,2048]{1,0:T(8,128)(2,1)}, bf16[256,2048]{1,0:T(8,128)(2,1)}, u32[]{:S(2)}, u32[]{:S(2)}) collective-permute-start(bf16[256,2048]{1,0:T(8,128)(2,1)} %refs_6_.1), channel_id=1, source_target_pairs={{0,2},{1,3},{2,0},{3,1},{4,6},{5,7},{6,4},{7,5},{8,10},{9,11},{10,... | collective-permute-start | bytes 3145736 | tf_op jit(solution)/shard_map/ppermute | solution.py:298
  1.5 0.8 %slice.3 = bf16[16,2048]{1,0:T(8,128)(2,1)S(1)} slice(bf16[1536,2048]{1,0:T(8,128)(2,1)} %x_ref.3), slice={[1520:1536], [0:2048]} | slice | bytes 131072 | tf_op jit(solution)/shard_map/slice | solution.py:409
  2.3 3.4 %collective-permute-start = (bf16[16,2048]{1,0:T(8,128)(2,1)S(1)}, bf16[16,2048]{1,0:T(8,128)(2,1)S(1)}, u32[]{:S(2)}, u32[]{:S(2)}) collective-permute-start(bf16[16,2048]{1,0:T(8,128)(2,1)S(1)} %slice.3), channel_id=1, source_target_pairs={{0,4},{4,8},{8,12},{12,16},{16,20},{20,24},{24,28},{1,5},{5,9},{9,... | collective-permute-start | bytes 196616 | tf_op jit(solution)/shard_map/ppermute | solution.py:408
  6.1 1.9 %constant_dynamic-slice_fusion = bf16[256,1024]{1,0:T(8,128)(2,1)} fusion(bf16[256,2048]{1,0:T(8,128)(2,1)} %refs_10_.1, s32[]{:T(128)S(6)} %select_n.11), kind=kLoop, calls=%fused_computation | loop fusion | bytes 1048580 | tf_op jit(solution)/shard_map/dynamic_slice | solution.py:362
  8.5 10.6 %state_kernel.1 = (f32[1536,128]{1,0:T(8,128)}, bf16[1536,256]{1,0:T(8,128)(2,1)}, bf16[1536,256]{1,0:T(8,128)(2,1)}, bf16[1536,256]{1,0:T(8,128)(2,1)}, bf16[12...) custom-call(bf16[1536,2048]{1,0:T(8,128)(2,1)} %x_ref.3, f32[16,128]{1,0:T(8,128)} %bitcast.6, ...), custom_call_target="tpu_custom_call" | custom-call | flops 3221225472 | bytes 6291456 | tf_op jit(solution)/shard_map/state_kernel/pallas_call | solution.py:378
  19.1 5.2 %all-to-all-start = ((bf16[8,2,144,128]{3,2,1,0:T(8,128)(2,1)}), bf16[8,2,144,128]{3,2,1,0:T(8,128)(2,1)S(1)}, u32[]{:S(2)}, u32[]{:S(2)}) async-start(bf16[8,2,144,128]{3,2,1,0:T(8,128)(2,1)} %get-tuple-element.23), calls=%async_computation | async-start | bytes 1179648 | tf_op jit(solution)/shard_map/all_to_all | solution.py:410
  24.3 2.1 %collective-permute-done.12.refs_8_ = bf16[256,2048]{1,0:T(8,128)(2,1)} collective-permute-done((bf16[256,2048]{1,0:T(8,128)(2,1)}, bf16[256,2048]{1,0:T(8,128)(2,1)}, u32[]{:S(2)}, u32[]{:S(2)}) %collective-permute-start.12) | collective-permute-done | bytes 1048608 | tf_op jit(solution)/shard_map/ppermute | solution.py:298
  26.4 0.6 copy-done.11
  27.0 13.8 %local_kernel.1 = (bf16[1536,256]{1,0:T(8,128)(2,1)}, bf16[1536,256]{1,0:T(8,128)(2,1)}, bf16[1536,256]{1,0:T(8,128)(2,1)}, bf16[384,256]{1,0:T(8,128)(2,1)}, bf...) custom-call(bf16[1536,2048]{1,0:T(8,128)(2,1)} %x_ref.3, bf16[16,2048]{1,0:T(8,128)(2,1)} %copy-done.11, ...), custom_call_target="tpu_custom_call" | custom-call | flops 4831838208 | bytes 6291456 | tf_op jit(solution)/shard_map/local_kernel/pallas_call | solution.py:411
  41.4 1.5 %collective-permute-start.4 = (bf16[256,1024]{1,0:T(8,128)(2,1)S(1)}, bf16[256,1024]{1,0:T(8,128)(2,1)}, u32[]{:S(2)}, u32[]{:S(2)}) collective-permute-start(bf16[256,1024]{1,0:T(8,128)(2,1)S(1)} %collective-permute-done.3.refs_2_), channel_id=1, source_target_pairs={{0,4},{4,0},{8,12},{12,8},{16,20},{20,16},{24,28},{28,24},{1,5},{5... | collective-permute-start | bytes 1572872 | tf_op jit(solution)/shard_map/ppermute | solution.py:298
  43.0 1.5 %collective-permute-start.8 = (bf16[384,256]{1,0:T(8,128)(2,1)}, bf16[384,256]{1,0:T(8,128)(2,1)S(1)}, u32[]{:S(2)}, u32[]{:S(2)}) collective-permute-start(bf16[384,256]{1,0:T(8,128)(2,1)} %get-tuple-element.37), channel_id=1, source_target_pairs={{0,2},{1,3},{2,0},{3,1},{4,6},{5,7},{6,4},{7,5},{8,10},{9,11},{10,... | collective-permute-start | bytes 589832 | tf_op jit(solution)/shard_map/ppermute | solution.py:298
  44.4 5.7 %collective-permute-done.8.refs_2_ = bf16[384,256]{1,0:T(8,128)(2,1)S(1)} collective-permute-done((bf16[384,256]{1,0:T(8,128)(2,1)}, bf16[384,256]{1,0:T(8,128)(2,1)S(1)}, u32[]{:S(2)}, u32[]{:S(2)}) %collective-permute-start.8) | collective-permute-done | bytes 196640 | tf_op jit(solution)/shard_map/ppermute | solution.py:298
  50.1 0.7 copy-done.6
  51.2 6.9 %collective-permute-done.9.refs_3_ = bf16[384,256]{1,0:T(8,128)(2,1)S(1)} collective-permute-done((bf16[384,256]{1,0:T(8,128)(2,1)}, bf16[384,256]{1,0:T(8,128)(2,1)S(1)}, u32[]{:S(2)}, u32[]{:S(2)}) %collective-permute-start.9) | collective-permute-done | bytes 196640 | tf_op jit(solution)/shard_map/ppermute | solution.py:298
  58.1 0.7 copy-done.8
  59.3 1.1 %copy-done.2 = bf16[1536,256]{1,0:T(8,128)(2,1)S(1)} copy-done((bf16[1536,256]{1,0:T(8,128)(2,1)S(1)}, bf16[1536,256]{1,0:T(8,128)(2,1)}, u32[]{:S(2)}) %copy-start.2) | copy-done | bytes 786456
  60.5 1.1 %copy-done.3 = bf16[1536,256]{1,0:T(8,128)(2,1)S(1)} copy-done((bf16[1536,256]{1,0:T(8,128)(2,1)S(1)}, bf16[1536,256]{1,0:T(8,128)(2,1)}, u32[]{:S(2)}) %copy-start.3) | copy-done | bytes 786456
  61.6 1.1 %copy-done.4 = bf16[1536,256]{1,0:T(8,128)(2,1)S(1)} copy-done((bf16[1536,256]{1,0:T(8,128)(2,1)S(1)}, bf16[1536,256]{1,0:T(8,128)(2,1)}, u32[]{:S(2)}) %copy-start.4) | copy-done | bytes 786456
  62.8 1.3 %output_kernel.1 = (bf16[384,256]{1,0:T(8,128)(2,1)S(1)}, bf16[384,256]{1,0:T(8,128)(2,1)S(1)}, bf16[384,256]{1,0:T(8,128)(2,1)S(1)}, bf16[384,256]{1,0:T(8,128)(2,1)S(1)}) custom-call(bf16[8,2,144,128]{3,2,1,0:T(8,128)(2,1)S(1)} %all-to-all-done.msgs_ref, f32[2,128,128]{2,1,0:T(8,128)S(1)} %copy-done.10, bf16[1536,256]{1,0:T(8,128)(2,1)S(1)} %copy-done.2, ...), custom_call_target="tpu_custom_call" | custom-call | flops 201326592 | bytes 3145728 | tf_op jit(solution)/shard_map/output_kernel/pallas_call | solution.py:445
  64.3 1.1 %collective-permute-start.1 = (bf16[384,256]{1,0:T(8,128)(2,1)S(1)}, bf16[384,256]{1,0:T(8,128)(2,1)S(1)}, u32[]{:S(2)}, u32[]{:S(2)}) collective-permute-start(bf16[384,256]{1,0:T(8,128)(2,1)S(1)} %get-tuple-element.33), channel_id=1, source_target_pairs={{0,2},{1,3},{2,0},{3,1},{4,6},{5,7},{6,4},{7,5},{8,10},{9,11},{10,... | collective-permute-start | bytes 589832 | tf_op jit(solution)/shard_map/ppermute | solution.py:298
  65.6 0.8 %collective-permute-start.2 = (bf16[384,256]{1,0:T(8,128)(2,1)S(1)}, bf16[384,256]{1,0:T(8,128)(2,1)S(1)}, u32[]{:S(2)}, u32[]{:S(2)}) collective-permute-start(bf16[384,256]{1,0:T(8,128)(2,1)S(1)} %get-tuple-element.34), channel_id=1, source_target_pairs={{0,3},{1,2},{2,1},{3,0},{4,7},{5,6},{6,5},{7,4},{8,11},{9,10},{10,... | collective-permute-start | bytes 589832 | tf_op jit(solution)/shard_map/ppermute | solution.py:298
  66.5 5.0 %project_kernel.2.refs_6_ = bf16[384,2048]{1,0:T(8,128)(2,1)S(1)} custom-call(bf16[384,256]{1,0:T(8,128)(2,1)S(1)} %copy-done.5, bf16[384,256]{1,0:T(8,128)(2,1)S(1)} %collective-permute-done.7.refs_1_, bf16[384,256]{1,0:T(8,128)(2,1)S(1)} %copy-done.7, bf16[384,256]{1,0:T(8,128)(2,1)S(1)} %copy-done.9, bf16[384,256]{1,0:T(8,128)(2,1)S(1)} %get-tuple-element.39.refs_4_, ...), custom_call_target="tpu_custom_call" | custom-call | flops 2415919104 | bytes 7864320 | tf_op jit(solution)/shard_map/project_kernel/pallas_call | solution.py:329
  72.1 3.1 %collective-permute-done.2.refs_1_ = bf16[384,256]{1,0:T(8,128)(2,1)S(1)} collective-permute-done((bf16[384,256]{1,0:T(8,128)(2,1)S(1)}, bf16[384,256]{1,0:T(8,128)(2,1)S(1)}, u32[]{:S(2)}, u32[]{:S(2)}) %collective-permute-start.2) | collective-permute-done | bytes 196640 | tf_op jit(solution)/shard_map/ppermute | solution.py:298
  75.1 4.4 %project_kernel.3 = bf16[384,2048]{1,0:T(8,128)(2,1)} custom-call(bf16[384,256]{1,0:T(8,128)(2,1)S(1)} %collective-permute-done.1.refs_0_, bf16[384,256]{1,0:T(8,128)(2,1)S(1)} %collective-permute-done.2.refs_1_, bf16[256,1024]{1,0:T(8,128)(2,1)S(1)} %collective-permute-done.3.refs_2_, bf16[256,1024]{1,0:T(8,128)(2,1)} %collective-permute-done.4.refs_3_, ...), custom_call_target="tpu_custom_call" | custom-call | flops 805306368 | bytes 3670016 | tf_op jit(solution)/shard_map/project_kernel/pallas_call | solution.py:329
  (39 shorter events, 3.5 us)
Async XLA Ops:
  0.0 26.3 %collective-permute-start.12 = (bf16[256,2048]{1,0:T(8,128)(2,1)}, bf16[256,2048]{1,0:T(8,128)(2,1)}, u32[]{:S(2)}, u32[]{:S(2)}) collective-permute-start(bf16[256,2048]{1,0:T(8,128)(2,1)} %refs_6_.1), channel_id=1, source_target_pairs={{0,2},{1,3},{2,0},{3,1},{4,6},{5,7},{6,4},{7,5},{8,10},{9,11},{10,... | collective-permute-start | bytes 3145736 | tf_op jit(solution)/shard_map/ppermute | solution.py:298
  1.5 62.6 %collective-permute-start.11 = (bf16[256,2048]{1,0:T(8,128)(2,1)}, bf16[256,2048]{1,0:T(8,128)(2,1)}, u32[]{:S(2)}, u32[]{:S(2)}) collective-permute-start(bf16[256,2048]{1,0:T(8,128)(2,1)} %refs_6_.1), channel_id=1, source_target_pairs={{0,1},{1,0},{2,3},{3,2},{4,5},{5,4},{6,7},{7,6},{8,9},{9,8},{10,11... | collective-permute-start | bytes 3145736 | tf_op jit(solution)/shard_map/ppermute | solution.py:298
  2.3 24.0 %collective-permute-start = (bf16[16,2048]{1,0:T(8,128)(2,1)S(1)}, bf16[16,2048]{1,0:T(8,128)(2,1)S(1)}, u32[]{:S(2)}, u32[]{:S(2)}) collective-permute-start(bf16[16,2048]{1,0:T(8,128)(2,1)S(1)} %slice.3), channel_id=1, source_target_pairs={{0,4},{4,8},{8,12},{12,16},{16,20},{20,24},{24,28},{1,5},{5,9},{9,... | collective-permute-start | bytes 196616 | tf_op jit(solution)/shard_map/ppermute | solution.py:408
  5.8 58.5 %collective-permute-start.14 = (bf16[256,2048]{1,0:T(8,128)(2,1)}, bf16[256,2048]{1,0:T(8,128)(2,1)}, u32[]{:S(2)}, u32[]{:S(2)}) collective-permute-start(bf16[256,2048]{1,0:T(8,128)(2,1)} %refs_10_.1), channel_id=1, source_target_pairs={{0,1},{1,0},{2,3},{3,2},{4,5},{5,4},{6,7},{7,6},{8,9},{9,8},{10,11... | collective-permute-start | bytes 3145736 | tf_op jit(solution)/shard_map/ppermute | solution.py:298
  7.9 33.5 %collective-permute-start.3 = (bf16[256,1024]{1,0:T(8,128)(2,1)}, bf16[256,1024]{1,0:T(8,128)(2,1)S(1)}, u32[]{:S(2)}, u32[]{:S(2)}) collective-permute-start(bf16[256,1024]{1,0:T(8,128)(2,1)} %constant_dynamic-slice_fusion), channel_id=1, source_target_pairs={{0,2},{1,3},{2,0},{3,1},{4,6},{5,7},{6,4},{7,5},{8,10},{9,11},{10,... | collective-permute-start | bytes 1572872 | tf_op jit(solution)/shard_map/ppermute | solution.py:298
  19.1 40.3 %all-to-all-start = ((bf16[8,2,144,128]{3,2,1,0:T(8,128)(2,1)}), bf16[8,2,144,128]{3,2,1,0:T(8,128)(2,1)S(1)}, u32[]{:S(2)}, u32[]{:S(2)}) async-start(bf16[8,2,144,128]{3,2,1,0:T(8,128)(2,1)} %get-tuple-element.23), calls=%async_computation | async-start | bytes 1179648 | tf_op jit(solution)/shard_map/all_to_all | solution.py:410
  26.3 40.1 %collective-permute-start.13 = (bf16[256,2048]{1,0:T(8,128)(2,1)}, bf16[256,2048]{1,0:T(8,128)(2,1)}, u32[]{:S(2)}, u32[]{:S(2)}) collective-permute-start(bf16[256,2048]{1,0:T(8,128)(2,1)} %collective-permute-done.12.refs_8_), channel_id=1, source_target_pairs={{0,1},{1,0},{2,3},{3,2},{4,5},{5,4},{6,7},{7,6},{8,9},{9,8},{10,11... | collective-permute-start | bytes 3145736 | tf_op jit(solution)/shard_map/ppermute | solution.py:298
  27.0 32.4 %copy-start.10 = (f32[2,128,128]{2,1,0:T(8,128)S(1)}, f32[2,128,128]{2,1,0:T(8,128)}, u32[]{:S(2)}) copy-start(f32[2,128,128]{2,1,0:T(8,128)} %init_ref.1) | copy-start | bytes 393220
  40.8 25.6 %copy-start = (bf16[256,2048]{1,0:T(8,128)(2,1)S(1)}, bf16[256,2048]{1,0:T(8,128)(2,1)}, u32[]{:S(2)}) copy-start(bf16[256,2048]{1,0:T(8,128)(2,1)} %refs_10_.1) | copy-start | bytes 3145732
  40.8 25.6 %copy-start.1 = (bf16[256,2048]{1,0:T(8,128)(2,1)S(1)}, bf16[256,2048]{1,0:T(8,128)(2,1)}, u32[]{:S(2)}) copy-start(bf16[256,2048]{1,0:T(8,128)(2,1)} %refs_6_.1) | copy-start | bytes 3145732
  40.9 2.1 %collective-permute-start.7 = (bf16[384,256]{1,0:T(8,128)(2,1)}, bf16[384,256]{1,0:T(8,128)(2,1)S(1)}, u32[]{:S(2)}, u32[]{:S(2)}) collective-permute-start(bf16[384,256]{1,0:T(8,128)(2,1)} %get-tuple-element.36), channel_id=1, source_target_pairs={{0,1},{1,0},{2,3},{3,2},{4,5},{5,4},{6,7},{7,6},{8,9},{9,8},{10,11... | collective-permute-start | bytes 589832 | tf_op jit(solution)/shard_map/ppermute | solution.py:298
  41.4 17.5 %collective-permute-start.4 = (bf16[256,1024]{1,0:T(8,128)(2,1)S(1)}, bf16[256,1024]{1,0:T(8,128)(2,1)}, u32[]{:S(2)}, u32[]{:S(2)}) collective-permute-start(bf16[256,1024]{1,0:T(8,128)(2,1)S(1)} %collective-permute-done.3.refs_2_), channel_id=1, source_target_pairs={{0,4},{4,0},{8,12},{12,8},{16,20},{20,16},{24,28},{28,24},{1,5},{5... | collective-permute-start | bytes 1572872 | tf_op jit(solution)/shard_map/ppermute | solution.py:298
  43.0 7.1 %collective-permute-start.8 = (bf16[384,256]{1,0:T(8,128)(2,1)}, bf16[384,256]{1,0:T(8,128)(2,1)S(1)}, u32[]{:S(2)}, u32[]{:S(2)}) collective-permute-start(bf16[384,256]{1,0:T(8,128)(2,1)} %get-tuple-element.37), channel_id=1, source_target_pairs={{0,2},{1,3},{2,0},{3,1},{4,6},{5,7},{6,4},{7,5},{8,10},{9,11},{10,... | collective-permute-start | bytes 589832 | tf_op jit(solution)/shard_map/ppermute | solution.py:298
  50.8 7.4 %collective-permute-start.9 = (bf16[384,256]{1,0:T(8,128)(2,1)}, bf16[384,256]{1,0:T(8,128)(2,1)S(1)}, u32[]{:S(2)}, u32[]{:S(2)}) collective-permute-start(bf16[384,256]{1,0:T(8,128)(2,1)} %get-tuple-element.38), channel_id=1, source_target_pairs={{0,3},{1,2},{2,1},{3,0},{4,7},{5,6},{6,5},{7,4},{8,11},{9,10},{10,... | collective-permute-start | bytes 589832 | tf_op jit(solution)/shard_map/ppermute | solution.py:298
  58.8 12.7 %collective-permute-start.5 = (bf16[256,1024]{1,0:T(8,128)(2,1)S(1)}, bf16[256,1024]{1,0:T(8,128)(2,1)}, u32[]{:S(2)}, u32[]{:S(2)}) collective-permute-start(bf16[256,1024]{1,0:T(8,128)(2,1)S(1)} %collective-permute-done.3.refs_2_), channel_id=1, source_target_pairs={{0,1},{1,0},{2,3},{3,2},{4,5},{5,4},{6,7},{7,6},{8,9},{9,8},{10,11... | collective-permute-start | bytes 1572872 | tf_op jit(solution)/shard_map/ppermute | solution.py:298
  58.9 16.2 %collective-permute-start.6 = (bf16[256,1024]{1,0:T(8,128)(2,1)}, bf16[256,1024]{1,0:T(8,128)(2,1)}, u32[]{:S(2)}, u32[]{:S(2)}) collective-permute-start(bf16[256,1024]{1,0:T(8,128)(2,1)} %collective-permute-done.4.refs_3_), channel_id=1, source_target_pairs={{0,1},{1,0},{2,3},{3,2},{4,5},{5,4},{6,7},{7,6},{8,9},{9,8},{10,11... | collective-permute-start | bytes 1572872 | tf_op jit(solution)/shard_map/ppermute | solution.py:298
  59.3 1.1 %copy-start.2 = (bf16[1536,256]{1,0:T(8,128)(2,1)S(1)}, bf16[1536,256]{1,0:T(8,128)(2,1)}, u32[]{:S(2)}) copy-start(bf16[1536,256]{1,0:T(8,128)(2,1)} %get-tuple-element.30.local_ref) | copy-start | bytes 2359300
  60.5 1.1 %copy-start.3 = (bf16[1536,256]{1,0:T(8,128)(2,1)S(1)}, bf16[1536,256]{1,0:T(8,128)(2,1)}, u32[]{:S(2)}) copy-start(bf16[1536,256]{1,0:T(8,128)(2,1)} %get-tuple-element.31.qtot_ref) | copy-start | bytes 2359300
  62.7 3.7 %copy-start.5 = (bf16[384,256]{1,0:T(8,128)(2,1)S(1)}, bf16[384,256]{1,0:T(8,128)(2,1)}, u32[]{:S(2)}) copy-start(bf16[384,256]{1,0:T(8,128)(2,1)} %get-tuple-element.35.refs_0_) | copy-start | bytes 589828
  62.7 3.7 %copy-start.7 = (bf16[384,256]{1,0:T(8,128)(2,1)S(1)}, bf16[384,256]{1,0:T(8,128)(2,1)}, u32[]{:S(2)}) copy-start(bf16[384,256]{1,0:T(8,128)(2,1)} %copy-done.6) | copy-start | bytes 589828
  62.8 3.7 %copy-start.9 = (bf16[384,256]{1,0:T(8,128)(2,1)S(1)}, bf16[384,256]{1,0:T(8,128)(2,1)}, u32[]{:S(2)}) copy-start(bf16[384,256]{1,0:T(8,128)(2,1)} %copy-done.8) | copy-start | bytes 589828
  64.1 1.5 %collective-permute-start.10 = (bf16[384,256]{1,0:T(8,128)(2,1)S(1)}, bf16[384,256]{1,0:T(8,128)(2,1)S(1)}, u32[]{:S(2)}, u32[]{:S(2)}) collective-permute-start(bf16[384,256]{1,0:T(8,128)(2,1)S(1)} %get-tuple-element.40), channel_id=1, source_target_pairs={{0,1},{1,0},{2,3},{3,2},{4,5},{5,4},{6,7},{7,6},{8,9},{9,8},{10,11... | collective-permute-start | bytes 589832 | tf_op jit(solution)/shard_map/ppermute | solution.py:298
  64.3 7.8 %collective-permute-start.1 = (bf16[384,256]{1,0:T(8,128)(2,1)S(1)}, bf16[384,256]{1,0:T(8,128)(2,1)S(1)}, u32[]{:S(2)}, u32[]{:S(2)}) collective-permute-start(bf16[384,256]{1,0:T(8,128)(2,1)S(1)} %get-tuple-element.33), channel_id=1, source_target_pairs={{0,2},{1,3},{2,0},{3,1},{4,6},{5,7},{6,4},{7,5},{8,10},{9,11},{10,... | collective-permute-start | bytes 589832 | tf_op jit(solution)/shard_map/ppermute | solution.py:298
  65.6 9.5 %collective-permute-start.2 = (bf16[384,256]{1,0:T(8,128)(2,1)S(1)}, bf16[384,256]{1,0:T(8,128)(2,1)S(1)}, u32[]{:S(2)}, u32[]{:S(2)}) collective-permute-start(bf16[384,256]{1,0:T(8,128)(2,1)S(1)} %get-tuple-element.34), channel_id=1, source_target_pairs={{0,3},{1,2},{2,1},{3,0},{4,7},{5,6},{6,5},{7,4},{8,11},{9,10},{10,... | collective-permute-start | bytes 589832 | tf_op jit(solution)/shard_map/ppermute | solution.py:298
  (4 other events, 3.1 us)

commit v3 on v2

v3 whole, which is shorter than its diff:
```python
import functools

import jax
import jax.numpy as jnp
from jax import lax
from jax.experimental import pallas as pl
from jax.experimental.pallas import tpu as pltpu
from jax.sharding import PartitionSpec as P


norm_eps = 1e-05
halo_rows = 16
chunk = 128
msg_pad = 16
f32 = jnp.float32
bf16 = jnp.bfloat16


def dot(a, b, dims=((1,), (0,))):
    return lax.dot_general(a, b, (dims, ((), ())), preferred_element_type=f32)


def sigmoid(x):
    return 1.0 / (1.0 + jnp.exp(-x))


def lower_triangle(size):
    row = lax.broadcasted_iota(jnp.int32, (size, size), 0)
    col = lax.broadcasted_iota(jnp.int32, (size, size), 1)
    return row >= col


def fold_gain(gain_ref, weight_refs, folded):
    lanes = gain_ref.shape[1]
    for b in range(gain_ref.shape[0]):
        rows = slice(b * lanes, (b + 1) * lanes)
        column = jnp.broadcast_to(gain_ref[b : b + 1, :], (lanes, lanes)).T
        at = 0
        for ref in weight_refs:
            for j in range(0, ref.shape[1], lanes):
                part = ref[rows, j : j + lanes].astype(f32) * column
                folded[rows, at : at + lanes] = part.astype(bf16)
                at += lanes


def row_scale(x):
    wide = x.astype(f32)
    return lax.rsqrt(jnp.mean(wide * wide, axis=-1, keepdims=True) + norm_eps)


def split(x):
    high = x.astype(bf16)
    return high, (x - high.astype(f32)).astype(bf16)


def stage_rows(stage, first, value):
    quarter = stage.shape[1]
    slot = (first // quarter) ^ lax.axis_index("tp")
    at = pl.multiple_of(first % quarter, chunk)
    stage[slot, pl.ds(at, value.shape[0]), :] = value


def unstage(stage, refs):
    @pl.when(pl.program_id(0) == pl.num_programs(0) - 1)
    def _():
        for k, ref in enumerate(refs):
            ref[...] = stage[k]


def state_kernel(
    x_ref, halo_ref, gain_ref, fw_ref, vw_ref, pw_ref, mix_ref, pool_scale_ref, lb_ref,
    extra_ref, weight_ref, scale_ref, kept_ref, start_ref, rows_ref, msg_ref, half_ref, *rest,
):
    ypool_refs, (folded, state, total, tail, band, stage) = rest[:-6], rest[-6:]
    step = pl.program_id(0)
    first_pos = lax.axis_index("sp") * (x_ref.shape[0] * pl.num_programs(0))
    window = jnp.left_shift(2, lax.axis_index("tp") * mix_ref.shape[0])
    heads, head_k = state.shape[0], state.shape[1]
    tile = x_ref.shape[0]
    channels = fw_ref.shape[1]

    @pl.when(step == 0)
    def _():
        state[...] = jnp.zeros_like(state)
        total[...] = jnp.zeros_like(total)
        half_ref[...] = weight_ref[...]
        fold_gain(gain_ref, (fw_ref, vw_ref, pw_ref), folded)
        halo = halo_ref[...]
        tail[...] = (dot(halo, folded[:, 2 * channels :]) * row_scale(halo)).astype(bf16)
        row = lax.broadcasted_iota(jnp.int32, band.shape, 0)
        col = lax.broadcasted_iota(jnp.int32, band.shape, 1) - halo_rows
        back = row - col
        band[...] = ((back >= 0) & (back < window)).astype(f32).astype(bf16)

    gap = 1.0 - lb_ref[...]
    pick = (
        lax.broadcasted_iota(jnp.int32, (heads, channels), 1) // head_k
        == lax.broadcasted_iota(jnp.int32, (heads, channels), 0)
    ).astype(f32).astype(bf16)
    triangle = lower_triangle(chunk).astype(f32).astype(bf16)
    triangle = jnp.concatenate([triangle, triangle], axis=1)
    first = ((0,), (0,))

    def project_block(b):
        return dot(x_ref[b * 256 : (b + 1) * 256, :], folded[...])

    extra_high, extra_low = split(extra_ref[...])
    extras = dot(extra_high, pick, first) + dot(extra_low, pick, first)
    tail_rows = tail[...]
    ahead = project_block(0)
    scale_ref[...] = jnp.broadcast_to(row_scale(x_ref[...]), scale_ref.shape)
    for b in range(tile // 256):
        block = slice(b * 256, (b + 1) * 256)
        raw = ahead
        if (b + 1) * 256 < tile:
            ahead = project_block(b + 1)
        scale = scale_ref[block, :]
        scales = jnp.concatenate([scale] * (channels // scale.shape[1]), axis=1)
        forget = raw[:, :channels] * scales
        value = (raw[:, channels : 2 * channels] * scales).astype(bf16)
        kept_ref[block, 2 * channels :] = value
        pool_in = (raw[:, 2 * channels :] * scales).astype(bf16)
        key = gap / (1.0 + jnp.exp(forget))
        extra = extras[block]
        high, low = split(jnp.log(1.0 - key) + extra)
        for j in range(256 // chunk):
            c = b * (256 // chunk) + j
            part = slice(j * chunk, (j + 1) * chunk)
            span = slice(c * chunk, (c + 1) * chunk)
            cum = dot(triangle, jnp.concatenate([high[part], low[part]], axis=0))
            middle = cum[chunk // 2 - 1 : chunk // 2]
            last = cum[chunk - 1 :]
            kept_ref[span, channels : 2 * channels] = jnp.exp(cum - middle).astype(bf16)
            key_dec = key[part] * jnp.exp(middle - cum)
            kept_ref[span, :channels] = key_dec.astype(bf16)
            key_end = (key_dec * jnp.exp(last - middle)).astype(bf16)
            before = total[...]
            rows_ref[c] = jnp.concatenate(
                [jnp.exp(middle), jnp.exp(before), jnp.zeros((6, middle.shape[1]), f32)], axis=0
            )
            total[...] = before + last
            whole = jnp.exp(last)
            for h in range(heads):
                lanes = slice(h * head_k, (h + 1) * head_k)
                old = state[h]
                start_ref[c, h] = old.astype(bf16)
                contrib = dot(value[part, lanes], key_end[:, lanes], first)
                state[h] = old * whole[:, lanes] + contrib

            pool_part = pool_in[part]
            sums = dot(band[...], jnp.concatenate([tail_rows, pool_part], axis=0))
            tail_rows = pool_part[chunk - halo_rows :]
            position = (
                first_pos + step * tile + c * chunk
                + lax.broadcasted_iota(jnp.int32, (chunk, 1), 0)
            )
            count = jnp.minimum(position + 1, window).astype(f32)
            pooled = (sums * (1.0 / count) - pool_part.astype(f32)).astype(bf16)
            y_pool = (dot(pooled, mix_ref[0]) * pool_scale_ref[...]).astype(bf16)
            stage_rows(stage, step * tile + c * chunk, y_pool)
    tail[...] = tail_rows
    unstage(stage, ypool_refs)

    @pl.when(step == pl.num_programs(0) - 1)
    def _():
        decay_high, decay_low = split(jnp.exp(total[...]))
        for h in range(heads):
            lanes = slice(h * head_k, (h + 1) * head_k)
            ending = state[h].astype(bf16)
            decays = jnp.concatenate(
                [
                    decay_high[:, lanes].astype(f32),
                    decay_low[:, lanes].astype(f32),
                    jnp.zeros((msg_pad - 2, head_k), f32),
                ],
                axis=0,
            ).astype(bf16)
            for i in range(msg_ref.shape[0]):
                msg_ref[i, h, :head_k, :] = ending
                msg_ref[i, h, head_k:, :] = decays


def local_kernel(
    x_ref, gain_ref, qw_ref, ow_ref, recur_gain_ref, scale_ref, kept_ref, start_ref, rows_ref,
    parts_ref, folded,
):
    step = pl.program_id(0)
    tile = x_ref.shape[0]
    channels = qw_ref.shape[1]
    head_k = start_ref.shape[-1]
    heads = start_ref.shape[1]

    @pl.when(step == 0)
    def _():
        fold_gain(gain_ref, (qw_ref, ow_ref), folded)

    causal = lower_triangle(chunk)

    def project_block(b):
        return dot(x_ref[b * 256 : (b + 1) * 256, :], folded[...])

    ahead = project_block(0)
    for b in range(tile // 256):
        block = slice(b * 256, (b + 1) * 256)
        raw = ahead
        if (b + 1) * 256 < tile:
            ahead = project_block(b + 1)
        scale = scale_ref[block, :]
        scales = jnp.concatenate([scale] * (channels // scale.shape[1]), axis=1)
        query = raw[:, :channels] * scales
        outgate = raw[:, channels:] * scales
        gate = outgate * sigmoid(outgate) * recur_gain_ref[...]
        parts_ref[block, 2 * channels :] = gate.astype(bf16)
        query = query * sigmoid(query)
        for j in range(256 // chunk):
            c = b * (256 // chunk) + j
            part = slice(j * chunk, (j + 1) * chunk)
            span = slice(c * chunk, (c + 1) * chunk)
            query_dec = query[part] * kept_ref[span, channels : 2 * channels].astype(f32)
            query_low = query_dec.astype(bf16)
            query_abs = query_dec * rows_ref[c, 0:1, :]
            parts_ref[span, channels : 2 * channels] = (query_abs * rows_ref[c, 1:2, :]).astype(bf16)
            query_abs = query_abs.astype(bf16)
            for h in range(heads):
                lanes = slice(h * head_k, (h + 1) * head_k)
                key = kept_ref[span, lanes]
                value = kept_ref[span, 2 * channels + h * head_k : 2 * channels + (h + 1) * head_k]
                scores = dot(query_low[:, lanes], key, ((1,), (1,)))
                scores = jnp.where(causal, scores, 0.0).astype(bf16)
                within = dot(scores, value)
                earlier = dot(query_abs[:, lanes], start_ref[c, h], ((1,), (1,)))
                parts_ref[span, lanes] = (within + earlier).astype(bf16)


def output_kernel(msgs_ref, init_ref, parts_ref, *rest):
    y_refs, carried = rest[:-1], rest[-1]
    channels = parts_ref.shape[1] // 3
    head_k = init_ref.shape[-1]
    heads = init_ref.shape[0]

    @pl.when(pl.program_id(0) == 0)
    def _():
        for h in range(heads):
            def step(i, state):
                decay = (
                    msgs_ref[i, h, head_k : head_k + 1, :].astype(f32)
                    + msgs_ref[i, h, head_k + 1 : head_k + 2, :].astype(f32)
                )
                return state * decay + msgs_ref[i, h, :head_k, :].astype(f32)

            carried[h] = lax.fori_loop(0, lax.axis_index("sp"), step, init_ref[h].T).astype(bf16)

    pieces = []
    for h in range(heads):
        local, qtot, gate = [
            parts_ref[:, k * channels + h * head_k : k * channels + (h + 1) * head_k]
            for k in range(3)
        ]
        recur = local.astype(f32) + dot(qtot, carried[h], ((1,), (1,)))
        mean = jnp.mean(recur * recur, axis=-1, keepdims=True)
        scaled = recur * lax.rsqrt(mean + norm_eps)
        pieces.append((scaled * gate.astype(f32)).astype(bf16))
    y_recur = jnp.concatenate(pieces, axis=1)
    for k, ref in enumerate(y_refs):
        @pl.when(pl.program_id(0) == k)
        def _():
            ref[...] = y_recur


def project_kernel(counts, *refs):
    refs = list(refs)
    seen = [refs.pop(0) for _ in counts]
    groups = [[refs.pop(0) for _ in range(count)] for count in counts]
    out_ref = refs.pop()
    total = refs.pop()[...].astype(f32) if refs else None
    for piece, group in zip(seen, groups):
        weight = group[0][...]
        if len(group) > 1:
            other, even = group[1][...], lax.axis_index("sp") % 2 == 0
            weight = jnp.concatenate(
                [jnp.where(even, weight, other), jnp.where(even, other, weight)], axis=0
            )
        term = dot(piece[...], weight)
        total = term if total is None else total + term
    out_ref[...] = total.astype(out_ref.dtype)


def fixed(*shape):
    return pl.BlockSpec(shape, lambda *_: (0,) * len(shape))


def moving(*shape):
    return pl.BlockSpec(shape, lambda i, *_: (i,) + (0,) * (len(shape) - 1))


def limits(mib):
    return pltpu.CompilerParams(
        dimension_semantics=("arbitrary",), vmem_limit_bytes=mib * 1024 * 1024
    )


def swapped(array, axis, bit):
    devices = lax.axis_size(axis)
    return lax.ppermute(array, axis, [(i, i ^ bit) for i in range(devices)])


def columns(size, block):
    return pl.BlockSpec((size, block), lambda i: (0, i))


def project(seen, weights, base, out_type):
    rows, channels = seen[0].shape
    width = weights[0][0].shape[1]
    block = width // 2
    extra = [] if base is None else [base]
    flat = [array for group in weights for array in group]
    counts = tuple(len(group) for group in weights)
    specs = [columns(channels // count, block) for count in counts for _ in range(count)]
    return pl.pallas_call(
        functools.partial(project_kernel, counts),
        grid=(width // block,),
        in_specs=[fixed(rows, channels)] * len(seen) + specs
        + [columns(rows, block)] * len(extra),
        out_specs=columns(rows, block),
        out_shape=jax.ShapeDtypeStruct((rows, width), out_type),
        compiler_params=limits(32),
        cost_estimate=pl.CostEstimate(
            flops=2 * len(seen) * rows * channels * width, transcendentals=0,
            bytes_accessed=2 * (len(weights) * channels * width + rows * width),
        ),
        name="project_kernel",
    )(*seen, *flat, *extra)


def per_device(
    inputs, norm_gain, pool_weight, query_weight, forget_weight, value_weight, outgate_weight,
    pool_mix, pool_scale, lower_bound, extra_decay, recur_gain, init_state, out_pool, out_recur,
):
    rows, width = inputs.shape
    heads, head_k = init_state.shape[:2]
    channels = query_weight.shape[1]
    sp, tp = lax.axis_size("sp"), lax.axis_size("tp")
    quarter, tile = rows // tp, 4 * chunk
    steps, chunks = rows // tile, tile // chunk
    lanes = 128
    gain = norm_gain.reshape(width // lanes, lanes)
    sds = jax.ShapeDtypeStruct

    assert tp == 4 and sp % 2 == 0
    far = swapped(out_pool, "tp", 2)
    w_pool = [
        [out_pool], [swapped(out_pool, "tp", 1)], [far],
        [swapped(far, "tp", 1)],
    ]
    halo = lax.ppermute(inputs[rows - halo_rows :], "sp", [(i, i + 1) for i in range(sp - 1)])
    scale, kept, starts, row_info, msgs, half, *y_pool = pl.pallas_call(
        state_kernel,
        grid=(steps,),
        in_specs=[
            moving(tile, width), fixed(halo_rows, width), fixed(*gain.shape),
            fixed(width, channels), fixed(width, channels), fixed(width, channels),
            fixed(*pool_mix.shape), fixed(1, channels), fixed(1, channels),
            pl.BlockSpec((heads, tile), lambda i: (0, i)),
            pl.BlockSpec((channels // 2, width), lambda i: (lax.axis_index("sp") % 2, 0)),
        ],
        out_specs=[
            moving(tile, lanes), moving(tile, 3 * channels),
            moving(chunks, heads, head_k, head_k), moving(chunks, 8, channels),
            fixed(sp, heads, head_k + msg_pad, head_k), fixed(channels // 2, width),
        ] + [fixed(quarter, channels)] * tp,
        out_shape=[
            sds((rows, lanes), f32), sds((rows, 3 * channels), bf16),
            sds((rows // chunk, heads, head_k, head_k), bf16),
            sds((rows // chunk, 8, channels), f32),
            sds((sp, heads, head_k + msg_pad, head_k), bf16), sds((channels // 2, width), bf16),
        ] + [sds((quarter, channels), bf16)] * tp,
        scratch_shapes=[
            pltpu.VMEM((width, 3 * channels), bf16), pltpu.VMEM((heads, head_k, head_k), f32),
            pltpu.VMEM((1, channels), f32), pltpu.VMEM((halo_rows, channels), bf16),
            pltpu.VMEM((chunk, chunk + halo_rows), bf16),
            pltpu.VMEM((tp, quarter, channels), bf16),
        ],
        compiler_params=limits(58),
        cost_estimate=pl.CostEstimate(
            flops=6 * rows * width * channels, transcendentals=0, bytes_accessed=2 * rows * width
        ),
        name="state_kernel",
    )(
        inputs, halo, gain, forget_weight, value_weight, pool_weight, pool_mix, pool_scale[None],
        lower_bound[None], extra_decay.T, out_recur,
    )
    fetched = swapped(half, "tp", 2)
    handed = swapped(fetched, "sp", 1)
    cross_fetched = swapped(fetched, "tp", 1)
    cross_handed = swapped(handed, "tp", 1)
    w_recur = [
        [out_recur], [swapped(out_recur, "tp", 1)], [fetched, handed],
        [cross_fetched, cross_handed],
    ]


    def exchange(pieces):
        return [pieces[0]] + [swapped(pieces[k], "tp", k) for k in range(1, tp)]

    msgs = lax.all_to_all(msgs, "sp", split_axis=0, concat_axis=0, tiled=True)
    pool_seen = exchange(y_pool)
    parts = pl.pallas_call(
        local_kernel,
        grid=(steps,),
        in_specs=[
            moving(tile, width), fixed(*gain.shape), fixed(width, channels),
            fixed(width, channels), fixed(1, channels),
            moving(tile, lanes), moving(tile, 3 * channels),
            moving(chunks, heads, head_k, head_k), moving(chunks, 8, channels),
        ],
        out_specs=moving(tile, 3 * channels),
        out_shape=sds((rows, 3 * channels), bf16),
        scratch_shapes=[pltpu.VMEM((width, 2 * channels), bf16)],
        compiler_params=limits(54),
        cost_estimate=pl.CostEstimate(
            flops=4 * rows * width * channels, transcendentals=0, bytes_accessed=2 * rows * width
        ),
        name="local_kernel",
    )(
        inputs, gain, query_weight, outgate_weight, recur_gain[None], scale, kept, starts, row_info,
    )

    def outputs(flip):
        part = pl.BlockSpec(
            (quarter, 3 * channels), lambda i: (lax.axis_index("tp") ^ (flip + i), 0)
        )
        return pl.pallas_call(
            output_kernel,
            grid=(2,),
            in_specs=[fixed(*msgs.shape), fixed(*init_state.shape), part],
            out_specs=[fixed(quarter, channels)] * 2,
            out_shape=[sds((quarter, channels), bf16)] * 2,
            scratch_shapes=[pltpu.VMEM((heads, head_k, head_k), bf16)],
            compiler_params=limits(40),
            cost_estimate=pl.CostEstimate(
                flops=2 * rows * head_k * channels, transcendentals=0,
                bytes_accessed=4 * rows * channels,
            ),
            name="output_kernel",
        )(msgs, init_state, parts)

    far_y = outputs(2)
    near_y = outputs(0)
    y_recur = near_y + far_y
    recur_seen = exchange(y_recur)
    partial_sum = project(pool_seen + recur_seen[:2], w_pool + w_recur[:2], None, bf16)
    return project(recur_seen[2:], w_recur[2:], partial_sum, bf16)


def solution(mesh):
    in_specs = (
        P("sp", None), P(), P(None, "tp"), P(None, "tp"), P(None, "tp"), P(None, "tp"),
        P(None, "tp"), P("tp", None, None), P("tp"), P("tp"), P("sp", "tp"), P("tp"),
        P("tp", None, None), P("tp", None), P("tp", None),
    )

    return jax.shard_map(
        per_device, mesh=mesh, in_specs=in_specs, out_specs=P(("sp", "tp"), None), check_vma=False
    )
```

time: 80.9 us -> 83.9 us (1.037)
  waiting for transfers between devices: 18.5 us -> 26.2 us
  local copies, waits for them, and re-layouts: 8.11 us -> 4.5 us
  starting transfers between devices: 17.6 us -> 15.4 us
  Pallas kernels: 35.2 us -> 36.1 us
    pallas_call x1, Pallas kernels: 10.6 us -> 15.4 us  [per_device(): pl.pallas_call(state_kernel, grid=(steps,), in_specs=[moving(tile, width)...]
    ppermute x14, waiting for transfers between devices: 18.5 us -> 22.6 us  [swapped(): return lax.ppermute(array, axis, [(i, i ^ bit) for i in range(devices)])]
    ppermute x1, waiting for transfers between devices: 0.01 us -> 3.62 us  [per_device(): lax.ppermute(inputs[rows - halo_rows:], 'sp', [(i, i + 1) for i in range(...]
    pallas_call x1, Pallas kernels: 13.8 us -> 10.9 us  [per_device(): pl.pallas_call(local_kernel, grid=(steps,), in_specs=[moving(tile, width)...]
    ppermute x14, starting transfers between devices: 8.95 us -> 6.72 us  [swapped(): return lax.ppermute(array, axis, [(i, i ^ bit) for i in range(devices)])]
    dynamic_slice x1 -> x0, local copies, waits for them, and re-layouts: 1.86 us -> none  [per_device(): lax.dynamic_slice_in_dim(out_recur, lax.axis_index('sp') % 2 * half_width...]
    unnamed x24 -> x20, local copies, waits for them, and re-layouts: 5.41 us -> 3.66 us
    pallas_call x2, Pallas kernels: 9.42 us -> 7.68 us  [project(): pl.pallas_call(functools.partial(project_kernel, counts), grid=(width //...]
  transfers between devices with their start and end apart: 16 -> 16, of which waited for: 6 -> 6; matrix products, arithmetic and copies ran while one was open for 3% -> 1% of each run, Pallas kernels for 39% -> 40%
where the time goes in v3:
time: 83.9 us; the launch traced here: 82.3 us
  Pallas kernels  36.1 us (43%)
  waiting for transfers between devices  26.2 us (31%)
  starting transfers between devices  15.4 us (18%)
  local copies, waits for them, and re-layouts  4.5 us (5%)
    ppermute x14, waiting for transfers between devices, swapped(): return lax.ppermute(array, axis, [(i, i ^ bit) for i in range(devices)])  22.6 us
    pallas_call x1, Pallas kernels, per_device(): pl.pallas_call(state_kernel, grid=(steps,), in_specs=[moving(tile, width)...  15.4 us
    pallas_call x1, Pallas kernels, per_device(): pl.pallas_call(local_kernel, grid=(steps,), in_specs=[moving(tile, width)...  10.9 us
    pallas_call x2, Pallas kernels, project(): pl.pallas_call(functools.partial(project_kernel, counts), grid=(width //...  7.68 us
    ppermute x14, starting transfers between devices, swapped(): return lax.ppermute(array, axis, [(i, i ^ bit) for i in range(devices)])  6.72 us
    all_to_all x1, starting transfers between devices, per_device(): msgs = lax.all_to_all(msgs, 'sp', split_axis=0, concat_axis=0, tiled=True)  5.27 us
    unnamed x20, local copies, waits for them, and re-layouts  3.66 us
    ppermute x1, waiting for transfers between devices, per_device(): lax.ppermute(inputs[rows - halo_rows:], 'sp', [(i, i + 1) for i in range(...  3.62 us
  transfers between devices with their start and end apart: 16, of which 6 were waited for; matrix products, arithmetic and copies ran while one was open for 1% of the time, Pallas kernels for 40%

profile of v3, /device:TPU:16, one launch (start us, length us, event | category | flops | bytes accessed | tf_op | source)
XLA Modules:
  0.0 82.3 jit_solution(16021032312303911068)
XLA Ops:
  0.0 1.5 %collective-permute-start.12 = (bf16[256,2048]{1,0:T(8,128)(2,1)}, bf16[256,2048]{1,0:T(8,128)(2,1)}, u32[]{:S(2)}, u32[]{:S(2)}) collective-permute-start(bf16[256,2048]{1,0:T(8,128)(2,1)} %refs_6_.1), channel_id=1, source_target_pairs={{0,2},{1,3},{2,0},{3,1},{4,6},{5,7},{6,4},{7,5},{8,10},{9,11},{10,... | collective-permute-start | bytes 3145736 | tf_op jit(solution)/shard_map/ppermute | solution.py:304
  1.5 0.8 %slice.3 = bf16[16,2048]{1,0:T(8,128)(2,1)S(1)} slice(bf16[1536,2048]{1,0:T(8,128)(2,1)} %x_ref.3), slice={[1520:1536], [0:2048]} | slice | bytes 131072 | tf_op jit(solution)/shard_map/slice | solution.py:355
  2.3 3.4 %collective-permute-start = (bf16[16,2048]{1,0:T(8,128)(2,1)S(1)}, bf16[16,2048]{1,0:T(8,128)(2,1)S(1)}, u32[]{:S(2)}, u32[]{:S(2)}) collective-permute-start(bf16[16,2048]{1,0:T(8,128)(2,1)S(1)} %slice.3), channel_id=1, source_target_pairs={{0,4},{4,8},{8,12},{12,16},{16,20},{20,24},{24,28},{1,5},{5,9},{9,... | collective-permute-start | bytes 196616 | tf_op jit(solution)/shard_map/ppermute | solution.py:355
  5.8 3.6 %collective-permute-done.halo_ref = bf16[16,2048]{1,0:T(8,128)(2,1)S(1)} collective-permute-done((bf16[16,2048]{1,0:T(8,128)(2,1)S(1)}, bf16[16,2048]{1,0:T(8,128)(2,1)S(1)}, u32[]{:S(2)}, u32[]{:S(2)}) %collective-permute-start) | collective-permute-done | bytes 65568 | tf_op jit(solution)/shard_map/ppermute | solution.py:355
  9.4 0.6 copy-done.9
  10.0 15.4 %state_kernel.1 = (f32[1536,128]{1,0:T(8,128)}, bf16[1536,768]{1,0:T(8,128)(2,1)}, bf16[12,2,128,128]{3,2,1,0:T(8,128)(2,1)}, f32[12,8,256]{2,1,0:T(8,128)}, bf1...) custom-call(bf16[1536,2048]{1,0:T(8,128)(2,1)} %x_ref.3, ...), custom_call_target="tpu_custom_call" | custom-call | flops 4831838208 | bytes 6291456 | tf_op jit(solution)/shard_map/state_kernel/pallas_call | solution.py:356
  25.4 0.6 collective-permute-start.3
  26.0 5.3 %all-to-all-start = ((bf16[8,2,144,128]{3,2,1,0:T(8,128)(2,1)}), bf16[8,2,144,128]{3,2,1,0:T(8,128)(2,1)S(1)}, u32[]{:S(2)}, u32[]{:S(2)}) async-start(bf16[8,2,144,128]{3,2,1,0:T(8,128)(2,1)} %get-tuple-element.19), calls=%async_computation | async-start | bytes 1179648 | tf_op jit(solution)/shard_map/all_to_all | solution.py:405
  31.9 6.0 %collective-permute-done.3.refs_2_ = bf16[128,2048]{1,0:T(8,128)(2,1)S(1)} collective-permute-done((bf16[128,2048]{1,0:T(8,128)(2,1)}, bf16[128,2048]{1,0:T(8,128)(2,1)S(1)}, u32[]{:S(2)}, u32[]{:S(2)}) %collective-permute-start.3) | collective-permute-done | bytes 524320 | tf_op jit(solution)/shard_map/ppermute | solution.py:304
  37.9 1.0 %collective-permute-start.4 = (bf16[128,2048]{1,0:T(8,128)(2,1)S(1)}, bf16[128,2048]{1,0:T(8,128)(2,1)}, u32[]{:S(2)}, u32[]{:S(2)}) collective-permute-start(bf16[128,2048]{1,0:T(8,128)(2,1)S(1)} %collective-permute-done.3.refs_2_), channel_id=1, source_target_pairs={{0,4},{4,0},{8,12},{12,8},{16,20},{20,16},{24,28},{28,24},{1,5},{5... | collective-permute-start | bytes 1572872 | tf_op jit(solution)/shard_map/ppermute | solution.py:304
  38.9 0.5 collective-permute-start.8
  39.5 5.3 %collective-permute-done.8.refs_2_ = bf16[384,256]{1,0:T(8,128)(2,1)S(1)} collective-permute-done((bf16[384,256]{1,0:T(8,128)(2,1)}, bf16[384,256]{1,0:T(8,128)(2,1)S(1)}, u32[]{:S(2)}, u32[]{:S(2)}) %collective-permute-start.8) | collective-permute-done | bytes 196640 | tf_op jit(solution)/shard_map/ppermute | solution.py:304
  44.8 0.7 copy-done.5
  45.5 6.5 %collective-permute-done.9.refs_3_ = bf16[384,256]{1,0:T(8,128)(2,1)S(1)} collective-permute-done((bf16[384,256]{1,0:T(8,128)(2,1)}, bf16[384,256]{1,0:T(8,128)(2,1)S(1)}, u32[]{:S(2)}, u32[]{:S(2)}) %collective-permute-start.9) | collective-permute-done | bytes 196640 | tf_op jit(solution)/shard_map/ppermute | solution.py:304
  52.0 0.7 copy-done.7
  53.2 10.9 %local_kernel.1.parts_ref = bf16[1536,768]{1,0:T(8,128)(2,1)} custom-call(bf16[1536,2048]{1,0:T(8,128)(2,1)} %x_ref.3, f32[16,128]{1,0:T(8,128)} %bitcast.6, bf16[2048,256]{1,0:T(8,128)(2,1)} %qw_ref.1, bf16[2048,256]{1,0:T(8,128)(2,1)} %ow_ref.1, f32[1,256]{1,0:T(1,128)} %bitcast.7, f32[1536,128]{1,0:T(8,128)} %get-tuple-element.20.scale_ref, ...), custom_call_target="tpu_custom_call" | custom-call | flops 3221225472 | bytes 6291456 | tf_op jit(solution)/shard_map/local_kernel/pallas_call | solution.py:407
  64.1 1.7 %copy-done = bf16[1536,768]{1,0:T(8,128)(2,1)S(1)} copy-done((bf16[1536,768]{1,0:T(8,128)(2,1)S(1)}, bf16[1536,768]{1,0:T(8,128)(2,1)}, u32[]{:S(2)}) %copy-start) | copy-done | bytes 2359320
  65.7 1.1 %output_kernel.3 = (bf16[384,256]{1,0:T(8,128)(2,1)S(1)}, bf16[384,256]{1,0:T(8,128)(2,1)S(1)}) custom-call(bf16[8,2,144,128]{3,2,1,0:T(8,128)(2,1)S(1)} %all-to-all-done.msgs_ref, f32[2,128,128]{2,1,0:T(8,128)S(1)} %copy-done.3, bf16[1536,768]{1,0:T(8,128)(2,1)S(1)} %copy-done), custom_call_target="tpu_custom_call" | custom-call | flops 100663296 | bytes 1572864 | tf_op jit(solution)/shard_map/output_kernel/pallas_call | solution.py:432
  66.9 1.1 %output_kernel.2 = (bf16[384,256]{1,0:T(8,128)(2,1)S(1)}, bf16[384,256]{1,0:T(8,128)(2,1)S(1)}) custom-call(bf16[8,2,144,128]{3,2,1,0:T(8,128)(2,1)S(1)} %all-to-all-done.msgs_ref, f32[2,128,128]{2,1,0:T(8,128)S(1)} %copy-done.3, bf16[1536,768]{1,0:T(8,128)(2,1)S(1)} %copy-done), custom_call_target="tpu_custom_call" | custom-call | flops 100663296 | bytes 1572864 | tf_op jit(solution)/shard_map/output_kernel/pallas_call | solution.py:432
  68.0 1.6 %collective-permute-start.1 = (bf16[384,256]{1,0:T(8,128)(2,1)S(1)}, bf16[384,256]{1,0:T(8,128)(2,1)S(1)}, u32[]{:S(2)}, u32[]{:S(2)}) collective-permute-start(bf16[384,256]{1,0:T(8,128)(2,1)S(1)} %get-tuple-element.24), channel_id=1, source_target_pairs={{0,2},{1,3},{2,0},{3,1},{4,6},{5,7},{6,4},{7,5},{8,10},{9,11},{10,... | collective-permute-start | bytes 589832 | tf_op jit(solution)/shard_map/ppermute | solution.py:304
  69.9 4.5 %project_kernel.2.refs_6_ = bf16[384,2048]{1,0:T(8,128)(2,1)S(1)} custom-call(bf16[384,256]{1,0:T(8,128)(2,1)S(1)} %copy-done.4, bf16[384,256]{1,0:T(8,128)(2,1)S(1)} %collective-permute-done.7.refs_1_, bf16[384,256]{1,0:T(8,128)(2,1)S(1)} %copy-done.6, bf16[384,256]{1,0:T(8,128)(2,1)S(1)} %copy-done.8, bf16[384,256]{1,0:T(8,128)(2,1)S(1)} %get-tuple-element.31.refs_4_, ...), custom_call_target="tpu_custom_call" | custom-call | flops 2415919104 | bytes 7864320 | tf_op jit(solution)/shard_map/project_kernel/pallas_call | solution.py:319
  74.4 1.4 %collective-permute-done.1.refs_0_ = bf16[384,256]{1,0:T(8,128)(2,1)S(1)} collective-permute-done((bf16[384,256]{1,0:T(8,128)(2,1)S(1)}, bf16[384,256]{1,0:T(8,128)(2,1)S(1)}, u32[]{:S(2)}, u32[]{:S(2)}) %collective-permute-start.1) | collective-permute-done | bytes 196640 | tf_op jit(solution)/shard_map/ppermute | solution.py:304
  75.9 3.2 %collective-permute-done.2.refs_1_ = bf16[384,256]{1,0:T(8,128)(2,1)S(1)} collective-permute-done((bf16[384,256]{1,0:T(8,128)(2,1)S(1)}, bf16[384,256]{1,0:T(8,128)(2,1)S(1)}, u32[]{:S(2)}, u32[]{:S(2)}) %collective-permute-start.2) | collective-permute-done | bytes 196640 | tf_op jit(solution)/shard_map/ppermute | solution.py:304
  79.1 3.2 %project_kernel.3 = bf16[384,2048]{1,0:T(8,128)(2,1)} custom-call(bf16[384,256]{1,0:T(8,128)(2,1)S(1)} %collective-permute-done.1.refs_0_, bf16[384,256]{1,0:T(8,128)(2,1)S(1)} %collective-permute-done.2.refs_1_, bf16[128,2048]{1,0:T(8,128)(2,1)S(1)} %collective-permute-done.3.refs_2_, bf16[128,2048]{1,0:T(8,128)(2,1)} %collective-permute-done.4.refs_3_, ...), custom_call_target="tpu_custom_call" | custom-call | flops 805306368 | bytes 3670016 | tf_op jit(solution)/shard_map/project_kernel/pallas_call | solution.py:319
  (35 shorter events, 1.6 us)
Async XLA Ops:
  0.0 31.8 %collective-permute-start.12 = (bf16[256,2048]{1,0:T(8,128)(2,1)}, bf16[256,2048]{1,0:T(8,128)(2,1)}, u32[]{:S(2)}, u32[]{:S(2)}) collective-permute-start(bf16[256,2048]{1,0:T(8,128)(2,1)} %refs_6_.1), channel_id=1, source_target_pairs={{0,2},{1,3},{2,0},{3,1},{4,6},{5,7},{6,4},{7,5},{8,10},{9,11},{10,... | collective-permute-start | bytes 3145736 | tf_op jit(solution)/shard_map/ppermute | solution.py:304
  2.3 7.0 %collective-permute-start = (bf16[16,2048]{1,0:T(8,128)(2,1)S(1)}, bf16[16,2048]{1,0:T(8,128)(2,1)S(1)}, u32[]{:S(2)}, u32[]{:S(2)}) collective-permute-start(bf16[16,2048]{1,0:T(8,128)(2,1)S(1)} %slice.3), channel_id=1, source_target_pairs={{0,4},{4,8},{8,12},{12,16},{16,20},{20,24},{24,28},{1,5},{5,9},{9,... | collective-permute-start | bytes 196616 | tf_op jit(solution)/shard_map/ppermute | solution.py:355
  10.0 16.0 %copy-start.2 = (bf16[256,2048]{1,0:T(8,128)(2,1)S(1)}, bf16[256,2048]{1,0:T(8,128)(2,1)}, u32[]{:S(2)}) copy-start(bf16[256,2048]{1,0:T(8,128)(2,1)} %refs_6_.1) | copy-start | bytes 3145732
  10.0 21.3 %copy-start.1 = (bf16[256,2048]{1,0:T(8,128)(2,1)S(1)}, bf16[256,2048]{1,0:T(8,128)(2,1)}, u32[]{:S(2)}) copy-start(bf16[256,2048]{1,0:T(8,128)(2,1)} %refs_10_.1) | copy-start | bytes 3145732
  25.4 12.5 %collective-permute-start.3 = (bf16[128,2048]{1,0:T(8,128)(2,1)}, bf16[128,2048]{1,0:T(8,128)(2,1)S(1)}, u32[]{:S(2)}, u32[]{:S(2)}) collective-permute-start(bf16[128,2048]{1,0:T(8,128)(2,1)} %get-tuple-element.26), channel_id=1, source_target_pairs={{0,2},{1,3},{2,0},{3,1},{4,6},{5,7},{6,4},{7,5},{8,10},{9,11},{10,... | collective-permute-start | bytes 1572872 | tf_op jit(solution)/shard_map/ppermute | solution.py:304
  26.0 40.8 %collective-permute-start.11 = (bf16[256,2048]{1,0:T(8,128)(2,1)S(1)}, bf16[256,2048]{1,0:T(8,128)(2,1)}, u32[]{:S(2)}, u32[]{:S(2)}) collective-permute-start(bf16[256,2048]{1,0:T(8,128)(2,1)S(1)} %copy-done.2), channel_id=1, source_target_pairs={{0,1},{1,0},{2,3},{3,2},{4,5},{5,4},{6,7},{7,6},{8,9},{9,8},{10,11... | collective-permute-start | bytes 3145736 | tf_op jit(solution)/shard_map/ppermute | solution.py:304
  26.0 38.0 %all-to-all-start = ((bf16[8,2,144,128]{3,2,1,0:T(8,128)(2,1)}), bf16[8,2,144,128]{3,2,1,0:T(8,128)(2,1)S(1)}, u32[]{:S(2)}, u32[]{:S(2)}) async-start(bf16[8,2,144,128]{3,2,1,0:T(8,128)(2,1)} %get-tuple-element.19), calls=%async_computation | async-start | bytes 1179648 | tf_op jit(solution)/shard_map/all_to_all | solution.py:405
  31.3 7.7 %collective-permute-start.7 = (bf16[384,256]{1,0:T(8,128)(2,1)}, bf16[384,256]{1,0:T(8,128)(2,1)S(1)}, u32[]{:S(2)}, u32[]{:S(2)}) collective-permute-start(bf16[384,256]{1,0:T(8,128)(2,1)} %get-tuple-element.28), channel_id=1, source_target_pairs={{0,1},{1,0},{2,3},{3,2},{4,5},{5,4},{6,7},{7,6},{8,9},{9,8},{10,11... | collective-permute-start | bytes 589832 | tf_op jit(solution)/shard_map/ppermute | solution.py:304
  31.3 36.7 %collective-permute-start.14 = (bf16[256,2048]{1,0:T(8,128)(2,1)S(1)}, bf16[256,2048]{1,0:T(8,128)(2,1)}, u32[]{:S(2)}, u32[]{:S(2)}) collective-permute-start(bf16[256,2048]{1,0:T(8,128)(2,1)S(1)} %copy-done.1), channel_id=1, source_target_pairs={{0,1},{1,0},{2,3},{3,2},{4,5},{5,4},{6,7},{7,6},{8,9},{9,8},{10,11... | collective-permute-start | bytes 3145736 | tf_op jit(solution)/shard_map/ppermute | solution.py:304
  31.8 38.1 %collective-permute-start.13 = (bf16[256,2048]{1,0:T(8,128)(2,1)}, bf16[256,2048]{1,0:T(8,128)(2,1)}, u32[]{:S(2)}, u32[]{:S(2)}) collective-permute-start(bf16[256,2048]{1,0:T(8,128)(2,1)} %collective-permute-done.12.refs_8_), channel_id=1, source_target_pairs={{0,1},{1,0},{2,3},{3,2},{4,5},{5,4},{6,7},{7,6},{8,9},{9,8},{10,11... | collective-permute-start | bytes 3145736 | tf_op jit(solution)/shard_map/ppermute | solution.py:304
  37.9 14.8 %collective-permute-start.4 = (bf16[128,2048]{1,0:T(8,128)(2,1)S(1)}, bf16[128,2048]{1,0:T(8,128)(2,1)}, u32[]{:S(2)}, u32[]{:S(2)}) collective-permute-start(bf16[128,2048]{1,0:T(8,128)(2,1)S(1)} %collective-permute-done.3.refs_2_), channel_id=1, source_target_pairs={{0,4},{4,0},{8,12},{12,8},{16,20},{20,16},{24,28},{28,24},{1,5},{5... | collective-permute-start | bytes 1572872 | tf_op jit(solution)/shard_map/ppermute | solution.py:304
  38.9 5.9 %collective-permute-start.8 = (bf16[384,256]{1,0:T(8,128)(2,1)}, bf16[384,256]{1,0:T(8,128)(2,1)S(1)}, u32[]{:S(2)}, u32[]{:S(2)}) collective-permute-start(bf16[384,256]{1,0:T(8,128)(2,1)} %get-tuple-element.29), channel_id=1, source_target_pairs={{0,2},{1,3},{2,0},{3,1},{4,6},{5,7},{6,4},{7,5},{8,10},{9,11},{10,... | collective-permute-start | bytes 589832 | tf_op jit(solution)/shard_map/ppermute | solution.py:304
  44.8 0.7 copy-start.5
  45.5 6.5 %collective-permute-start.9 = (bf16[384,256]{1,0:T(8,128)(2,1)}, bf16[384,256]{1,0:T(8,128)(2,1)S(1)}, u32[]{:S(2)}, u32[]{:S(2)}) collective-permute-start(bf16[384,256]{1,0:T(8,128)(2,1)} %get-tuple-element.30), channel_id=1, source_target_pairs={{0,3},{1,2},{2,1},{3,0},{4,7},{5,6},{6,5},{7,4},{8,11},{9,10},{10,... | collective-permute-start | bytes 589832 | tf_op jit(solution)/shard_map/ppermute | solution.py:304
  52.7 21.8 %collective-permute-start.5 = (bf16[128,2048]{1,0:T(8,128)(2,1)S(1)}, bf16[128,2048]{1,0:T(8,128)(2,1)}, u32[]{:S(2)}, u32[]{:S(2)}) collective-permute-start(bf16[128,2048]{1,0:T(8,128)(2,1)S(1)} %collective-permute-done.3.refs_2_), channel_id=1, source_target_pairs={{0,1},{1,0},{2,3},{3,2},{4,5},{5,4},{6,7},{7,6},{8,9},{9,8},{10,11... | collective-permute-start | bytes 1572872 | tf_op jit(solution)/shard_map/ppermute | solution.py:304
  52.7 26.4 %collective-permute-start.6 = (bf16[128,2048]{1,0:T(8,128)(2,1)}, bf16[128,2048]{1,0:T(8,128)(2,1)}, u32[]{:S(2)}, u32[]{:S(2)}) collective-permute-start(bf16[128,2048]{1,0:T(8,128)(2,1)} %collective-permute-done.4.refs_3_), channel_id=1, source_target_pairs={{0,1},{1,0},{2,3},{3,2},{4,5},{5,4},{6,7},{7,6},{8,9},{9,8},{10,11... | collective-permute-start | bytes 1572872 | tf_op jit(solution)/shard_map/ppermute | solution.py:304
  53.2 10.9 %copy-start.3 = (f32[2,128,128]{2,1,0:T(8,128)S(1)}, f32[2,128,128]{2,1,0:T(8,128)}, u32[]{:S(2)}) copy-start(f32[2,128,128]{2,1,0:T(8,128)} %init_ref.3) | copy-start | bytes 393220
  64.1 1.7 %copy-start = (bf16[1536,768]{1,0:T(8,128)(2,1)S(1)}, bf16[1536,768]{1,0:T(8,128)(2,1)}, u32[]{:S(2)}) copy-start(bf16[1536,768]{1,0:T(8,128)(2,1)} %local_kernel.1.parts_ref) | copy-start | bytes 7077892
  65.7 4.2 %copy-start.4 = (bf16[384,256]{1,0:T(8,128)(2,1)S(1)}, bf16[384,256]{1,0:T(8,128)(2,1)}, u32[]{:S(2)}) copy-start(bf16[384,256]{1,0:T(8,128)(2,1)} %get-tuple-element.27.refs_0_) | copy-start | bytes 589828
  65.7 4.2 %copy-start.6 = (bf16[384,256]{1,0:T(8,128)(2,1)S(1)}, bf16[384,256]{1,0:T(8,128)(2,1)}, u32[]{:S(2)}) copy-start(bf16[384,256]{1,0:T(8,128)(2,1)} %copy-done.5) | copy-start | bytes 589828
  65.7 4.2 %copy-start.8 = (bf16[384,256]{1,0:T(8,128)(2,1)S(1)}, bf16[384,256]{1,0:T(8,128)(2,1)}, u32[]{:S(2)}) copy-start(bf16[384,256]{1,0:T(8,128)(2,1)} %copy-done.7) | copy-start | bytes 589828
  66.8 2.7 %collective-permute-start.10 = (bf16[384,256]{1,0:T(8,128)(2,1)S(1)}, bf16[384,256]{1,0:T(8,128)(2,1)S(1)}, u32[]{:S(2)}, u32[]{:S(2)}) collective-permute-start(bf16[384,256]{1,0:T(8,128)(2,1)S(1)} %get-tuple-element.32), channel_id=1, source_target_pairs={{0,1},{1,0},{2,3},{3,2},{4,5},{5,4},{6,7},{7,6},{8,9},{9,8},{10,11... | collective-permute-start | bytes 589832 | tf_op jit(solution)/shard_map/ppermute | solution.py:304
  68.0 7.8 %collective-permute-start.1 = (bf16[384,256]{1,0:T(8,128)(2,1)S(1)}, bf16[384,256]{1,0:T(8,128)(2,1)S(1)}, u32[]{:S(2)}, u32[]{:S(2)}) collective-permute-start(bf16[384,256]{1,0:T(8,128)(2,1)S(1)} %get-tuple-element.24), channel_id=1, source_target_pairs={{0,2},{1,3},{2,0},{3,1},{4,6},{5,7},{6,4},{7,5},{8,10},{9,11},{10,... | collective-permute-start | bytes 589832 | tf_op jit(solution)/shard_map/ppermute | solution.py:304
  69.6 9.5 %collective-permute-start.2 = (bf16[384,256]{1,0:T(8,128)(2,1)S(1)}, bf16[384,256]{1,0:T(8,128)(2,1)S(1)}, u32[]{:S(2)}, u32[]{:S(2)}) collective-permute-start(bf16[384,256]{1,0:T(8,128)(2,1)S(1)} %get-tuple-element.25), channel_id=1, source_target_pairs={{0,3},{1,2},{2,1},{3,0},{4,7},{5,6},{6,5},{7,4},{8,11},{9,10},{10,... | collective-permute-start | bytes 589832 | tf_op jit(solution)/shard_map/ppermute | solution.py:304
  (2 other events, 1.3 us)

commit v4 on v3

--- a/solution.py
+++ b/solution.py
@@ -69,7 +69,7 @@
 
 def state_kernel(
     x_ref, halo_ref, gain_ref, fw_ref, vw_ref, pw_ref, mix_ref, pool_scale_ref, lb_ref,
-    extra_ref, weight_ref, scale_ref, kept_ref, start_ref, rows_ref, msg_ref, half_ref, *rest,
+    extra_ref, scale_ref, kept_ref, start_ref, rows_ref, msg_ref, *rest,
 ):
     ypool_refs, (folded, state, total, tail, band, stage) = rest[:-6], rest[-6:]
     step = pl.program_id(0)
@@ -83,7 +83,6 @@
     def _():
         state[...] = jnp.zeros_like(state)
         total[...] = jnp.zeros_like(total)
-        half_ref[...] = weight_ref[...]
         fold_gain(gain_ref, (fw_ref, vw_ref, pw_ref), folded)
         halo = halo_ref[...]
         tail[...] = (dot(halo, folded[:, 2 * channels :]) * row_scale(halo)).astype(bf16)
@@ -182,7 +181,7 @@
 
 def local_kernel(
     x_ref, gain_ref, qw_ref, ow_ref, recur_gain_ref, scale_ref, kept_ref, start_ref, rows_ref,
-    parts_ref, folded,
+    parts_ref, folded, diagonal,
 ):
     step = pl.program_id(0)
     tile = x_ref.shape[0]
@@ -193,8 +192,9 @@
     @pl.when(step == 0)
     def _():
         fold_gain(gain_ref, (qw_ref, ow_ref), folded)
-
-    causal = lower_triangle(chunk)
+        diagonal[...] = jnp.zeros_like(diagonal)
+
+    causal = jnp.concatenate([lower_triangle(chunk)] * heads, axis=1)
 
     def project_block(b):
         return dot(x_ref[b * 256 : (b + 1) * 256, :], folded[...])
@@ -221,15 +221,19 @@
             query_abs = query_dec * rows_ref[c, 0:1, :]
             parts_ref[span, channels : 2 * channels] = (query_abs * rows_ref[c, 1:2, :]).astype(bf16)
             query_abs = query_abs.astype(bf16)
+            keys, values, states = [diagonal.at[3 * (c % 2) + k] for k in range(3)]
             for h in range(heads):
                 lanes = slice(h * head_k, (h + 1) * head_k)
-                key = kept_ref[span, lanes]
-                value = kept_ref[span, 2 * channels + h * head_k : 2 * channels + (h + 1) * head_k]
-                scores = dot(query_low[:, lanes], key, ((1,), (1,)))
-                scores = jnp.where(causal, scores, 0.0).astype(bf16)
-                within = dot(scores, value)
-                earlier = dot(query_abs[:, lanes], start_ref[c, h], ((1,), (1,)))
-                parts_ref[span, lanes] = (within + earlier).astype(bf16)
+                keys[lanes, lanes] = kept_ref[span, lanes]
+                values[lanes, lanes] = kept_ref[
+                    span, 2 * channels + h * head_k : 2 * channels + (h + 1) * head_k
+                ]
+                states[lanes, lanes] = start_ref[c, h]
+            scores = dot(query_low, keys[...], ((1,), (1,)))
+            scores = jnp.where(causal, scores, 0.0).astype(bf16)
+            within = dot(scores, values[...])
+            earlier = dot(query_abs, states[...], ((1,), (1,)))
+            parts_ref[span, :channels] = (within + earlier).astype(bf16)
 
 
 def output_kernel(msgs_ref, init_ref, parts_ref, *rest):
@@ -353,7 +357,7 @@
         [swapped(far, "tp", 1)],
     ]
     halo = lax.ppermute(inputs[rows - halo_rows :], "sp", [(i, i + 1) for i in range(sp - 1)])
-    scale, kept, starts, row_info, msgs, half, *y_pool = pl.pallas_call(
+    scale, kept, starts, row_info, msgs, *y_pool = pl.pallas_call(
         state_kernel,
         grid=(steps,),
         in_specs=[
@@ -361,18 +365,17 @@
             fixed(width, channels), fixed(width, channels), fixed(width, channels),
             fixed(*pool_mix.shape), fixed(1, channels), fixed(1, channels),
             pl.BlockSpec((heads, tile), lambda i: (0, i)),
-            pl.BlockSpec((channels // 2, width), lambda i: (lax.axis_index("sp") % 2, 0)),
         ],
         out_specs=[
             moving(tile, lanes), moving(tile, 3 * channels),
             moving(chunks, heads, head_k, head_k), moving(chunks, 8, channels),
-            fixed(sp, heads, head_k + msg_pad, head_k), fixed(channels // 2, width),
+            fixed(sp, heads, head_k + msg_pad, head_k),
         ] + [fixed(quarter, channels)] * tp,
         out_shape=[
             sds((rows, lanes), f32), sds((rows, 3 * channels), bf16),
             sds((rows // chunk, heads, head_k, head_k), bf16),
             sds((rows // chunk, 8, channels), f32),
-            sds((sp, heads, head_k + msg_pad, head_k), bf16), sds((channels // 2, width), bf16),
+            sds((sp, heads, head_k + msg_pad, head_k), bf16),
         ] + [sds((quarter, channels), bf16)] * tp,
         scratch_shapes=[
             pltpu.VMEM((width, 3 * channels), bf16), pltpu.VMEM((heads, head_k, head_k), f32),
@@ -387,7 +390,10 @@
         name="state_kernel",
     )(
         inputs, halo, gain, forget_weight, value_weight, pool_weight, pool_mix, pool_scale[None],
-        lower_bound[None], extra_decay.T, out_recur,
+        lower_bound[None], extra_decay.T,
+    )
+    half = lax.dynamic_slice_in_dim(
+        out_recur, (lax.axis_index("sp") % 2) * (channels // 2), channels // 2, axis=0
     )
     fetched = swapped(half, "tp", 2)
     handed = swapped(fetched, "sp", 1)
@@ -415,7 +421,9 @@
         ],
         out_specs=moving(tile, 3 * channels),
         out_shape=sds((rows, 3 * channels), bf16),
-        scratch_shapes=[pltpu.VMEM((width, 2 * channels), bf16)],
+        scratch_shapes=[
+            pltpu.VMEM((width, 2 * channels), bf16), pltpu.VMEM((6, channels, channels), bf16),
+        ],
         compiler_params=limits(54),
         cost_estimate=pl.CostEstimate(
             flops=4 * rows * width * channels, transcendentals=0, bytes_accessed=2 * rows * width

time: 83.9 us -> 83.2 us (level)
  waiting for transfers between devices: 26.2 us -> 23.8 us
  local copies, waits for them, and re-layouts: 4.5 us -> 6.38 us
  Pallas kernels: 36.1 us -> 34.5 us
  starting transfers between devices: 15.4 us -> 16.8 us
    ppermute x1, waiting for transfers between devices: 3.62 us -> 1.41 us  [per_device(): lax.ppermute(inputs[rows - halo_rows:], 'sp', [(i, i + 1) for i in range(...]
    dynamic_slice x0 -> x1, local copies, waits for them, and re-layouts: none -> 1.9 us  [per_device(): lax.dynamic_slice_in_dim(out_recur, lax.axis_index('sp') % 2 * (channels...]
    ppermute x14, starting transfers between devices: 6.72 us -> 8.13 us  [swapped(): return lax.ppermute(array, axis, [(i, i ^ bit) for i in range(devices)])]
    pallas_call x1, Pallas kernels: 15.4 us -> 14.4 us  [per_device(): pl.pallas_call(state_kernel, grid=(steps,), in_specs=[moving(tile, width)...]
  transfers between devices with their start and end apart: 16 -> 16, of which waited for: 6 -> 6; matrix products, arithmetic and copies ran while one was open for 1% -> 3% of each run, Pallas kernels for 40% -> 38%
where the time goes in v4:
time: 83.2 us; the launch traced here: 81.6 us
  Pallas kernels  34.5 us (41%)
  waiting for transfers between devices  23.8 us (29%)
  starting transfers between devices  16.8 us (20%)
  local copies, waits for them, and re-layouts  6.38 us (8%)
    ppermute x14, waiting for transfers between devices, swapped(): return lax.ppermute(array, axis, [(i, i ^ bit) for i in range(devices)])  22.3 us
    pallas_call x1, Pallas kernels, per_device(): pl.pallas_call(state_kernel, grid=(steps,), in_specs=[moving(tile, width)...  14.4 us
    pallas_call x1, Pallas kernels, per_device(): pl.pallas_call(local_kernel, grid=(steps,), in_specs=[moving(tile, width)...  10.4 us
    ppermute x14, starting transfers between devices, swapped(): return lax.ppermute(array, axis, [(i, i ^ bit) for i in range(devices)])  8.13 us
    pallas_call x2, Pallas kernels, project(): pl.pallas_call(functools.partial(project_kernel, counts), grid=(width //...  7.53 us
    all_to_all x1, starting transfers between devices, per_device(): msgs = lax.all_to_all(msgs, 'sp', split_axis=0, concat_axis=0, tiled=True)  5.28 us
    unnamed x20, local copies, waits for them, and re-layouts  3.64 us
    ppermute x1, starting transfers between devices, per_device(): lax.ppermute(inputs[rows - halo_rows:], 'sp', [(i, i + 1) for i in range(...  3.42 us
  transfers between devices with their start and end apart: 16, of which 6 were waited for; matrix products, arithmetic and copies ran while one was open for 3% of the time, Pallas kernels for 38%

profile of v4, /device:TPU:16, one launch (start us, length us, event | category | flops | bytes accessed | tf_op | source)
XLA Modules:
  0.0 81.6 jit_solution(17817914083192332128)
XLA Ops:
  0.0 1.5 %collective-permute-start.12 = (bf16[256,2048]{1,0:T(8,128)(2,1)}, bf16[256,2048]{1,0:T(8,128)(2,1)S(1)}, u32[]{:S(2)}, u32[]{:S(2)}) collective-permute-start(bf16[256,2048]{1,0:T(8,128)(2,1)} %refs_6_.1), channel_id=1, source_target_pairs={{0,2},{1,3},{2,0},{3,1},{4,6},{5,7},{6,4},{7,5},{8,10},{9,11},{10,... | collective-permute-start | bytes 3145736 | tf_op jit(solution)/shard_map/ppermute | solution.py:308
  1.5 0.8 %slice.3 = bf16[16,2048]{1,0:T(8,128)(2,1)S(1)} slice(bf16[1536,2048]{1,0:T(8,128)(2,1)} %x_ref.3), slice={[1520:1536], [0:2048]} | slice | bytes 131072 | tf_op jit(solution)/shard_map/slice | solution.py:359
  2.3 3.4 %collective-permute-start = (bf16[16,2048]{1,0:T(8,128)(2,1)S(1)}, bf16[16,2048]{1,0:T(8,128)(2,1)S(1)}, u32[]{:S(2)}, u32[]{:S(2)}) collective-permute-start(bf16[16,2048]{1,0:T(8,128)(2,1)S(1)} %slice.3), channel_id=1, source_target_pairs={{0,4},{4,8},{8,12},{12,16},{16,20},{20,24},{24,28},{1,5},{5,9},{9,... | collective-permute-start | bytes 196616 | tf_op jit(solution)/shard_map/ppermute | solution.py:359
  5.8 1.9 %constant_dynamic-slice_fusion = bf16[128,2048]{1,0:T(8,128)(2,1)} fusion(bf16[256,2048]{1,0:T(8,128)(2,1)} %refs_10_.1, s32[]{:T(128)S(6)} %select_n.11), kind=kLoop, calls=%fused_computation | loop fusion | bytes 1048580 | tf_op jit(solution)/shard_map/dynamic_slice | solution.py:395
  8.2 1.4 %collective-permute-done.halo_ref = bf16[16,2048]{1,0:T(8,128)(2,1)S(1)} collective-permute-done((bf16[16,2048]{1,0:T(8,128)(2,1)S(1)}, bf16[16,2048]{1,0:T(8,128)(2,1)S(1)}, u32[]{:S(2)}, u32[]{:S(2)}) %collective-permute-start) | collective-permute-done | bytes 65568 | tf_op jit(solution)/shard_map/ppermute | solution.py:359
  9.6 0.6 copy-done.9
  10.2 14.4 %state_kernel.1 = (f32[1536,128]{1,0:T(8,128)}, bf16[1536,768]{1,0:T(8,128)(2,1)}, bf16[12,2,128,128]{3,2,1,0:T(8,128)(2,1)}, f32[12,8,256]{2,1,0:T(8,128)}, bf1...) custom-call(bf16[1536,2048]{1,0:T(8,128)(2,1)} %x_ref.3, ...), custom_call_target="tpu_custom_call" | custom-call | flops 4831838208 | bytes 6291456 | tf_op jit(solution)/shard_map/state_kernel/pallas_call | solution.py:360
  24.6 5.3 %all-to-all-start = ((bf16[8,2,144,128]{3,2,1,0:T(8,128)(2,1)}), bf16[8,2,144,128]{3,2,1,0:T(8,128)(2,1)S(1)}, u32[]{:S(2)}, u32[]{:S(2)}) async-start(bf16[8,2,144,128]{3,2,1,0:T(8,128)(2,1)} %get-tuple-element.18), calls=%async_computation | async-start | bytes 1179648 | tf_op jit(solution)/shard_map/all_to_all | solution.py:411
  30.5 5.8 %collective-permute-done.3.refs_2_ = bf16[128,2048]{1,0:T(8,128)(2,1)S(1)} collective-permute-done((bf16[128,2048]{1,0:T(8,128)(2,1)}, bf16[128,2048]{1,0:T(8,128)(2,1)S(1)}, u32[]{:S(2)}, u32[]{:S(2)}) %collective-permute-start.3) | collective-permute-done | bytes 524320 | tf_op jit(solution)/shard_map/ppermute | solution.py:308
  36.3 1.5 %collective-permute-start.4 = (bf16[128,2048]{1,0:T(8,128)(2,1)S(1)}, bf16[128,2048]{1,0:T(8,128)(2,1)}, u32[]{:S(2)}, u32[]{:S(2)}) collective-permute-start(bf16[128,2048]{1,0:T(8,128)(2,1)S(1)} %collective-permute-done.3.refs_2_), channel_id=1, source_target_pairs={{0,4},{4,0},{8,12},{12,8},{16,20},{20,16},{24,28},{28,24},{1,5},{5... | collective-permute-start | bytes 1572872 | tf_op jit(solution)/shard_map/ppermute | solution.py:308
  37.9 1.5 %collective-permute-start.8 = (bf16[384,256]{1,0:T(8,128)(2,1)}, bf16[384,256]{1,0:T(8,128)(2,1)S(1)}, u32[]{:S(2)}, u32[]{:S(2)}) collective-permute-start(bf16[384,256]{1,0:T(8,128)(2,1)} %get-tuple-element.27), channel_id=1, source_target_pairs={{0,2},{1,3},{2,0},{3,1},{4,6},{5,7},{6,4},{7,5},{8,10},{9,11},{10,... | collective-permute-start | bytes 589832 | tf_op jit(solution)/shard_map/ppermute | solution.py:308
  39.4 4.4 %collective-permute-done.8.refs_2_ = bf16[384,256]{1,0:T(8,128)(2,1)S(1)} collective-permute-done((bf16[384,256]{1,0:T(8,128)(2,1)}, bf16[384,256]{1,0:T(8,128)(2,1)S(1)}, u32[]{:S(2)}, u32[]{:S(2)}) %collective-permute-start.8) | collective-permute-done | bytes 196640 | tf_op jit(solution)/shard_map/ppermute | solution.py:308
  43.8 0.7 copy-done.5
  44.4 7.4 %collective-permute-done.9.refs_3_ = bf16[384,256]{1,0:T(8,128)(2,1)S(1)} collective-permute-done((bf16[384,256]{1,0:T(8,128)(2,1)}, bf16[384,256]{1,0:T(8,128)(2,1)S(1)}, u32[]{:S(2)}, u32[]{:S(2)}) %collective-permute-start.9) | collective-permute-done | bytes 196640 | tf_op jit(solution)/shard_map/ppermute | solution.py:308
  51.8 0.7 copy-done.7
  53.0 10.4 %local_kernel.1.parts_ref = bf16[1536,768]{1,0:T(8,128)(2,1)} custom-call(bf16[1536,2048]{1,0:T(8,128)(2,1)} %x_ref.3, f32[16,128]{1,0:T(8,128)} %bitcast.6, bf16[2048,256]{1,0:T(8,128)(2,1)} %qw_ref.1, bf16[2048,256]{1,0:T(8,128)(2,1)} %ow_ref.1, f32[1,256]{1,0:T(1,128)} %bitcast.7, f32[1536,128]{1,0:T(8,128)} %get-tuple-element.19.scale_ref, ...), custom_call_target="tpu_custom_call" | custom-call | flops 3221225472 | bytes 6291456 | tf_op jit(solution)/shard_map/local_kernel/pallas_call | solution.py:413
  63.4 1.7 %copy-done = bf16[1536,768]{1,0:T(8,128)(2,1)S(1)} copy-done((bf16[1536,768]{1,0:T(8,128)(2,1)S(1)}, bf16[1536,768]{1,0:T(8,128)(2,1)}, u32[]{:S(2)}) %copy-start) | copy-done | bytes 2359320
  65.1 1.1 %output_kernel.3 = (bf16[384,256]{1,0:T(8,128)(2,1)S(1)}, bf16[384,256]{1,0:T(8,128)(2,1)S(1)}) custom-call(bf16[8,2,144,128]{3,2,1,0:T(8,128)(2,1)S(1)} %all-to-all-done.msgs_ref, f32[2,128,128]{2,1,0:T(8,128)S(1)} %copy-done.3, bf16[1536,768]{1,0:T(8,128)(2,1)S(1)} %copy-done), custom_call_target="tpu_custom_call" | custom-call | flops 100663296 | bytes 1572864 | tf_op jit(solution)/shard_map/output_kernel/pallas_call | solution.py:440
  66.4 1.1 %output_kernel.2 = (bf16[384,256]{1,0:T(8,128)(2,1)S(1)}, bf16[384,256]{1,0:T(8,128)(2,1)S(1)}) custom-call(bf16[8,2,144,128]{3,2,1,0:T(8,128)(2,1)S(1)} %all-to-all-done.msgs_ref, f32[2,128,128]{2,1,0:T(8,128)S(1)} %copy-done.3, bf16[1536,768]{1,0:T(8,128)(2,1)S(1)} %copy-done), custom_call_target="tpu_custom_call" | custom-call | flops 100663296 | bytes 1572864 | tf_op jit(solution)/shard_map/output_kernel/pallas_call | solution.py:440
  68.1 1.2 %collective-permute-start.2 = (bf16[384,256]{1,0:T(8,128)(2,1)S(1)}, bf16[384,256]{1,0:T(8,128)(2,1)S(1)}, u32[]{:S(2)}, u32[]{:S(2)}) collective-permute-start(bf16[384,256]{1,0:T(8,128)(2,1)S(1)} %get-tuple-element.24), channel_id=1, source_target_pairs={{0,3},{1,2},{2,1},{3,0},{4,7},{5,6},{6,5},{7,4},{8,11},{9,10},{10,... | collective-permute-start | bytes 589832 | tf_op jit(solution)/shard_map/ppermute | solution.py:308
  69.3 4.3 %project_kernel.2.refs_6_ = bf16[384,2048]{1,0:T(8,128)(2,1)S(1)} custom-call(bf16[384,256]{1,0:T(8,128)(2,1)S(1)} %copy-done.4, bf16[384,256]{1,0:T(8,128)(2,1)S(1)} %collective-permute-done.7.refs_1_, bf16[384,256]{1,0:T(8,128)(2,1)S(1)} %copy-done.6, bf16[384,256]{1,0:T(8,128)(2,1)S(1)} %copy-done.8, bf16[384,256]{1,0:T(8,128)(2,1)S(1)} %get-tuple-element.29.refs_4_, ...), custom_call_target="tpu_custom_call" | custom-call | flops 2415919104 | bytes 7864320 | tf_op jit(solution)/shard_map/project_kernel/pallas_call | solution.py:323
  73.7 1.7 %collective-permute-done.1.refs_0_ = bf16[384,256]{1,0:T(8,128)(2,1)S(1)} collective-permute-done((bf16[384,256]{1,0:T(8,128)(2,1)S(1)}, bf16[384,256]{1,0:T(8,128)(2,1)S(1)}, u32[]{:S(2)}, u32[]{:S(2)}) %collective-permute-start.1) | collective-permute-done | bytes 196640 | tf_op jit(solution)/shard_map/ppermute | solution.py:308
  75.3 3.1 %collective-permute-done.2.refs_1_ = bf16[384,256]{1,0:T(8,128)(2,1)S(1)} collective-permute-done((bf16[384,256]{1,0:T(8,128)(2,1)S(1)}, bf16[384,256]{1,0:T(8,128)(2,1)S(1)}, u32[]{:S(2)}, u32[]{:S(2)}) %collective-permute-start.2) | collective-permute-done | bytes 196640 | tf_op jit(solution)/shard_map/ppermute | solution.py:308
  78.4 3.2 %project_kernel.3 = bf16[384,2048]{1,0:T(8,128)(2,1)} custom-call(bf16[384,256]{1,0:T(8,128)(2,1)S(1)} %collective-permute-done.1.refs_0_, bf16[384,256]{1,0:T(8,128)(2,1)S(1)} %collective-permute-done.2.refs_1_, bf16[128,2048]{1,0:T(8,128)(2,1)S(1)} %collective-permute-done.3.refs_2_, bf16[128,2048]{1,0:T(8,128)(2,1)} %collective-permute-done.4.refs_3_, ...), custom_call_target="tpu_custom_call" | custom-call | flops 805306368 | bytes 3670016 | tf_op jit(solution)/shard_map/project_kernel/pallas_call | solution.py:323
  (36 shorter events, 2.5 us)
Async XLA Ops:
  0.0 30.4 %collective-permute-start.12 = (bf16[256,2048]{1,0:T(8,128)(2,1)}, bf16[256,2048]{1,0:T(8,128)(2,1)S(1)}, u32[]{:S(2)}, u32[]{:S(2)}) collective-permute-start(bf16[256,2048]{1,0:T(8,128)(2,1)} %refs_6_.1), channel_id=1, source_target_pairs={{0,2},{1,3},{2,0},{3,1},{4,6},{5,7},{6,4},{7,5},{8,10},{9,11},{10,... | collective-permute-start | bytes 3145736 | tf_op jit(solution)/shard_map/ppermute | solution.py:308
  1.5 64.7 %collective-permute-start.11 = (bf16[256,2048]{1,0:T(8,128)(2,1)}, bf16[256,2048]{1,0:T(8,128)(2,1)}, u32[]{:S(2)}, u32[]{:S(2)}) collective-permute-start(bf16[256,2048]{1,0:T(8,128)(2,1)} %refs_6_.1), channel_id=1, source_target_pairs={{0,1},{1,0},{2,3},{3,2},{4,5},{5,4},{6,7},{7,6},{8,9},{9,8},{10,11... | collective-permute-start | bytes 3145736 | tf_op jit(solution)/shard_map/ppermute | solution.py:308
  2.3 7.3 %collective-permute-start = (bf16[16,2048]{1,0:T(8,128)(2,1)S(1)}, bf16[16,2048]{1,0:T(8,128)(2,1)S(1)}, u32[]{:S(2)}, u32[]{:S(2)}) collective-permute-start(bf16[16,2048]{1,0:T(8,128)(2,1)S(1)} %slice.3), channel_id=1, source_target_pairs={{0,4},{4,8},{8,12},{12,16},{16,20},{20,24},{24,28},{1,5},{5,9},{9,... | collective-permute-start | bytes 196616 | tf_op jit(solution)/shard_map/ppermute | solution.py:359
  7.7 28.7 %collective-permute-start.3 = (bf16[128,2048]{1,0:T(8,128)(2,1)}, bf16[128,2048]{1,0:T(8,128)(2,1)S(1)}, u32[]{:S(2)}, u32[]{:S(2)}) collective-permute-start(bf16[128,2048]{1,0:T(8,128)(2,1)} %constant_dynamic-slice_fusion), channel_id=1, source_target_pairs={{0,2},{1,3},{2,0},{3,1},{4,6},{5,7},{6,4},{7,5},{8,10},{9,11},{10,... | collective-permute-start | bytes 1572872 | tf_op jit(solution)/shard_map/ppermute | solution.py:308
  10.2 19.7 %copy-start.1 = (bf16[256,2048]{1,0:T(8,128)(2,1)S(1)}, bf16[256,2048]{1,0:T(8,128)(2,1)}, u32[]{:S(2)}) copy-start(bf16[256,2048]{1,0:T(8,128)(2,1)} %refs_10_.1) | copy-start | bytes 3145732
  24.6 38.8 %all-to-all-start = ((bf16[8,2,144,128]{3,2,1,0:T(8,128)(2,1)}), bf16[8,2,144,128]{3,2,1,0:T(8,128)(2,1)S(1)}, u32[]{:S(2)}, u32[]{:S(2)}) async-start(bf16[8,2,144,128]{3,2,1,0:T(8,128)(2,1)} %get-tuple-element.18), calls=%async_computation | async-start | bytes 1179648 | tf_op jit(solution)/shard_map/all_to_all | solution.py:411
  29.9 8.0 %collective-permute-start.7 = (bf16[384,256]{1,0:T(8,128)(2,1)}, bf16[384,256]{1,0:T(8,128)(2,1)S(1)}, u32[]{:S(2)}, u32[]{:S(2)}) collective-permute-start(bf16[384,256]{1,0:T(8,128)(2,1)} %get-tuple-element.26), channel_id=1, source_target_pairs={{0,1},{1,0},{2,3},{3,2},{4,5},{5,4},{6,7},{7,6},{8,9},{9,8},{10,11... | collective-permute-start | bytes 589832 | tf_op jit(solution)/shard_map/ppermute | solution.py:308
  29.9 37.5 %collective-permute-start.14 = (bf16[256,2048]{1,0:T(8,128)(2,1)S(1)}, bf16[256,2048]{1,0:T(8,128)(2,1)}, u32[]{:S(2)}, u32[]{:S(2)}) collective-permute-start(bf16[256,2048]{1,0:T(8,128)(2,1)S(1)} %copy-done.1), channel_id=1, source_target_pairs={{0,1},{1,0},{2,3},{3,2},{4,5},{5,4},{6,7},{7,6},{8,9},{9,8},{10,11... | collective-permute-start | bytes 3145736 | tf_op jit(solution)/shard_map/ppermute | solution.py:308
  30.4 38.9 %collective-permute-start.13 = (bf16[256,2048]{1,0:T(8,128)(2,1)S(1)}, bf16[256,2048]{1,0:T(8,128)(2,1)}, u32[]{:S(2)}, u32[]{:S(2)}) collective-permute-start(bf16[256,2048]{1,0:T(8,128)(2,1)S(1)} %collective-permute-done.12.refs_8_), channel_id=1, source_target_pairs={{0,1},{1,0},{2,3},{3,2},{4,5},{5,4},{6,7},{7,6},{8,9},{9,8},{10,11... | collective-permute-start | bytes 3145736 | tf_op jit(solution)/shard_map/ppermute | solution.py:308
  36.3 16.2 %collective-permute-start.4 = (bf16[128,2048]{1,0:T(8,128)(2,1)S(1)}, bf16[128,2048]{1,0:T(8,128)(2,1)}, u32[]{:S(2)}, u32[]{:S(2)}) collective-permute-start(bf16[128,2048]{1,0:T(8,128)(2,1)S(1)} %collective-permute-done.3.refs_2_), channel_id=1, source_target_pairs={{0,4},{4,0},{8,12},{12,8},{16,20},{20,16},{24,28},{28,24},{1,5},{5... | collective-permute-start | bytes 1572872 | tf_op jit(solution)/shard_map/ppermute | solution.py:308
  37.9 5.9 %collective-permute-start.8 = (bf16[384,256]{1,0:T(8,128)(2,1)}, bf16[384,256]{1,0:T(8,128)(2,1)S(1)}, u32[]{:S(2)}, u32[]{:S(2)}) collective-permute-start(bf16[384,256]{1,0:T(8,128)(2,1)} %get-tuple-element.27), channel_id=1, source_target_pairs={{0,2},{1,3},{2,0},{3,1},{4,6},{5,7},{6,4},{7,5},{8,10},{9,11},{10,... | collective-permute-start | bytes 589832 | tf_op jit(solution)/shard_map/ppermute | solution.py:308
  44.4 7.4 %collective-permute-start.9 = (bf16[384,256]{1,0:T(8,128)(2,1)}, bf16[384,256]{1,0:T(8,128)(2,1)S(1)}, u32[]{:S(2)}, u32[]{:S(2)}) collective-permute-start(bf16[384,256]{1,0:T(8,128)(2,1)} %get-tuple-element.28), channel_id=1, source_target_pairs={{0,3},{1,2},{2,1},{3,0},{4,7},{5,6},{6,5},{7,4},{8,11},{9,10},{10,... | collective-permute-start | bytes 589832 | tf_op jit(solution)/shard_map/ppermute | solution.py:308
  51.8 0.7 copy-start.7
  52.5 21.2 %collective-permute-start.5 = (bf16[128,2048]{1,0:T(8,128)(2,1)S(1)}, bf16[128,2048]{1,0:T(8,128)(2,1)}, u32[]{:S(2)}, u32[]{:S(2)}) collective-permute-start(bf16[128,2048]{1,0:T(8,128)(2,1)S(1)} %collective-permute-done.3.refs_2_), channel_id=1, source_target_pairs={{0,1},{1,0},{2,3},{3,2},{4,5},{5,4},{6,7},{7,6},{8,9},{9,8},{10,11... | collective-permute-start | bytes 1572872 | tf_op jit(solution)/shard_map/ppermute | solution.py:308
  52.6 25.8 %collective-permute-start.6 = (bf16[128,2048]{1,0:T(8,128)(2,1)}, bf16[128,2048]{1,0:T(8,128)(2,1)}, u32[]{:S(2)}, u32[]{:S(2)}) collective-permute-start(bf16[128,2048]{1,0:T(8,128)(2,1)} %collective-permute-done.4.refs_3_), channel_id=1, source_target_pairs={{0,1},{1,0},{2,3},{3,2},{4,5},{5,4},{6,7},{7,6},{8,9},{9,8},{10,11... | collective-permute-start | bytes 1572872 | tf_op jit(solution)/shard_map/ppermute | solution.py:308
  53.0 10.4 %copy-start.3 = (f32[2,128,128]{2,1,0:T(8,128)S(1)}, f32[2,128,128]{2,1,0:T(8,128)}, u32[]{:S(2)}) copy-start(f32[2,128,128]{2,1,0:T(8,128)} %init_ref.3) | copy-start | bytes 393220
  63.4 1.7 %copy-start = (bf16[1536,768]{1,0:T(8,128)(2,1)S(1)}, bf16[1536,768]{1,0:T(8,128)(2,1)}, u32[]{:S(2)}) copy-start(bf16[1536,768]{1,0:T(8,128)(2,1)} %local_kernel.1.parts_ref) | copy-start | bytes 7077892
  65.1 4.2 %copy-start.2 = (bf16[256,2048]{1,0:T(8,128)(2,1)S(1)}, bf16[256,2048]{1,0:T(8,128)(2,1)}, u32[]{:S(2)}) copy-start(bf16[256,2048]{1,0:T(8,128)(2,1)} %refs_6_.1) | copy-start | bytes 3145732
  65.1 4.2 %copy-start.4 = (bf16[384,256]{1,0:T(8,128)(2,1)S(1)}, bf16[384,256]{1,0:T(8,128)(2,1)}, u32[]{:S(2)}) copy-start(bf16[384,256]{1,0:T(8,128)(2,1)} %get-tuple-element.25.refs_0_) | copy-start | bytes 589828
  65.1 4.2 %copy-start.6 = (bf16[384,256]{1,0:T(8,128)(2,1)S(1)}, bf16[384,256]{1,0:T(8,128)(2,1)}, u32[]{:S(2)}) copy-start(bf16[384,256]{1,0:T(8,128)(2,1)} %copy-done.5) | copy-start | bytes 589828
  65.1 4.2 %copy-start.8 = (bf16[384,256]{1,0:T(8,128)(2,1)S(1)}, bf16[384,256]{1,0:T(8,128)(2,1)}, u32[]{:S(2)}) copy-start(bf16[384,256]{1,0:T(8,128)(2,1)} %copy-done.7) | copy-start | bytes 589828
  66.2 1.9 %collective-permute-start.10 = (bf16[384,256]{1,0:T(8,128)(2,1)S(1)}, bf16[384,256]{1,0:T(8,128)(2,1)S(1)}, u32[]{:S(2)}, u32[]{:S(2)}) collective-permute-start(bf16[384,256]{1,0:T(8,128)(2,1)S(1)} %get-tuple-element.30), channel_id=1, source_target_pairs={{0,1},{1,0},{2,3},{3,2},{4,5},{5,4},{6,7},{7,6},{8,9},{9,8},{10,11... | collective-permute-start | bytes 589832 | tf_op jit(solution)/shard_map/ppermute | solution.py:308
  67.5 7.8 %collective-permute-start.1 = (bf16[384,256]{1,0:T(8,128)(2,1)S(1)}, bf16[384,256]{1,0:T(8,128)(2,1)S(1)}, u32[]{:S(2)}, u32[]{:S(2)}) collective-permute-start(bf16[384,256]{1,0:T(8,128)(2,1)S(1)} %get-tuple-element.23), channel_id=1, source_target_pairs={{0,2},{1,3},{2,0},{3,1},{4,6},{5,7},{6,4},{7,5},{8,10},{9,11},{10,... | collective-permute-start | bytes 589832 | tf_op jit(solution)/shard_map/ppermute | solution.py:308
  68.1 10.3 %collective-permute-start.2 = (bf16[384,256]{1,0:T(8,128)(2,1)S(1)}, bf16[384,256]{1,0:T(8,128)(2,1)S(1)}, u32[]{:S(2)}, u32[]{:S(2)}) collective-permute-start(bf16[384,256]{1,0:T(8,128)(2,1)S(1)} %get-tuple-element.24), channel_id=1, source_target_pairs={{0,3},{1,2},{2,1},{3,0},{4,7},{5,6},{6,5},{7,4},{8,11},{9,10},{10,... | collective-permute-start | bytes 589832 | tf_op jit(solution)/shard_map/ppermute | solution.py:308
  (2 other events, 1.3 us)

commit v5 on v4

--- a/solution.py
+++ b/solution.py
@@ -163,20 +163,17 @@
     @pl.when(step == pl.num_programs(0) - 1)
     def _():
         decay_high, decay_low = split(jnp.exp(total[...]))
-        for h in range(heads):
-            lanes = slice(h * head_k, (h + 1) * head_k)
-            ending = state[h].astype(bf16)
-            decays = jnp.concatenate(
-                [
-                    decay_high[:, lanes].astype(f32),
-                    decay_low[:, lanes].astype(f32),
-                    jnp.zeros((msg_pad - 2, head_k), f32),
-                ],
-                axis=0,
-            ).astype(bf16)
-            for i in range(msg_ref.shape[0]):
-                msg_ref[i, h, :head_k, :] = ending
-                msg_ref[i, h, head_k:, :] = decays
+        decays = [
+            part[:, h * head_k : (h + 1) * head_k].astype(f32)
+            for h in range(heads) for part in (decay_high, decay_low)
+        ]
+        decays.append(jnp.zeros((msg_pad - 2 * heads, head_k), f32))
+        decays = jnp.concatenate(decays, axis=0).astype(bf16)
+        endings = [state[h].astype(bf16) for h in range(heads)]
+        for i in range(msg_ref.shape[0]):
+            for h in range(heads):
+                msg_ref[i, h * head_k : (h + 1) * head_k, :] = endings[h]
+            msg_ref[i, heads * head_k :, :] = decays
 
 
 def local_kernel(
@@ -246,11 +243,12 @@
     def _():
         for h in range(heads):
             def step(i, state):
+                at = heads * head_k + 2 * h
                 decay = (
-                    msgs_ref[i, h, head_k : head_k + 1, :].astype(f32)
-                    + msgs_ref[i, h, head_k + 1 : head_k + 2, :].astype(f32)
+                    msgs_ref[i, at : at + 1, :].astype(f32)
+                    + msgs_ref[i, at + 1 : at + 2, :].astype(f32)
                 )
-                return state * decay + msgs_ref[i, h, :head_k, :].astype(f32)
+                return state * decay + msgs_ref[i, h * head_k : (h + 1) * head_k, :].astype(f32)
 
             carried[h] = lax.fori_loop(0, lax.axis_index("sp"), step, init_ref[h].T).astype(bf16)
 
@@ -369,13 +367,13 @@
         out_specs=[
             moving(tile, lanes), moving(tile, 3 * channels),
             moving(chunks, heads, head_k, head_k), moving(chunks, 8, channels),
-            fixed(sp, heads, head_k + msg_pad, head_k),
+            fixed(sp, heads * head_k + msg_pad, head_k),
         ] + [fixed(quarter, channels)] * tp,
         out_shape=[
             sds((rows, lanes), f32), sds((rows, 3 * channels), bf16),
             sds((rows // chunk, heads, head_k, head_k), bf16),
             sds((rows // chunk, 8, channels), f32),
-            sds((sp, heads, head_k + msg_pad, head_k), bf16),
+            sds((sp, heads * head_k + msg_pad, head_k), bf16),
         ] + [sds((quarter, channels), bf16)] * tp,
         scratch_shapes=[
             pltpu.VMEM((width, 3 * channels), bf16), pltpu.VMEM((heads, head_k, head_k), f32),

time: 83.2 us -> 83.2 us (level)
  no operation moved by 1% of the time
where the time goes in v5:
time: 83.2 us; the launch traced here: 81.6 us
  Pallas kernels  34.5 us (41%)
  waiting for transfers between devices  23.8 us (29%)
  starting transfers between devices  16.8 us (20%)
  local copies, waits for them, and re-layouts  6.38 us (8%)
    ppermute x14, waiting for transfers between devices, swapped(): return lax.ppermute(array, axis, [(i, i ^ bit) for i in range(devices)])  22.3 us
    pallas_call x1, Pallas kernels, per_device(): pl.pallas_call(state_kernel, grid=(steps,), in_specs=[moving(tile, width)...  14.4 us
    pallas_call x1, Pallas kernels, per_device(): pl.pallas_call(local_kernel, grid=(steps,), in_specs=[moving(tile, width)...  10.4 us
    ppermute x14, starting transfers between devices, swapped(): return lax.ppermute(array, axis, [(i, i ^ bit) for i in range(devices)])  8.13 us
    pallas_call x2, Pallas kernels, project(): pl.pallas_call(functools.partial(project_kernel, counts), grid=(width //...  7.53 us
    all_to_all x1, starting transfers between devices, per_device(): msgs = lax.all_to_all(msgs, 'sp', split_axis=0, concat_axis=0, tiled=True)  5.28 us
    unnamed x20, local copies, waits for them, and re-layouts  3.64 us
    ppermute x1, starting transfers between devices, per_device(): lax.ppermute(inputs[rows - halo_rows:], 'sp', [(i, i + 1) for i in range(...  3.42 us
  transfers between devices with their start and end apart: 16, of which 6 were waited for; matrix products, arithmetic and copies ran while one was open for 3% of the time, Pallas kernels for 38%

profile of v5, /device:TPU:16, one launch (start us, length us, event | category | flops | bytes accessed | tf_op | source)
XLA Modules:
  0.0 81.6 jit_solution(9364387663612624777)
XLA Ops:
  0.0 1.5 %collective-permute-start.12 = (bf16[256,2048]{1,0:T(8,128)(2,1)}, bf16[256,2048]{1,0:T(8,128)(2,1)S(1)}, u32[]{:S(2)}, u32[]{:S(2)}) collective-permute-start(bf16[256,2048]{1,0:T(8,128)(2,1)} %refs_6_.1), channel_id=1, source_target_pairs={{0,2},{1,3},{2,0},{3,1},{4,6},{5,7},{6,4},{7,5},{8,10},{9,11},{10,... | collective-permute-start | bytes 3145736 | tf_op jit(solution)/shard_map/ppermute | solution.py:306
  1.5 0.8 %slice.3 = bf16[16,2048]{1,0:T(8,128)(2,1)S(1)} slice(bf16[1536,2048]{1,0:T(8,128)(2,1)} %x_ref.3), slice={[1520:1536], [0:2048]} | slice | bytes 131072 | tf_op jit(solution)/shard_map/slice | solution.py:357
  2.3 3.4 %collective-permute-start = (bf16[16,2048]{1,0:T(8,128)(2,1)S(1)}, bf16[16,2048]{1,0:T(8,128)(2,1)S(1)}, u32[]{:S(2)}, u32[]{:S(2)}) collective-permute-start(bf16[16,2048]{1,0:T(8,128)(2,1)S(1)} %slice.3), channel_id=1, source_target_pairs={{0,4},{4,8},{8,12},{12,16},{16,20},{20,24},{24,28},{1,5},{5,9},{9,... | collective-permute-start | bytes 196616 | tf_op jit(solution)/shard_map/ppermute | solution.py:357
  5.8 1.9 %constant_dynamic-slice_fusion = bf16[128,2048]{1,0:T(8,128)(2,1)} fusion(bf16[256,2048]{1,0:T(8,128)(2,1)} %refs_10_.1, s32[]{:T(128)S(6)} %select_n.11), kind=kLoop, calls=%fused_computation | loop fusion | bytes 1048580 | tf_op jit(solution)/shard_map/dynamic_slice | solution.py:393
  8.2 1.4 %collective-permute-done.halo_ref = bf16[16,2048]{1,0:T(8,128)(2,1)S(1)} collective-permute-done((bf16[16,2048]{1,0:T(8,128)(2,1)S(1)}, bf16[16,2048]{1,0:T(8,128)(2,1)S(1)}, u32[]{:S(2)}, u32[]{:S(2)}) %collective-permute-start) | collective-permute-done | bytes 65568 | tf_op jit(solution)/shard_map/ppermute | solution.py:357
  9.6 0.6 copy-done.9
  10.2 14.4 %state_kernel.1 = (f32[1536,128]{1,0:T(8,128)}, bf16[1536,768]{1,0:T(8,128)(2,1)}, bf16[12,2,128,128]{3,2,1,0:T(8,128)(2,1)}, f32[12,8,256]{2,1,0:T(8,128)}, bf1...) custom-call(bf16[1536,2048]{1,0:T(8,128)(2,1)} %x_ref.3, ...), custom_call_target="tpu_custom_call" | custom-call | flops 4831838208 | bytes 6291456 | tf_op jit(solution)/shard_map/state_kernel/pallas_call | solution.py:358
  24.6 5.3 %all-to-all-start = ((bf16[8,272,128]{2,1,0:T(8,128)(2,1)}), bf16[8,272,128]{2,1,0:T(8,128)(2,1)S(1)}, u32[]{:S(2)}, u32[]{:S(2)}) async-start(bf16[8,272,128]{2,1,0:T(8,128)(2,1)} %get-tuple-element.18), calls=%async_computation | async-start | bytes 1114112 | tf_op jit(solution)/shard_map/all_to_all | solution.py:409
  30.5 5.9 %collective-permute-done.3.refs_2_ = bf16[128,2048]{1,0:T(8,128)(2,1)S(1)} collective-permute-done((bf16[128,2048]{1,0:T(8,128)(2,1)}, bf16[128,2048]{1,0:T(8,128)(2,1)S(1)}, u32[]{:S(2)}, u32[]{:S(2)}) %collective-permute-start.3) | collective-permute-done | bytes 524320 | tf_op jit(solution)/shard_map/ppermute | solution.py:306
  36.3 1.5 %collective-permute-start.4 = (bf16[128,2048]{1,0:T(8,128)(2,1)S(1)}, bf16[128,2048]{1,0:T(8,128)(2,1)}, u32[]{:S(2)}, u32[]{:S(2)}) collective-permute-start(bf16[128,2048]{1,0:T(8,128)(2,1)S(1)} %collective-permute-done.3.refs_2_), channel_id=1, source_target_pairs={{0,4},{4,0},{8,12},{12,8},{16,20},{20,16},{24,28},{28,24},{1,5},{5... | collective-permute-start | bytes 1572872 | tf_op jit(solution)/shard_map/ppermute | solution.py:306
  37.9 1.5 %collective-permute-start.8 = (bf16[384,256]{1,0:T(8,128)(2,1)}, bf16[384,256]{1,0:T(8,128)(2,1)S(1)}, u32[]{:S(2)}, u32[]{:S(2)}) collective-permute-start(bf16[384,256]{1,0:T(8,128)(2,1)} %get-tuple-element.27), channel_id=1, source_target_pairs={{0,2},{1,3},{2,0},{3,1},{4,6},{5,7},{6,4},{7,5},{8,10},{9,11},{10,... | collective-permute-start | bytes 589832 | tf_op jit(solution)/shard_map/ppermute | solution.py:306
  39.4 4.4 %collective-permute-done.8.refs_2_ = bf16[384,256]{1,0:T(8,128)(2,1)S(1)} collective-permute-done((bf16[384,256]{1,0:T(8,128)(2,1)}, bf16[384,256]{1,0:T(8,128)(2,1)S(1)}, u32[]{:S(2)}, u32[]{:S(2)}) %collective-permute-start.8) | collective-permute-done | bytes 196640 | tf_op jit(solution)/shard_map/ppermute | solution.py:306
  43.8 0.7 copy-done.5
  44.4 7.4 %collective-permute-done.9.refs_3_ = bf16[384,256]{1,0:T(8,128)(2,1)S(1)} collective-permute-done((bf16[384,256]{1,0:T(8,128)(2,1)}, bf16[384,256]{1,0:T(8,128)(2,1)S(1)}, u32[]{:S(2)}, u32[]{:S(2)}) %collective-permute-start.9) | collective-permute-done | bytes 196640 | tf_op jit(solution)/shard_map/ppermute | solution.py:306
  51.8 0.7 copy-done.7
  53.0 10.4 %local_kernel.1.parts_ref = bf16[1536,768]{1,0:T(8,128)(2,1)} custom-call(bf16[1536,2048]{1,0:T(8,128)(2,1)} %x_ref.3, f32[16,128]{1,0:T(8,128)} %bitcast.6, bf16[2048,256]{1,0:T(8,128)(2,1)} %qw_ref.1, bf16[2048,256]{1,0:T(8,128)(2,1)} %ow_ref.1, f32[1,256]{1,0:T(1,128)} %bitcast.7, f32[1536,128]{1,0:T(8,128)} %get-tuple-element.19.scale_ref, ...), custom_call_target="tpu_custom_call" | custom-call | flops 3221225472 | bytes 6291456 | tf_op jit(solution)/shard_map/local_kernel/pallas_call | solution.py:411
  63.4 1.7 %copy-done = bf16[1536,768]{1,0:T(8,128)(2,1)S(1)} copy-done((bf16[1536,768]{1,0:T(8,128)(2,1)S(1)}, bf16[1536,768]{1,0:T(8,128)(2,1)}, u32[]{:S(2)}) %copy-start) | copy-done | bytes 2359320
  65.1 1.1 %output_kernel.3 = (bf16[384,256]{1,0:T(8,128)(2,1)S(1)}, bf16[384,256]{1,0:T(8,128)(2,1)S(1)}) custom-call(bf16[8,272,128]{2,1,0:T(8,128)(2,1)S(1)} %all-to-all-done.msgs_ref, f32[2,128,128]{2,1,0:T(8,128)S(1)} %copy-done.3, bf16[1536,768]{1,0:T(8,128)(2,1)S(1)} %copy-done), custom_call_target="tpu_custom_call" | custom-call | flops 100663296 | bytes 1572864 | tf_op jit(solution)/shard_map/output_kernel/pallas_call | solution.py:438
  66.4 1.1 %output_kernel.2 = (bf16[384,256]{1,0:T(8,128)(2,1)S(1)}, bf16[384,256]{1,0:T(8,128)(2,1)S(1)}) custom-call(bf16[8,272,128]{2,1,0:T(8,128)(2,1)S(1)} %all-to-all-done.msgs_ref, f32[2,128,128]{2,1,0:T(8,128)S(1)} %copy-done.3, bf16[1536,768]{1,0:T(8,128)(2,1)S(1)} %copy-done), custom_call_target="tpu_custom_call" | custom-call | flops 100663296 | bytes 1572864 | tf_op jit(solution)/shard_map/output_kernel/pallas_call | solution.py:438
  68.1 1.2 %collective-permute-start.2 = (bf16[384,256]{1,0:T(8,128)(2,1)S(1)}, bf16[384,256]{1,0:T(8,128)(2,1)S(1)}, u32[]{:S(2)}, u32[]{:S(2)}) collective-permute-start(bf16[384,256]{1,0:T(8,128)(2,1)S(1)} %get-tuple-element.24), channel_id=1, source_target_pairs={{0,3},{1,2},{2,1},{3,0},{4,7},{5,6},{6,5},{7,4},{8,11},{9,10},{10,... | collective-permute-start | bytes 589832 | tf_op jit(solution)/shard_map/ppermute | solution.py:306
  69.3 4.3 %project_kernel.2.refs_6_ = bf16[384,2048]{1,0:T(8,128)(2,1)S(1)} custom-call(bf16[384,256]{1,0:T(8,128)(2,1)S(1)} %copy-done.4, bf16[384,256]{1,0:T(8,128)(2,1)S(1)} %collective-permute-done.7.refs_1_, bf16[384,256]{1,0:T(8,128)(2,1)S(1)} %copy-done.6, bf16[384,256]{1,0:T(8,128)(2,1)S(1)} %copy-done.8, bf16[384,256]{1,0:T(8,128)(2,1)S(1)} %get-tuple-element.29.refs_4_, ...), custom_call_target="tpu_custom_call" | custom-call | flops 2415919104 | bytes 7864320 | tf_op jit(solution)/shard_map/project_kernel/pallas_call | solution.py:321
  73.7 1.7 %collective-permute-done.1.refs_0_ = bf16[384,256]{1,0:T(8,128)(2,1)S(1)} collective-permute-done((bf16[384,256]{1,0:T(8,128)(2,1)S(1)}, bf16[384,256]{1,0:T(8,128)(2,1)S(1)}, u32[]{:S(2)}, u32[]{:S(2)}) %collective-permute-start.1) | collective-permute-done | bytes 196640 | tf_op jit(solution)/shard_map/ppermute | solution.py:306
  75.3 3.1 %collective-permute-done.2.refs_1_ = bf16[384,256]{1,0:T(8,128)(2,1)S(1)} collective-permute-done((bf16[384,256]{1,0:T(8,128)(2,1)S(1)}, bf16[384,256]{1,0:T(8,128)(2,1)S(1)}, u32[]{:S(2)}, u32[]{:S(2)}) %collective-permute-start.2) | collective-permute-done | bytes 196640 | tf_op jit(solution)/shard_map/ppermute | solution.py:306
  78.4 3.2 %project_kernel.3 = bf16[384,2048]{1,0:T(8,128)(2,1)} custom-call(bf16[384,256]{1,0:T(8,128)(2,1)S(1)} %collective-permute-done.1.refs_0_, bf16[384,256]{1,0:T(8,128)(2,1)S(1)} %collective-permute-done.2.refs_1_, bf16[128,2048]{1,0:T(8,128)(2,1)S(1)} %collective-permute-done.3.refs_2_, bf16[128,2048]{1,0:T(8,128)(2,1)} %collective-permute-done.4.refs_3_, ...), custom_call_target="tpu_custom_call" | custom-call | flops 805306368 | bytes 3670016 | tf_op jit(solution)/shard_map/project_kernel/pallas_call | solution.py:321
  (36 shorter events, 2.5 us)
Async XLA Ops:
  0.0 30.4 %collective-permute-start.12 = (bf16[256,2048]{1,0:T(8,128)(2,1)}, bf16[256,2048]{1,0:T(8,128)(2,1)S(1)}, u32[]{:S(2)}, u32[]{:S(2)}) collective-permute-start(bf16[256,2048]{1,0:T(8,128)(2,1)} %refs_6_.1), channel_id=1, source_target_pairs={{0,2},{1,3},{2,0},{3,1},{4,6},{5,7},{6,4},{7,5},{8,10},{9,11},{10,... | collective-permute-start | bytes 3145736 | tf_op jit(solution)/shard_map/ppermute | solution.py:306
  1.5 64.7 %collective-permute-start.11 = (bf16[256,2048]{1,0:T(8,128)(2,1)}, bf16[256,2048]{1,0:T(8,128)(2,1)}, u32[]{:S(2)}, u32[]{:S(2)}) collective-permute-start(bf16[256,2048]{1,0:T(8,128)(2,1)} %refs_6_.1), channel_id=1, source_target_pairs={{0,1},{1,0},{2,3},{3,2},{4,5},{5,4},{6,7},{7,6},{8,9},{9,8},{10,11... | collective-permute-start | bytes 3145736 | tf_op jit(solution)/shard_map/ppermute | solution.py:306
  2.3 7.3 %collective-permute-start = (bf16[16,2048]{1,0:T(8,128)(2,1)S(1)}, bf16[16,2048]{1,0:T(8,128)(2,1)S(1)}, u32[]{:S(2)}, u32[]{:S(2)}) collective-permute-start(bf16[16,2048]{1,0:T(8,128)(2,1)S(1)} %slice.3), channel_id=1, source_target_pairs={{0,4},{4,8},{8,12},{12,16},{16,20},{20,24},{24,28},{1,5},{5,9},{9,... | collective-permute-start | bytes 196616 | tf_op jit(solution)/shard_map/ppermute | solution.py:357
  7.7 28.7 %collective-permute-start.3 = (bf16[128,2048]{1,0:T(8,128)(2,1)}, bf16[128,2048]{1,0:T(8,128)(2,1)S(1)}, u32[]{:S(2)}, u32[]{:S(2)}) collective-permute-start(bf16[128,2048]{1,0:T(8,128)(2,1)} %constant_dynamic-slice_fusion), channel_id=1, source_target_pairs={{0,2},{1,3},{2,0},{3,1},{4,6},{5,7},{6,4},{7,5},{8,10},{9,11},{10,... | collective-permute-start | bytes 1572872 | tf_op jit(solution)/shard_map/ppermute | solution.py:306
  10.2 19.7 %copy-start.1 = (bf16[256,2048]{1,0:T(8,128)(2,1)S(1)}, bf16[256,2048]{1,0:T(8,128)(2,1)}, u32[]{:S(2)}) copy-start(bf16[256,2048]{1,0:T(8,128)(2,1)} %refs_10_.1) | copy-start | bytes 3145732
  24.6 38.8 %all-to-all-start = ((bf16[8,272,128]{2,1,0:T(8,128)(2,1)}), bf16[8,272,128]{2,1,0:T(8,128)(2,1)S(1)}, u32[]{:S(2)}, u32[]{:S(2)}) async-start(bf16[8,272,128]{2,1,0:T(8,128)(2,1)} %get-tuple-element.18), calls=%async_computation | async-start | bytes 1114112 | tf_op jit(solution)/shard_map/all_to_all | solution.py:409
  29.9 8.0 %collective-permute-start.7 = (bf16[384,256]{1,0:T(8,128)(2,1)}, bf16[384,256]{1,0:T(8,128)(2,1)S(1)}, u32[]{:S(2)}, u32[]{:S(2)}) collective-permute-start(bf16[384,256]{1,0:T(8,128)(2,1)} %get-tuple-element.26), channel_id=1, source_target_pairs={{0,1},{1,0},{2,3},{3,2},{4,5},{5,4},{6,7},{7,6},{8,9},{9,8},{10,11... | collective-permute-start | bytes 589832 | tf_op jit(solution)/shard_map/ppermute | solution.py:306
  29.9 37.6 %collective-permute-start.14 = (bf16[256,2048]{1,0:T(8,128)(2,1)S(1)}, bf16[256,2048]{1,0:T(8,128)(2,1)}, u32[]{:S(2)}, u32[]{:S(2)}) collective-permute-start(bf16[256,2048]{1,0:T(8,128)(2,1)S(1)} %copy-done.1), channel_id=1, source_target_pairs={{0,1},{1,0},{2,3},{3,2},{4,5},{5,4},{6,7},{7,6},{8,9},{9,8},{10,11... | collective-permute-start | bytes 3145736 | tf_op jit(solution)/shard_map/ppermute | solution.py:306
  30.4 38.9 %collective-permute-start.13 = (bf16[256,2048]{1,0:T(8,128)(2,1)S(1)}, bf16[256,2048]{1,0:T(8,128)(2,1)}, u32[]{:S(2)}, u32[]{:S(2)}) collective-permute-start(bf16[256,2048]{1,0:T(8,128)(2,1)S(1)} %collective-permute-done.12.refs_8_), channel_id=1, source_target_pairs={{0,1},{1,0},{2,3},{3,2},{4,5},{5,4},{6,7},{7,6},{8,9},{9,8},{10,11... | collective-permute-start | bytes 3145736 | tf_op jit(solution)/shard_map/ppermute | solution.py:306
  36.3 16.2 %collective-permute-start.4 = (bf16[128,2048]{1,0:T(8,128)(2,1)S(1)}, bf16[128,2048]{1,0:T(8,128)(2,1)}, u32[]{:S(2)}, u32[]{:S(2)}) collective-permute-start(bf16[128,2048]{1,0:T(8,128)(2,1)S(1)} %collective-permute-done.3.refs_2_), channel_id=1, source_target_pairs={{0,4},{4,0},{8,12},{12,8},{16,20},{20,16},{24,28},{28,24},{1,5},{5... | collective-permute-start | bytes 1572872 | tf_op jit(solution)/shard_map/ppermute | solution.py:306
  37.9 5.9 %collective-permute-start.8 = (bf16[384,256]{1,0:T(8,128)(2,1)}, bf16[384,256]{1,0:T(8,128)(2,1)S(1)}, u32[]{:S(2)}, u32[]{:S(2)}) collective-permute-start(bf16[384,256]{1,0:T(8,128)(2,1)} %get-tuple-element.27), channel_id=1, source_target_pairs={{0,2},{1,3},{2,0},{3,1},{4,6},{5,7},{6,4},{7,5},{8,10},{9,11},{10,... | collective-permute-start | bytes 589832 | tf_op jit(solution)/shard_map/ppermute | solution.py:306
  43.8 0.7 copy-start.5
  44.4 7.4 %collective-permute-start.9 = (bf16[384,256]{1,0:T(8,128)(2,1)}, bf16[384,256]{1,0:T(8,128)(2,1)S(1)}, u32[]{:S(2)}, u32[]{:S(2)}) collective-permute-start(bf16[384,256]{1,0:T(8,128)(2,1)} %get-tuple-element.28), channel_id=1, source_target_pairs={{0,3},{1,2},{2,1},{3,0},{4,7},{5,6},{6,5},{7,4},{8,11},{9,10},{10,... | collective-permute-start | bytes 589832 | tf_op jit(solution)/shard_map/ppermute | solution.py:306
  52.5 21.2 %collective-permute-start.5 = (bf16[128,2048]{1,0:T(8,128)(2,1)S(1)}, bf16[128,2048]{1,0:T(8,128)(2,1)}, u32[]{:S(2)}, u32[]{:S(2)}) collective-permute-start(bf16[128,2048]{1,0:T(8,128)(2,1)S(1)} %collective-permute-done.3.refs_2_), channel_id=1, source_target_pairs={{0,1},{1,0},{2,3},{3,2},{4,5},{5,4},{6,7},{7,6},{8,9},{9,8},{10,11... | collective-permute-start | bytes 1572872 | tf_op jit(solution)/shard_map/ppermute | solution.py:306
  52.6 25.8 %collective-permute-start.6 = (bf16[128,2048]{1,0:T(8,128)(2,1)}, bf16[128,2048]{1,0:T(8,128)(2,1)}, u32[]{:S(2)}, u32[]{:S(2)}) collective-permute-start(bf16[128,2048]{1,0:T(8,128)(2,1)} %collective-permute-done.4.refs_3_), channel_id=1, source_target_pairs={{0,1},{1,0},{2,3},{3,2},{4,5},{5,4},{6,7},{7,6},{8,9},{9,8},{10,11... | collective-permute-start | bytes 1572872 | tf_op jit(solution)/shard_map/ppermute | solution.py:306
  53.0 10.4 %copy-start.3 = (f32[2,128,128]{2,1,0:T(8,128)S(1)}, f32[2,128,128]{2,1,0:T(8,128)}, u32[]{:S(2)}) copy-start(f32[2,128,128]{2,1,0:T(8,128)} %init_ref.3) | copy-start | bytes 393220
  63.4 1.7 %copy-start = (bf16[1536,768]{1,0:T(8,128)(2,1)S(1)}, bf16[1536,768]{1,0:T(8,128)(2,1)}, u32[]{:S(2)}) copy-start(bf16[1536,768]{1,0:T(8,128)(2,1)} %local_kernel.1.parts_ref) | copy-start | bytes 7077892
  65.1 4.2 %copy-start.2 = (bf16[256,2048]{1,0:T(8,128)(2,1)S(1)}, bf16[256,2048]{1,0:T(8,128)(2,1)}, u32[]{:S(2)}) copy-start(bf16[256,2048]{1,0:T(8,128)(2,1)} %refs_6_.1) | copy-start | bytes 3145732
  65.1 4.2 %copy-start.4 = (bf16[384,256]{1,0:T(8,128)(2,1)S(1)}, bf16[384,256]{1,0:T(8,128)(2,1)}, u32[]{:S(2)}) copy-start(bf16[384,256]{1,0:T(8,128)(2,1)} %get-tuple-element.25.refs_0_) | copy-start | bytes 589828
  65.1 4.2 %copy-start.6 = (bf16[384,256]{1,0:T(8,128)(2,1)S(1)}, bf16[384,256]{1,0:T(8,128)(2,1)}, u32[]{:S(2)}) copy-start(bf16[384,256]{1,0:T(8,128)(2,1)} %copy-done.5) | copy-start | bytes 589828
  65.1 4.2 %copy-start.8 = (bf16[384,256]{1,0:T(8,128)(2,1)S(1)}, bf16[384,256]{1,0:T(8,128)(2,1)}, u32[]{:S(2)}) copy-start(bf16[384,256]{1,0:T(8,128)(2,1)} %copy-done.7) | copy-start | bytes 589828
  66.2 1.9 %collective-permute-start.10 = (bf16[384,256]{1,0:T(8,128)(2,1)S(1)}, bf16[384,256]{1,0:T(8,128)(2,1)S(1)}, u32[]{:S(2)}, u32[]{:S(2)}) collective-permute-start(bf16[384,256]{1,0:T(8,128)(2,1)S(1)} %get-tuple-element.30), channel_id=1, source_target_pairs={{0,1},{1,0},{2,3},{3,2},{4,5},{5,4},{6,7},{7,6},{8,9},{9,8},{10,11... | collective-permute-start | bytes 589832 | tf_op jit(solution)/shard_map/ppermute | solution.py:306
  67.5 7.8 %collective-permute-start.1 = (bf16[384,256]{1,0:T(8,128)(2,1)S(1)}, bf16[384,256]{1,0:T(8,128)(2,1)S(1)}, u32[]{:S(2)}, u32[]{:S(2)}) collective-permute-start(bf16[384,256]{1,0:T(8,128)(2,1)S(1)} %get-tuple-element.23), channel_id=1, source_target_pairs={{0,2},{1,3},{2,0},{3,1},{4,6},{5,7},{6,4},{7,5},{8,10},{9,11},{10,... | collective-permute-start | bytes 589832 | tf_op jit(solution)/shard_map/ppermute | solution.py:306
  68.1 10.3 %collective-permute-start.2 = (bf16[384,256]{1,0:T(8,128)(2,1)S(1)}, bf16[384,256]{1,0:T(8,128)(2,1)S(1)}, u32[]{:S(2)}, u32[]{:S(2)}) collective-permute-start(bf16[384,256]{1,0:T(8,128)(2,1)S(1)} %get-tuple-element.24), channel_id=1, source_target_pairs={{0,3},{1,2},{2,1},{3,0},{4,7},{5,6},{6,5},{7,4},{8,11},{9,10},{10,... | collective-permute-start | bytes 589832 | tf_op jit(solution)/shard_map/ppermute | solution.py:306
  (2 other events, 1.3 us)
